TPU v7x, 128 devices: a whole 4x4x4 slice. The times are simulated.
128 devices in a mesh: ra: 16 (over z, x), cb: 4 (over y), dp: 2 (over core).
Axes of the slice: x: 4, y: 4, z: 4, core: 2. Of those that a mesh axis runs over, the one named last changes fastest.
Arguments:
- tokens: bfloat16 [1024, 4096], P('dp', 'ra'), may hold values from -160 to 160, as said below
- first_gain: bfloat16 [4096], P('ra'), may hold values from 0.099609375 to 1.8984375
- first_gate: bfloat16 [4096, 6144], P('ra', 'cb'), may hold values from -0.125 to 0.125
- first_up: bfloat16 [4096, 6144], P('ra', 'cb'), may hold values from -0.125 to 0.125
- first_down: bfloat16 [6144, 4096], P(('cb', 'ra')), may hold values from -0.21875 to 0.21875
- first_branch: bfloat16 [4096], P('ra'), may hold values from 1 to 4
- second_gain: bfloat16 [4096], P('ra'), may hold values from 0.099609375 to 1.8984375
- second_gate: bfloat16 [4096, 6144], P('ra', 'cb'), may hold values from -0.125 to 0.125
- second_up: bfloat16 [4096, 6144], P('ra', 'cb'), may hold values from -0.125 to 0.125
- second_down: bfloat16 [6144, 4096], P(('cb', 'ra')), may hold values from -0.21875 to 0.21875
- second_branch: bfloat16 [4096], P('ra'), may hold values from 1 to 4
Outputs:
- mixed_out: bfloat16 [1024, 4096], P('dp', 'ra')
Inputs may be any that keep to these rules, and one draw needn't show every extreme that they name: `tokens`: activations whose scale varies by token and by feature.
All inputs are finite; a program needn't handle non-finite values.
Results may differ from a plain program's by a relative error of at most 0.035.
Values may be sent and summed in bfloat16 or wider, within the bound.
No kernel may reach another device: no remote copies, remote signals or barrier semaphores. Data moves between devices by JAX's collectives and lax.ppermute only.
A program may use at most 64 MiB of HBM per device.

v0:
```python
import jax
import jax.numpy as jnp
from jax import lax
from jax.experimental import pallas as pl
from jax.experimental.pallas import tpu as pltpu
from jax.sharding import Mesh, PartitionSpec as P

epsilon = 1e-06
residual_scale = 0.25
f32 = jnp.float32
bf16 = jnp.bfloat16
VMEM = pl.BlockSpec(memory_space=pltpu.VMEM)
SMEM = pl.BlockSpec(memory_space=pltpu.SMEM)
ANY = pl.BlockSpec(memory_space=pl.ANY)


def exchange(x, axes):
    return lax.all_to_all(x, axes, 0, 0, tiled=True)


def other_core(x):
    return lax.ppermute(x, "dp", [(0, 1), (1, 0)])


def shifted(x, axis, step):
    return lax.ppermute(x, axis, [(i, (i + step) % 4) for i in range(4)])


def dot(a, b, dims):
    return lax.dot_general(a, b, (dims, ((), ())), preferred_element_type=f32)


def silu(v):
    return v / (1.0 + jnp.exp(-v))


def at_lane(core, half):
    return pl.ds(pl.multiple_of(core * half, 128), half)


def pack(core_ref, z_ref, gate, upward, down1, down2, *refs):
    sends, mine1, mine2, sems = refs[:3], refs[3], refs[4], refs[5]
    core, z = core_ref[0], z_ref[0]
    rows, wide = sends[0].shape
    part, half = wide // 2, mine1.shape[1]
    copies = []
    for step, send in enumerate(sends, 1):
        at = pl.ds(pl.multiple_of(((z + step) % 4) * part, 128), part)
        for side, w in enumerate((gate, upward)):
            source = w.at[pl.ds(core * rows, rows), at]
            copies.append((source, send.at[:, pl.ds(side * part, part)]))
    for w, mine in ((down1, mine1), (down2, mine2)):
        copies.append((w.at[:, at_lane(core, half)], mine))
    copies = [pltpu.make_async_copy(*c, sems.at[i]) for i, c in enumerate(copies)]
    for copy in copies:
        copy.start()
    for copy in copies:
        copy.wait()


def up_part(core_ref, x_ref, z_ref, gate, upward, *refs):
    xs, mine, other = refs[:4], refs[4:7], refs[7:10]
    own, sends, acc, whole, sems = refs[10], refs[11:14], refs[14], refs[15], refs[16]
    core, x, z = core_ref[0], x_ref[0], z_ref[0]
    rows, wide = mine[0].shape
    part = wide // 2
    at = pl.ds(pl.multiple_of(z * part, 128), part)
    copies = [[]]
    for side, w in enumerate((gate, upward)):
        copies[0].append((w.at[:, at], whole.at[0, :, pl.ds(side * part, part)]))
    for step in range(3):
        here = (mine[step], whole.at[step + 1, pl.ds(core * rows, rows), :])
        there = (other[step], whole.at[step + 1, pl.ds((1 - core) * rows, rows), :])
        copies.append([here, there])
    copies = [
        [pltpu.make_async_copy(*c, sems.at[2 * step + i]) for i, c in enumerate(group)]
        for step, group in enumerate(copies)
    ]
    for group in copies:
        for copy in group:
            copy.start()
    total = None
    for step, tokens in enumerate(xs):
        for copy in copies[step]:
            copy.wait()
        one = dot(tokens[...], whole[step], ((1,), (0,)))
        total = one if total is None else total + one
    acc[...] = total
    own[...] = acc[pl.ds(x * 128, 128), :]
    for step, send in enumerate(sends, 1):
        send[...] = acc[pl.ds(((x + step) % 4) * 128, 128), :].astype(bf16)


def down_part(core_ref, x_ref, own, a, b, c, scale, w, *refs):
    mine, other, out, whole, sems = refs[:3], refs[3:6], refs[6], refs[7], refs[8]
    core, x = core_ref[0], x_ref[0]
    rows, full = w.shape
    half = full // 2
    copies = [(w, whole.at[pl.ds(x * rows, rows), :])]
    for step in range(1, 4):
        at = pl.ds(((x + 4 - step) % 4) * rows, rows)
        copies.append((mine[step - 1], whole.at[at, at_lane(core, half)]))
        copies.append((other[step - 1], whole.at[at, at_lane(1 - core, half)]))
    copies = [pltpu.make_async_copy(*c, sems.at[i]) for i, c in enumerate(copies)]
    for copy in copies:
        copy.start()
    both = own[...] + a[...].astype(f32) + b[...].astype(f32) + c[...].astype(f32)
    both = both * scale[...]
    part = both.shape[1] // 2
    hidden = (silu(both[:, :part]) * both[:, part:]).astype(bf16)
    for copy in copies:
        copy.wait()
    out[...] = dot(hidden, whole[...], ((1,), (0,))).astype(bf16)


def join(got, side, branch, gain, send):
    total = jnp.sum(got[...].astype(f32), axis=0)
    middle = (residual_scale * side[...].astype(f32) + 0.5 * branch[...] * total).astype(bf16)
    mid = middle.astype(f32)
    square = jnp.mean(mid * mid, axis=1, keepdims=True)
    normed = (mid * lax.rsqrt(square + epsilon) * gain[...]).astype(bf16)
    full = normed.shape[1]
    width = full // 16
    for x in range(4):
        for z in range(4):
            block = (4 * z + x) * width
            send[4 * x + z, :, :full] = normed
            send[4 * x + z, :, full:] = middle[:, block : block + width]


def feed_forward(core_ref, got, w_down, *refs):
    ups, mine, other, out = refs[:8], refs[8:11], refs[11:14], refs[14]
    tokens, up, whole, up_sems, down_sems = refs[15:]
    core = core_ref[0]
    blocks, cols, width = ups[0].shape
    rows, full = w_down.shape
    half = full // 2
    groups = up_sems.shape[0]
    each = blocks // groups
    up_copies = []
    for group in range(groups):
        at = pl.ds(group * each, each)
        copies = []
        for step in range(4):
            for side, place in enumerate((core, 1 - core)):
                to = up.at[at, pl.ds(step * 2 * cols + place * cols, cols), :]
                source = ups[2 * step + side].at[at]
                copies.append(pltpu.make_async_copy(source, to, up_sems.at[group, 2 * step + side]))
        up_copies.append(copies)
    down_copies = [(w_down, whole.at[pl.ds(0, rows), :])]
    for step in range(1, 4):
        at = pl.ds(step * rows, rows)
        down_copies.append((mine[step - 1], whole.at[at, at_lane(core, half)]))
        down_copies.append((other[step - 1], whole.at[at, at_lane(1 - core, half)]))
    down_copies = [pltpu.make_async_copy(*c, down_sems.at[i]) for i, c in enumerate(down_copies)]
    for copy in [c for copies in up_copies for c in copies] + down_copies:
        copy.start()
    for j in range(got.shape[0]):
        tokens[8 * j : 8 * j + 8, :] = got[j, :, :full]
    total = None
    for group in range(groups):
        for copy in up_copies[group]:
            copy.wait()
        for block in range(group * each, (group + 1) * each):
            part = dot(up[block], tokens[:, block * width : (block + 1) * width], ((1,), (1,)))
            total = part if total is None else total + part
    hidden = []
    for step in range(4):
        gate = total[2 * step * cols : (2 * step + 1) * cols]
        upward = total[(2 * step + 1) * cols : (2 * step + 2) * cols]
        hidden.append(silu(gate) * upward)
    hidden = jnp.concatenate(hidden, 0).T.astype(bf16)
    for copy in down_copies:
        copy.wait()
    for block in range(blocks):
        lanes = slice(block * width, (block + 1) * width)
        out[block] = dot(hidden, whole[:, lanes], ((1,), (0,))).astype(bf16)


def shards(
    tokens,
    first_gain,
    first_gate,
    first_up,
    first_down,
    first_branch,
    second_gain,
    second_gate,
    second_up,
    second_down,
    second_branch,
):
    core, x, y, z = (lax.axis_index(name) for name in ("dp", "rx", "cb", "rz"))
    core_ref, x_ref, z_ref = (i.astype(jnp.int32).reshape(1) for i in (core, x, z))
    n_tok, width = tokens.shape
    full = width * 16
    half = width // 2
    cols = first_gate.shape[1]
    part = cols // 4
    few = n_tok // 4
    w_half = jax.ShapeDtypeStruct((first_down.shape[0], full // 2), bf16)

    def kernel(body, ins, *outs, scratch=(), mib=16):
        flat = list(outs)
        return pl.pallas_call(
            body,
            out_shape=flat if len(flat) > 1 else flat[0],
            in_specs=ins,
            out_specs=[VMEM] * len(flat) if len(flat) > 1 else VMEM,
            scratch_shapes=list(scratch),
            compiler_params=pltpu.CompilerParams(vmem_limit_bytes=mib * 2**20),
        )

    *w1, d1, d2 = kernel(
        pack,
        [SMEM] * 2 + [ANY] * 4,
        *[jax.ShapeDtypeStruct((half, 2 * part), bf16)] * 3,
        w_half,
        w_half,
        scratch=[pltpu.SemaphoreType.DMA((8,))],
    )(core_ref, z_ref, first_gate, first_up, first_down, second_down)
    wide = tokens.astype(f32)
    squares = jnp.sum(wide * wide, axis=1)
    scaled = (wide * first_gain.astype(f32)).astype(bf16)

    w1 = [shifted(w, "rz", step) for step, w in enumerate(w1, 1)]
    x1 = [scaled] + [shifted(scaled, "rz", step) for step in (1, 2, 3)]
    w1_other = [other_core(w) for w in w1]

    rows = tokens.reshape(4, 4, 4, 8, width)
    rows = lax.dynamic_index_in_dim(rows, y, 2, keepdims=False)
    rows = rows.transpose(1, 0, 2, 3).reshape(16, 8, width)
    high = lax.reduce_precision(squares, 8, 7)
    mid = lax.reduce_precision(squares - high, 8, 7)
    low = squares - high - mid
    pieces = [v.astype(bf16).reshape(4, 1, 128) for v in (high, mid, low)]
    sq = jnp.concatenate(
        [jnp.concatenate(pieces[:2], 2), jnp.concatenate([pieces[2], jnp.zeros((4, 1, 128), bf16)], 2)], 1
    )
    sq = jnp.broadcast_to(sq[None], (4, 4, 2, width)).reshape(16, 2, width)
    side = jnp.stack([first_branch, second_gain], 0)
    side = jnp.broadcast_to(side[None], (16, 2, width))
    turned = jnp.where(core == 0, second_gate, second_up).T.reshape(16, cols // 16, width)
    side = jnp.concatenate([turned, rows, side, sq, jnp.zeros((16, 4, width), bf16)], 1)
    side = exchange(side, ("rz", "rx"))
    v1 = side[:, : cols // 16]
    side = side[:, cols // 16 :]
    sq = jnp.sum(side[:, 10:12].astype(f32), axis=0)
    sq = sq[0, :half] + sq[0, half:] + sq[1, :half]
    scale = lax.rsqrt(sq / full + epsilon)[:, None]
    side = side.transpose(1, 0, 2).reshape(16, full)
    rows, branch, gain = side[:8], side[8:9].astype(f32), side[9:10].astype(f32)

    d1 = [shifted(d1, "rx", step) for step in (1, 2, 3)]
    d2 = [shifted(d2, "cb", step) for step in (1, 2, 3)]
    v1 = [v1] + [shifted(v1, "cb", step) for step in (1, 2, 3)]
    d1_other = [other_core(w) for w in d1]
    d2_other = [other_core(w) for w in d2]
    v1 = [w for mine in v1 for w in (mine, other_core(mine))]

    own, *sends = kernel(
        up_part,
        [SMEM] * 3 + [ANY] * 2 + [VMEM] * 4 + [ANY] * 6,
        jax.ShapeDtypeStruct((few, 2 * part), f32),
        *[jax.ShapeDtypeStruct((few, 2 * part), bf16)] * 3,
        scratch=[
            pltpu.VMEM((n_tok, 2 * part), f32),
            pltpu.VMEM((4, width, 2 * part), bf16),
            pltpu.SemaphoreType.DMA((8,)),
        ],
    )(core_ref, x_ref, z_ref, first_gate, first_up, *x1, *w1, *w1_other)
    got = [shifted(send, "rx", step) for step, send in enumerate(sends, 1)]
    partial = kernel(
        down_part,
        [SMEM] * 2 + [VMEM] * 5 + [ANY] * 7,
        jax.ShapeDtypeStruct((few, full), bf16),
        scratch=[pltpu.VMEM((part, full), bf16), pltpu.SemaphoreType.DMA((7,))],
    )(core_ref, x_ref, own, *got, scale, first_down, *d1, *d1_other)
    got = exchange(partial.reshape(16, 8, full), ("rz", "cb"))
    send = kernel(
        join,
        [VMEM] * 4,
        jax.ShapeDtypeStruct((16, 8, full + width), bf16),
    )(got, rows, branch, gain)
    got = exchange(send, ("rx", "rz"))
    middle = got[:, :, full:].reshape(few, width).astype(f32)
    partial = kernel(
        feed_forward,
        [SMEM, VMEM] + [ANY] * 15,
        jax.ShapeDtypeStruct((16, few, width), bf16),
        scratch=[
            pltpu.VMEM((few, full), bf16),
            pltpu.VMEM((16, 2 * part, width), bf16),
            pltpu.VMEM((part, full), bf16),
            pltpu.SemaphoreType.DMA((4, 8)),
            pltpu.SemaphoreType.DMA((7,)),
        ],
        mib=24,
    )(core_ref, got, second_down, *v1, *d2, *d2_other)
    got = exchange(partial, ("rz", "rx"))
    total = jnp.sum(got.astype(f32), axis=0)
    out = (residual_scale * middle + 0.5 * second_branch.astype(f32) * total).astype(bf16)
    parts = [out] + [shifted(out, "cb", step) for step in (1, 2, 3)]
    blocks = []
    for at in range(4):
        back = (y - at) % 4
        block = jnp.where(back == 0, parts[0], jnp.where(back == 1, parts[1], jnp.where(back == 2, parts[2], parts[3])))
        blocks.append(block.reshape(16, 8, width))
    return jnp.stack(blocks, 1).reshape(n_tok, width)


def solution(mesh):
    fine = Mesh(mesh.devices.reshape(4, 4, 4, 2), ("rz", "rx", "cb", "dp"))
    ra = ("rz", "rx")
    vector, up, dn = P(ra), P(ra, "cb"), P(("cb", *ra), None)
    layer = (vector, up, up, dn, vector)
    return jax.shard_map(
        shards,
        mesh=fine,
        in_specs=(P("dp", ra), *layer, *layer),
        out_specs=P("dp", ra),
        check_vma=False,
    )
```

profile of v0, /device:TPU:0, one launch (start us, length us, event | category | flops | bytes accessed | tf_op | source)
XLA Modules:
  0.0 216.5 jit_solution(14968624356418798630)
XLA Ops:
  3.6 4.0 %concatenate.15 = bf16[16,112,256]{2,1,0:T(8,128)(2,1)} concatenate(bf16[16,96,256]{2,1,0:T(8,128)(2,1)S(1)} %bitcast.52, bf16[16,8,256]{2,1,0:T(8,128)(2,1)S(1)} %bitcast.54, bf16[16,2,256]{2,1,0:T(2,128)(2,1)S(1)} %broadcast_in_dim.6, bf16[16,2,256]{2,1,0:T(2,128)(2,1)S(1)} %bitcast.55, bf16[16,4,256]{2,1,0:T(4,128)(2,1)S(1)} %broadcast_in_dim.8), dimensions={1} | concatenate | bytes 1835008 | tf_op jit(solution)/shard_map/concatenate | solution.py:244
  7.7 8.2 %all-to-all-start = ((bf16[16,112,256]{2,1,0:T(8,128)(2,1)}), bf16[16,112,256]{2,1,0:T(8,128)(2,1)}, u32[]{:S(2)}, u32[]{:S(2)}) async-start(bf16[16,112,256]{2,1,0:T(8,128)(2,1)} %concatenate.15), calls=%async_computation | async-start | bytes 1835008 | tf_op jit(solution)/shard_map/all_to_all | solution.py:18
  17.1 1.9 collective-permute-start.3
  21.8 2.2 %collective-permute-start.4 = (bf16[128,768]{1,0:T(8,128)(2,1)S(1)}, bf16[128,768]{1,0:T(8,128)(2,1)}, u32[]{:S(2)}, u32[]{:S(2)}) collective-permute-start(bf16[128,768]{1,0:T(8,128)(2,1)S(1)} %get-tuple-element.15), channel_id=1, source_target_pairs={{0,64},{32,96},{64,0},{96,32},{1,65},{33,97},{65,1},{97,33},{2,66}... | collective-permute-start | bytes 589832 | tf_op jit(solution)/shard_map/ppermute | solution.py:26
  25.8 8.8 %collective-permute-done.3.refs_4_ = bf16[128,768]{1,0:T(8,128)(2,1)S(1)} collective-permute-done((bf16[128,768]{1,0:T(8,128)(2,1)S(1)}, bf16[128,768]{1,0:T(8,128)(2,1)S(1)}, u32[]{:S(2)}, u32[]{:S(2)}) %collective-permute-start.3) | collective-permute-done | bytes 196640 | tf_op jit(solution)/shard_map/ppermute | solution.py:26
  34.6 15.7 %collective-permute-done.4.refs_5_ = bf16[128,768]{1,0:T(8,128)(2,1)} collective-permute-done((bf16[128,768]{1,0:T(8,128)(2,1)S(1)}, bf16[128,768]{1,0:T(8,128)(2,1)}, u32[]{:S(2)}, u32[]{:S(2)}) %collective-permute-start.4) | collective-permute-done | bytes 196640 | tf_op jit(solution)/shard_map/ppermute | solution.py:26
  53.2 2.7 %collective-permute-start.13 = (bf16[96,2048]{1,0:T(8,128)(2,1)}, bf16[96,2048]{1,0:T(8,128)(2,1)}, u32[]{:S(2)}, u32[]{:S(2)}) collective-permute-start(bf16[96,2048]{1,0:T(8,128)(2,1)} %get-tuple-element.21), channel_id=1, source_target_pairs={{0,16},{8,24},{16,0},{24,8},{1,17},{9,25},{17,1},{25,9},{2,18},{10... | collective-permute-start | bytes 1179656 | tf_op jit(solution)/shard_map/ppermute | solution.py:26
  66.1 3.2 %shard_map.110 = (f32[128,768]{1,0:T(8,128)S(1)}, bf16[128,768]{1,0:T(8,128)(2,1)S(1)}, bf16[128,768]{1,0:T(8,128)(2,1)}, bf16[128,768]{1,0:T(8,128)(2,1)}) custom-call(s32[1]{0:T(128)} %bitcast.core_ref, s32[1]{0:T(128)} %bitcast.1.x_ref, s32[1]{0:T(128)} %bitcast.2.z_ref, bf16[256,1536]{1,0:T(8,128)(2,1)S(1)} %copy-done.1, ...), custom_call_target="tpu_custom_call" | custom-call | tf_op jit(solution)/shard_map/pallas_call | solution.py:261
  71.4 2.0 collective-permute-done.13.refs_1_
  74.6 2.6 %collective-permute-start.11 = (bf16[128,768]{1,0:T(8,128)(2,1)}, bf16[128,768]{1,0:T(8,128)(2,1)S(1)}, u32[]{:S(2)}, u32[]{:S(2)}) collective-permute-start(bf16[128,768]{1,0:T(8,128)(2,1)} %get-tuple-element.20), channel_id=1, source_target_pairs={{0,24},{8,0},{16,8},{24,16},{1,25},{9,1},{17,9},{25,17},{2,26},{10... | collective-permute-start | bytes 589832 | tf_op jit(solution)/shard_map/ppermute | solution.py:26
  82.3 5.2 %collective-permute-done.9.a = bf16[128,768]{1,0:T(8,128)(2,1)S(1)} collective-permute-done((bf16[128,768]{1,0:T(8,128)(2,1)}, bf16[128,768]{1,0:T(8,128)(2,1)S(1)}, u32[]{:S(2)}, u32[]{:S(2)}) %collective-permute-start.9) | collective-permute-done | bytes 196640 | tf_op jit(solution)/shard_map/ppermute | solution.py:26
  88.5 3.1 %shard_map.111 = bf16[128,4096]{1,0:T(8,128)(2,1)} custom-call(s32[1]{0:T(128)} %bitcast.core_ref, s32[1]{0:T(128)} %bitcast.1.x_ref, f32[128,768]{1,0:T(8,128)S(1)} %copy-done.19, bf16[128,768]{1,0:T(8,128)(2,1)S(1)} %collective-permute-done.9.a, bf16[128,768]{1,0:T(8,128)(2,1)S(1)} %collective-permute-done.10.b, ...), custom_call_target="tpu_custom_call" | custom-call | tf_op jit(solution)/shard_map/pallas_call | solution.py:273
  91.6 4.6 %all-to-all-start.1 = ((bf16[16,8,4096]{2,1,0:T(8,128)(2,1)}), bf16[16,8,4096]{2,1,0:T(8,128)(2,1)S(1)}, u32[]{:S(2)}, u32[]{:S(2)}) async-start(bf16[16,8,4096]{2,1,0:T(8,128)(2,1)} %bitcast.12), calls=%async_computation.1 | async-start | bytes 2097152 | tf_op jit(solution)/shard_map/all_to_all | solution.py:18
  98.1 2.7 %collective-permute-start.26 = (bf16[96,2048]{1,0:T(8,128)(2,1)}, bf16[96,2048]{1,0:T(8,128)(2,1)S(1)}, u32[]{:S(2)}, u32[]{:S(2)}) collective-permute-start(bf16[96,2048]{1,0:T(8,128)(2,1)} %get-tuple-element.22), channel_id=1, source_target_pairs={{0,4},{2,6},{4,0},{6,2},{1,5},{3,7},{5,1},{7,3},{8,12},{10,14},{12... | collective-permute-start | bytes 1179656 | tf_op jit(solution)/shard_map/ppermute | solution.py:26
  102.0 2.9 %collective-permute-start.21 = (bf16[16,96,256]{2,1,0:T(8,128)(2,1)S(1)}, bf16[16,96,256]{2,1,0:T(8,128)(2,1)}, u32[]{:S(2)}, u32[]{:S(2)}) collective-permute-start(bf16[16,96,256]{2,1,0:T(8,128)(2,1)S(1)} %slice.56.refs_0_), channel_id=1, source_target_pairs={{0,4},{2,6},{4,0},{6,2},{1,5},{3,7},{5,1},{7,3},{8,12},{10,14},{12... | collective-permute-start | bytes 2359304 | tf_op jit(solution)/shard_map/ppermute | solution.py:26
  106.4 18.2 %collective-permute-done.25.refs_8_ = bf16[96,2048]{1,0:T(8,128)(2,1)} collective-permute-done((bf16[96,2048]{1,0:T(8,128)(2,1)}, bf16[96,2048]{1,0:T(8,128)(2,1)}, u32[]{:S(2)}, u32[]{:S(2)}) %collective-permute-start.25) | collective-permute-done | bytes 393248 | tf_op jit(solution)/shard_map/ppermute | solution.py:26
  124.7 4.8 %collective-permute-done.26.refs_9_ = bf16[96,2048]{1,0:T(8,128)(2,1)S(1)} collective-permute-done((bf16[96,2048]{1,0:T(8,128)(2,1)}, bf16[96,2048]{1,0:T(8,128)(2,1)S(1)}, u32[]{:S(2)}, u32[]{:S(2)}) %collective-permute-start.26) | collective-permute-done | bytes 393248 | tf_op jit(solution)/shard_map/ppermute | solution.py:26
  131.7 4.4 %all-to-all-start.2 = ((bf16[16,8,4352]{2,1,0:T(8,128)(2,1)}), bf16[16,8,4352]{2,1,0:T(8,128)(2,1)S(1)}, u32[]{:S(2)}, u32[]{:S(2)}) async-start(bf16[16,8,4352]{2,1,0:T(8,128)(2,1)} %shard_map.112), calls=%async_computation.2 | async-start | bytes 2228224 | tf_op jit(solution)/shard_map/all_to_all | solution.py:18
  136.1 23.1 %collective-permute-done.27.refs_10_ = bf16[96,2048]{1,0:T(8,128)(2,1)} collective-permute-done((bf16[96,2048]{1,0:T(8,128)(2,1)}, bf16[96,2048]{1,0:T(8,128)(2,1)}, u32[]{:S(2)}, u32[]{:S(2)}) %collective-permute-start.27) | collective-permute-done | bytes 393248 | tf_op jit(solution)/shard_map/ppermute | solution.py:26
  162.0 4.2 %collective-permute-done.30.refs_13_ = bf16[96,2048]{1,0:T(8,128)(2,1)S(1)} collective-permute-done((bf16[96,2048]{1,0:T(8,128)(2,1)}, bf16[96,2048]{1,0:T(8,128)(2,1)S(1)}, u32[]{:S(2)}, u32[]{:S(2)}) %collective-permute-start.30) | collective-permute-done | bytes 393248 | tf_op jit(solution)/shard_map/ppermute | solution.py:22
  178.1 7.7 %shard_map.113 = bf16[16,128,256]{2,1,0:T(8,128)(2,1)} custom-call(s32[1]{0:T(128)} %bitcast.core_ref, bf16[16,8,4352]{2,1,0:T(8,128)(2,1)S(1)} %all-to-all-done.2.got, bf16[96,4096]{1,0:T(8,128)(2,1)S(1)} %copy-done, bf16[16,96,256]{2,1,0:T(8,128)(2,1)S(1)} %slice.56.refs_0_, bf16[16,96,256]{2,1,0:T(8,128)(2,1)S(1)} %copy-done.5, ...), custom_call_target="tpu_custom_call" | custom-call | tf_op jit(solution)/shard_map/pallas_call | solution.py:287
  185.9 4.4 %all-to-all-start.3 = ((bf16[16,128,256]{2,1,0:T(8,128)(2,1)}), bf16[16,128,256]{2,1,0:T(8,128)(2,1)S(1)}, u32[]{:S(2)}, u32[]{:S(2)}) async-start(bf16[16,128,256]{2,1,0:T(8,128)(2,1)} %shard_map.113), calls=%async_computation.3 | async-start | bytes 2097152 | tf_op jit(solution)/shard_map/all_to_all | solution.py:18
  190.2 17.8 %all-to-all-done.3 = bf16[16,128,256]{2,1,0:T(8,128)(2,1)S(1)} async-done(((bf16[16,128,256]{2,1,0:T(8,128)(2,1)}), bf16[16,128,256]{2,1,0:T(8,128)(2,1)S(1)}, u32[]{:S(2)}, u32[]{:S(2)}) %all-to-all-start.3) | async-done | bytes 1048608 | tf_op jit(solution)/shard_map/all_to_all | solution.py:18
  211.5 2.2 collective-permute-start.33
  (157 shorter events, 59.8 us)
Async XLA Ops:
  7.7 69.5 %all-to-all-start = ((bf16[16,112,256]{2,1,0:T(8,128)(2,1)}), bf16[16,112,256]{2,1,0:T(8,128)(2,1)}, u32[]{:S(2)}, u32[]{:S(2)}) async-start(bf16[16,112,256]{2,1,0:T(8,128)(2,1)} %concatenate.15), calls=%async_computation | async-start | bytes 1835008 | tf_op jit(solution)/shard_map/all_to_all | solution.py:18
  17.1 17.5 %collective-permute-start.3 = (bf16[128,768]{1,0:T(8,128)(2,1)S(1)}, bf16[128,768]{1,0:T(8,128)(2,1)S(1)}, u32[]{:S(2)}, u32[]{:S(2)}) collective-permute-start(bf16[128,768]{1,0:T(8,128)(2,1)S(1)} %get-tuple-element.14), channel_id=1, source_target_pairs={{0,32},{32,64},{64,96},{96,0},{1,33},{33,65},{65,97},{97,1},{2,34}... | collective-permute-start | bytes 589832 | tf_op jit(solution)/shard_map/ppermute | solution.py:26
  19.0 33.5 %collective-permute-start = (bf16[512,256]{1,0:T(8,128)(2,1)S(1)}, bf16[512,256]{1,0:T(8,128)(2,1)S(1)}, u32[]{:S(2)}, u32[]{:S(2)}) collective-permute-start(bf16[512,256]{1,0:T(8,128)(2,1)S(1)} %get-tuple-element.28.refs_0_), channel_id=1, source_target_pairs={{0,32},{32,64},{64,96},{96,0},{1,33},{33,65},{65,97},{97,1},{2,34}... | collective-permute-start | bytes 786440 | tf_op jit(solution)/shard_map/ppermute | solution.py:26
  20.5 35.4 %collective-permute-start.1 = (bf16[512,256]{1,0:T(8,128)(2,1)S(1)}, bf16[512,256]{1,0:T(8,128)(2,1)S(1)}, u32[]{:S(2)}, u32[]{:S(2)}) collective-permute-start(bf16[512,256]{1,0:T(8,128)(2,1)S(1)} %get-tuple-element.28.refs_0_), channel_id=1, source_target_pairs={{0,64},{32,96},{64,0},{96,32},{1,65},{33,97},{65,1},{97,33},{2,66}... | collective-permute-start | bytes 786440 | tf_op jit(solution)/shard_map/ppermute | solution.py:26
  21.8 28.5 %collective-permute-start.4 = (bf16[128,768]{1,0:T(8,128)(2,1)S(1)}, bf16[128,768]{1,0:T(8,128)(2,1)}, u32[]{:S(2)}, u32[]{:S(2)}) collective-permute-start(bf16[128,768]{1,0:T(8,128)(2,1)S(1)} %get-tuple-element.15), channel_id=1, source_target_pairs={{0,64},{32,96},{64,0},{96,32},{1,65},{33,97},{65,1},{97,33},{2,66}... | collective-permute-start | bytes 589832 | tf_op jit(solution)/shard_map/ppermute | solution.py:26
  24.0 27.0 %collective-permute-start.5 = (bf16[128,768]{1,0:T(8,128)(2,1)S(1)}, bf16[128,768]{1,0:T(8,128)(2,1)}, u32[]{:S(2)}, u32[]{:S(2)}) collective-permute-start(bf16[128,768]{1,0:T(8,128)(2,1)S(1)} %get-tuple-element.16), channel_id=1, source_target_pairs={{0,96},{32,0},{64,32},{96,64},{1,97},{33,1},{65,33},{97,65},{2,98}... | collective-permute-start | bytes 589832 | tf_op jit(solution)/shard_map/ppermute | solution.py:26
  34.6 23.5 %collective-permute-start.2 = (bf16[512,256]{1,0:T(8,128)(2,1)S(1)}, bf16[512,256]{1,0:T(8,128)(2,1)S(1)}, u32[]{:S(2)}, u32[]{:S(2)}) collective-permute-start(bf16[512,256]{1,0:T(8,128)(2,1)S(1)} %get-tuple-element.28.refs_0_), channel_id=1, source_target_pairs={{0,96},{32,0},{64,32},{96,64},{1,97},{33,1},{65,33},{97,65},{2,98}... | collective-permute-start | bytes 786440 | tf_op jit(solution)/shard_map/ppermute | solution.py:26
  51.0 20.3 %collective-permute-start.12 = (bf16[96,2048]{1,0:T(8,128)(2,1)}, bf16[96,2048]{1,0:T(8,128)(2,1)}, u32[]{:S(2)}, u32[]{:S(2)}) collective-permute-start(bf16[96,2048]{1,0:T(8,128)(2,1)} %get-tuple-element.21), channel_id=1, source_target_pairs={{0,8},{8,16},{16,24},{24,0},{1,9},{9,17},{17,25},{25,1},{2,10},{10... | collective-permute-start | bytes 1179656 | tf_op jit(solution)/shard_map/ppermute | solution.py:26
  53.2 20.2 %collective-permute-start.13 = (bf16[96,2048]{1,0:T(8,128)(2,1)}, bf16[96,2048]{1,0:T(8,128)(2,1)}, u32[]{:S(2)}, u32[]{:S(2)}) collective-permute-start(bf16[96,2048]{1,0:T(8,128)(2,1)} %get-tuple-element.21), channel_id=1, source_target_pairs={{0,16},{8,24},{16,0},{24,8},{1,17},{9,25},{17,1},{25,9},{2,18},{10... | collective-permute-start | bytes 1179656 | tf_op jit(solution)/shard_map/ppermute | solution.py:26
  56.5 18.0 %collective-permute-start.14 = (bf16[96,2048]{1,0:T(8,128)(2,1)}, bf16[96,2048]{1,0:T(8,128)(2,1)}, u32[]{:S(2)}, u32[]{:S(2)}) collective-permute-start(bf16[96,2048]{1,0:T(8,128)(2,1)} %get-tuple-element.21), channel_id=1, source_target_pairs={{0,24},{8,0},{16,8},{24,16},{1,25},{9,1},{17,9},{25,17},{2,26},{10... | collective-permute-start | bytes 1179656 | tf_op jit(solution)/shard_map/ppermute | solution.py:26
  71.3 16.1 %collective-permute-start.15 = (bf16[96,2048]{1,0:T(8,128)(2,1)}, bf16[96,2048]{1,0:T(8,128)(2,1)S(1)}, u32[]{:S(2)}, u32[]{:S(2)}) collective-permute-start(bf16[96,2048]{1,0:T(8,128)(2,1)} %collective-permute-done.12.refs_0_), channel_id=1, source_target_pairs={{0,1},{1,0},{2,3},{3,2},{4,5},{5,4},{6,7},{7,6},{8,9},{9,8},{10,11... | collective-permute-start | bytes 1179656 | tf_op jit(solution)/shard_map/ppermute | solution.py:22
  73.4 14.1 %collective-permute-start.16 = (bf16[96,2048]{1,0:T(8,128)(2,1)}, bf16[96,2048]{1,0:T(8,128)(2,1)S(1)}, u32[]{:S(2)}, u32[]{:S(2)}) collective-permute-start(bf16[96,2048]{1,0:T(8,128)(2,1)} %collective-permute-done.13.refs_1_), channel_id=1, source_target_pairs={{0,1},{1,0},{2,3},{3,2},{4,5},{5,4},{6,7},{7,6},{8,9},{9,8},{10,11... | collective-permute-start | bytes 1179656 | tf_op jit(solution)/shard_map/ppermute | solution.py:22
  74.6 12.9 %collective-permute-start.17 = (bf16[96,2048]{1,0:T(8,128)(2,1)}, bf16[96,2048]{1,0:T(8,128)(2,1)S(1)}, u32[]{:S(2)}, u32[]{:S(2)}) collective-permute-start(bf16[96,2048]{1,0:T(8,128)(2,1)} %collective-permute-done.14.refs_2_), channel_id=1, source_target_pairs={{0,1},{1,0},{2,3},{3,2},{4,5},{5,4},{6,7},{7,6},{8,9},{9,8},{10,11... | collective-permute-start | bytes 1179656 | tf_op jit(solution)/shard_map/ppermute | solution.py:22
  91.6 38.7 %all-to-all-start.1 = ((bf16[16,8,4096]{2,1,0:T(8,128)(2,1)}), bf16[16,8,4096]{2,1,0:T(8,128)(2,1)S(1)}, u32[]{:S(2)}, u32[]{:S(2)}) async-start(bf16[16,8,4096]{2,1,0:T(8,128)(2,1)} %bitcast.12), calls=%async_computation.1 | async-start | bytes 2097152 | tf_op jit(solution)/shard_map/all_to_all | solution.py:18
  96.2 28.5 %collective-permute-start.25 = (bf16[96,2048]{1,0:T(8,128)(2,1)}, bf16[96,2048]{1,0:T(8,128)(2,1)}, u32[]{:S(2)}, u32[]{:S(2)}) collective-permute-start(bf16[96,2048]{1,0:T(8,128)(2,1)} %get-tuple-element.22), channel_id=1, source_target_pairs={{0,2},{2,4},{4,6},{6,0},{1,3},{3,5},{5,7},{7,1},{8,10},{10,12},{12... | collective-permute-start | bytes 1179656 | tf_op jit(solution)/shard_map/ppermute | solution.py:26
  98.1 31.4 %collective-permute-start.26 = (bf16[96,2048]{1,0:T(8,128)(2,1)}, bf16[96,2048]{1,0:T(8,128)(2,1)S(1)}, u32[]{:S(2)}, u32[]{:S(2)}) collective-permute-start(bf16[96,2048]{1,0:T(8,128)(2,1)} %get-tuple-element.22), channel_id=1, source_target_pairs={{0,4},{2,6},{4,0},{6,2},{1,5},{3,7},{5,1},{7,3},{8,12},{10,14},{12... | collective-permute-start | bytes 1179656 | tf_op jit(solution)/shard_map/ppermute | solution.py:26
  101.9 57.8 %collective-permute-start.19 = (bf16[16,96,256]{2,1,0:T(8,128)(2,1)S(1)}, bf16[16,96,256]{2,1,0:T(8,128)(2,1)S(1)}, u32[]{:S(2)}, u32[]{:S(2)}) collective-permute-start(bf16[16,96,256]{2,1,0:T(8,128)(2,1)S(1)} %slice.56.refs_0_), channel_id=1, source_target_pairs={{0,2},{2,4},{4,6},{6,0},{1,3},{3,5},{5,7},{7,1},{8,10},{10,12},{12... | collective-permute-start | bytes 2359304 | tf_op jit(solution)/shard_map/ppermute | solution.py:26
  102.0 58.7 %collective-permute-start.21 = (bf16[16,96,256]{2,1,0:T(8,128)(2,1)S(1)}, bf16[16,96,256]{2,1,0:T(8,128)(2,1)}, u32[]{:S(2)}, u32[]{:S(2)}) collective-permute-start(bf16[16,96,256]{2,1,0:T(8,128)(2,1)S(1)} %slice.56.refs_0_), channel_id=1, source_target_pairs={{0,4},{2,6},{4,0},{6,2},{1,5},{3,7},{5,1},{7,3},{8,12},{10,14},{12... | collective-permute-start | bytes 2359304 | tf_op jit(solution)/shard_map/ppermute | solution.py:26
  104.9 55.8 %collective-permute-start.23 = (bf16[16,96,256]{2,1,0:T(8,128)(2,1)S(1)}, bf16[16,96,256]{2,1,0:T(8,128)(2,1)}, u32[]{:S(2)}, u32[]{:S(2)}) collective-permute-start(bf16[16,96,256]{2,1,0:T(8,128)(2,1)S(1)} %slice.56.refs_0_), channel_id=1, source_target_pairs={{0,6},{2,0},{4,2},{6,4},{1,7},{3,1},{5,3},{7,5},{8,14},{10,8},{12,... | collective-permute-start | bytes 2359304 | tf_op jit(solution)/shard_map/ppermute | solution.py:26
  124.7 34.5 %collective-permute-start.27 = (bf16[96,2048]{1,0:T(8,128)(2,1)}, bf16[96,2048]{1,0:T(8,128)(2,1)}, u32[]{:S(2)}, u32[]{:S(2)}) collective-permute-start(bf16[96,2048]{1,0:T(8,128)(2,1)} %get-tuple-element.22), channel_id=1, source_target_pairs={{0,6},{2,0},{4,2},{6,4},{1,7},{3,1},{5,3},{7,5},{8,14},{10,8},{12,... | collective-permute-start | bytes 1179656 | tf_op jit(solution)/shard_map/ppermute | solution.py:26
  129.5 29.7 %collective-permute-start.28 = (bf16[96,2048]{1,0:T(8,128)(2,1)}, bf16[96,2048]{1,0:T(8,128)(2,1)}, u32[]{:S(2)}, u32[]{:S(2)}) collective-permute-start(bf16[96,2048]{1,0:T(8,128)(2,1)} %collective-permute-done.25.refs_8_), channel_id=1, source_target_pairs={{0,1},{1,0},{2,3},{3,2},{4,5},{5,4},{6,7},{7,6},{8,9},{9,8},{10,11... | collective-permute-start | bytes 1179656 | tf_op jit(solution)/shard_map/ppermute | solution.py:22
  131.7 38.9 %all-to-all-start.2 = ((bf16[16,8,4352]{2,1,0:T(8,128)(2,1)}), bf16[16,8,4352]{2,1,0:T(8,128)(2,1)S(1)}, u32[]{:S(2)}, u32[]{:S(2)}) async-start(bf16[16,8,4352]{2,1,0:T(8,128)(2,1)} %shard_map.112), calls=%async_computation.2 | async-start | bytes 2228224 | tf_op jit(solution)/shard_map/all_to_all | solution.py:18
  160.7 9.0 %collective-permute-start.24 = (bf16[16,96,256]{2,1,0:T(8,128)(2,1)}, bf16[16,96,256]{2,1,0:T(8,128)(2,1)S(1)}, u32[]{:S(2)}, u32[]{:S(2)}) collective-permute-start(bf16[16,96,256]{2,1,0:T(8,128)(2,1)} %collective-permute-done.23.refs_6_), channel_id=1, source_target_pairs={{0,1},{1,0},{2,3},{3,2},{4,5},{5,4},{6,7},{7,6},{8,9},{9,8},{10,11... | collective-permute-start | bytes 2359304 | tf_op jit(solution)/shard_map/ppermute | solution.py:22
  185.9 22.2 %all-to-all-start.3 = ((bf16[16,128,256]{2,1,0:T(8,128)(2,1)}), bf16[16,128,256]{2,1,0:T(8,128)(2,1)S(1)}, u32[]{:S(2)}, u32[]{:S(2)}) async-start(bf16[16,128,256]{2,1,0:T(8,128)(2,1)} %shard_map.113), calls=%async_computation.3 | async-start | bytes 2097152 | tf_op jit(solution)/shard_map/all_to_all | solution.py:18
  (49 other events, 155.9 us)
where the time goes:
time: 218 us; the launch traced here: 217 us
  waiting for transfers between devices  108 us (50%)
  starting transfers between devices  55.3 us (25%)
  local copies, waits for them, and re-layouts  31.9 us (15%)
  Pallas kernels  16.6 us (8%)
  other arithmetic  3.81 us (2%)
    ppermute x21, waiting for transfers between devices, shifted(): return lax.ppermute(x, axis, [(i, (i + step) % 4) for i in range(4)])  85.1 us
    ppermute x21, starting transfers between devices, shifted(): return lax.ppermute(x, axis, [(i, (i + step) % 4) for i in range(4)])  32.1 us
    unnamed x70, local copies, waits for them, and re-layouts  24.5 us
    all_to_all x4, starting transfers between devices, exchange(): return lax.all_to_all(x, axes, 0, 0, tiled=True)  21.5 us
    all_to_all x4, waiting for transfers between devices, exchange(): return lax.all_to_all(x, axes, 0, 0, tiled=True)  17.8 us
    pallas_call x1, Pallas kernels, shards(): kernel(feed_forward, [SMEM, VMEM] + [ANY] * 15, jax.ShapeDtypeStruct((16,...  7.72 us
    ppermute x13, waiting for transfers between devices, other_core(): return lax.ppermute(x, 'dp', [(0, 1), (1, 0)])  5.59 us
  transfers between devices with their start and end apart: 38, of which 18 were waited for; matrix products, arithmetic and copies ran while one was open for 1% of the time, Pallas kernels for 3%

commit v1 on v0

v1 whole, which is shorter than its diff:
```python
import jax
import jax.numpy as jnp
from jax import lax
from jax.experimental import pallas as pl
from jax.experimental.pallas import tpu as pltpu
from jax.sharding import Mesh, PartitionSpec as P

epsilon = 1e-06
residual_scale = 0.25
f32 = jnp.float32
bf16 = jnp.bfloat16
VMEM = pl.BlockSpec(memory_space=pltpu.VMEM)
SMEM = pl.BlockSpec(memory_space=pltpu.SMEM)
HBM = pl.BlockSpec(memory_space=pltpu.HBM)


def exchange(x, axes):
    return lax.all_to_all(x, axes, 0, 0, tiled=True)


def other_core(x):
    return lax.ppermute(x, "dp", [(0, 1), (1, 0)])


def shifted(x, axis, step):
    return lax.ppermute(x, axis, [(i, (i + step) % 4) for i in range(4)])


def dot(a, b, dims):
    return lax.dot_general(a, b, (dims, ((), ())), preferred_element_type=f32)


def silu(v):
    return v / (1.0 + jnp.exp(-v))


def at_lane(core, half):
    return pl.ds(pl.multiple_of(core * half, 128), half)


def together(pairs, sems):
    copies = [pltpu.make_async_copy(*pair, sems.at[i]) for i, pair in enumerate(pairs)]
    for copy in copies:
        copy.start()
    return copies


def wait_for(copies):
    for copy in copies:
        copy.wait()


def pack(core_ref, z_ref, gain, tokens, gate, upward, down1, down2, *refs):
    sends, mine1, mine2, scaled, here, sems = refs[:3], refs[3], refs[4], refs[5], refs[6], refs[7]
    core, z = core_ref[0], z_ref[0]
    rows, wide = sends[0].shape
    part, half = wide // 2, mine1.shape[1]
    pairs = [(tokens, here)]
    for step, send in enumerate(sends, 1):
        at = pl.ds(pl.multiple_of(((z + step) % 4) * part, 128), part)
        for side, w in enumerate((gate, upward)):
            source = w.at[pl.ds(core * rows, rows), at]
            pairs.append((source, send.at[:, pl.ds(side * part, part)]))
    for w, mine in ((down1, mine1), (down2, mine2)):
        pairs.append((w.at[:, at_lane(core, half)], mine))
    copies = together(pairs, sems)
    copies[0].wait()
    scaled[...] = (here[...].astype(f32) * gain[...].astype(f32)).astype(bf16)
    wait_for(copies[1:])


def message(core_ref, y_ref, branch, gain, here, tokens, gate, upward, out, picked, sems):
    core, y = core_ref[0], y_ref[0]
    width, cols = picked.shape
    each = cols // 16

    @pl.when(core == 0)
    def _():
        pltpu.make_async_copy(gate, picked, sems.at[16]).start()

    @pl.when(core == 1)
    def _():
        pltpu.make_async_copy(upward, picked, sems.at[16]).start()

    pairs = []
    for z in range(4):
        for x in range(4):
            source = tokens.at[pl.ds(x * 128 + 32 * z + 8 * y, 8), :]
            pairs.append((source, out.at[4 * z + x, pl.ds(each, 8), :]))
    copies = together(pairs, sems)
    wide = here[...].astype(f32)
    squares = lax.dot_general(
        jnp.ones((8, width), f32),
        wide * wide,
        (((1,), (1,)), ((), ())),
        precision=lax.Precision.HIGHEST,
        preferred_element_type=f32,
    )
    high = squares.astype(bf16).astype(f32)
    mid = (squares - high).astype(bf16).astype(f32)
    low = squares - high - mid
    row = lax.broadcasted_iota(jnp.int32, (8, width), 0)
    fixed = jnp.where(row == 0, branch[...].astype(f32), jnp.where(row == 1, gain[...].astype(f32), 0.0))
    blocks = []
    for x in range(4):
        at = slice(128 * x, 128 * x + 128)
        first = jnp.concatenate([high[:, at], mid[:, at]], 1)
        second = jnp.concatenate([low[:, at], jnp.zeros_like(low[:, at])], 1)
        blocks.append(jnp.where(row == 2, first, jnp.where(row == 3, second, fixed)).astype(bf16))
    pltpu.make_async_copy(gate, picked, sems.at[16]).wait()
    turned = picked[...].T
    for z in range(4):
        for x in range(4):
            to = 4 * z + x
            out[to, :each, :] = turned[to * each : (to + 1) * each, :]
            out[to, each + 8 :, :] = blocks[x]
    wait_for(copies)


def up_part(core_ref, x_ref, z_ref, first_x, gate, upward, *refs):
    xs, mine, other = refs[:3], refs[3:6], refs[6:9]
    own, sends, acc, whole, held, sems = refs[9], refs[10:13], refs[13], refs[14], refs[15], refs[16]
    core, x, z = core_ref[0], x_ref[0], z_ref[0]
    rows, wide = mine[0].shape
    part = wide // 2
    at = pl.ds(pl.multiple_of(z * part, 128), part)
    copies = [[]]
    for side, w in enumerate((gate, upward)):
        copies[0].append((w.at[:, at], whole.at[0, :, pl.ds(side * part, part)]))
    for step in range(3):
        here = (mine[step], whole.at[step + 1, pl.ds(core * rows, rows), :])
        there = (other[step], whole.at[step + 1, pl.ds((1 - core) * rows, rows), :])
        copies.append([here, there, (xs[step], held.at[step])])
    copies = [together(group, sems.at[step]) for step, group in enumerate(copies)]
    total = None
    for step in range(4):
        wait_for(copies[step])
        tokens = held[step - 1] if step else first_x[...]
        one = dot(tokens, whole[step], ((1,), (0,)))
        total = one if total is None else total + one
    acc[...] = total
    own[...] = acc[pl.ds(x * 128, 128), :]
    for step, send in enumerate(sends, 1):
        send[...] = acc[pl.ds(((x + step) % 4) * 128, 128), :].astype(bf16)


def down_part(core_ref, x_ref, own, a, b, c, side, w, *refs):
    mine, other, out, whole, small, sems = refs[:3], refs[3:6], refs[6], refs[7], refs[8], refs[9]
    core, x = core_ref[0], x_ref[0]
    rows, full = w.shape
    half = full // 2
    copies = [(side.at[:, pl.ds(rows, 16), :], small), (w, whole.at[pl.ds(x * rows, rows), :])]
    for step in range(1, 4):
        at = pl.ds(((x + 4 - step) % 4) * rows, rows)
        copies.append((mine[step - 1], whole.at[at, at_lane(core, half)]))
        copies.append((other[step - 1], whole.at[at, at_lane(1 - core, half)]))
    copies = together(copies, sems)
    both = own[...] + a[...].astype(f32) + b[...].astype(f32) + c[...].astype(f32)
    copies[0].wait()
    squares = jnp.sum(small[...].astype(f32), axis=0)[10:12]
    squares = squares[0:1, :128] + squares[0:1, 128:] + squares[1:2, :128]
    scale = lax.rsqrt(squares / full + epsilon)
    both = both * jnp.broadcast_to(scale, (8, 128)).T[:, :1]
    part = both.shape[1] // 2
    hidden = (silu(both[:, :part]) * both[:, part:]).astype(bf16)
    wait_for(copies[1:])
    out[...] = dot(hidden, whole[...], ((1,), (0,))).astype(bf16)


def join(got, side, send, small, sem):
    copy = pltpu.make_async_copy(side.at[:, pl.ds(side.shape[1] - 16, 16), :], small, sem)
    copy.start()
    total = jnp.sum(got[...].astype(f32), axis=0)
    copy.wait()
    blocks = [small[i].astype(f32) for i in range(16)]
    tokens, branch, gain = (jnp.concatenate([b[at] for b in blocks], 1) for at in (slice(0, 8), slice(8, 9), slice(9, 10)))
    middle = (residual_scale * tokens + 0.5 * branch * total).astype(bf16)
    mid = middle.astype(f32)
    square = jnp.mean(mid * mid, axis=1, keepdims=True)
    normed = (mid * lax.rsqrt(square + epsilon) * gain).astype(bf16)
    full = normed.shape[1]
    width = full // 16
    for x in range(4):
        for z in range(4):
            block = (4 * z + x) * width
            send[4 * x + z, :, :full] = normed
            send[4 * x + z, :, full:] = middle[:, block : block + width]


def finish(got, branch, send, out, middle, sems):
    count, rows = send.shape[:2]
    width = out.shape[1]
    pairs = [(send.at[:, :, pl.ds(send.shape[2] - width, width)], middle)]
    copies = together(pairs, sems)
    total = jnp.sum(got[...].astype(f32), axis=0)
    wait_for(copies)
    for j in range(count):
        at = slice(j * rows, (j + 1) * rows)
        mid = middle[j].astype(f32)
        out[at, :] = (residual_scale * mid + 0.5 * branch[...].astype(f32) * total[at]).astype(bf16)


def feed_forward(core_ref, got, w_down, *refs):
    ups, mine, other, out = refs[:8], refs[8:11], refs[11:14], refs[14]
    tokens, up, whole, up_sems, down_sems = refs[15:]
    core = core_ref[0]
    blocks, cols, width = ups[0].shape
    rows, full = w_down.shape
    half = full // 2
    groups = up_sems.shape[0]
    each = blocks // groups
    up_copies = []
    for group in range(groups):
        at = pl.ds(group * each, each)
        copies = []
        for step in range(4):
            for side, place in enumerate((core, 1 - core)):
                to = up.at[at, pl.ds(step * 2 * cols + place * cols, cols), :]
                source = ups[2 * step + side].at[at]
                copies.append(pltpu.make_async_copy(source, to, up_sems.at[group, 2 * step + side]))
        up_copies.append(copies)
    down_copies = [(w_down, whole.at[pl.ds(0, rows), :])]
    for step in range(1, 4):
        at = pl.ds(step * rows, rows)
        down_copies.append((mine[step - 1], whole.at[at, at_lane(core, half)]))
        down_copies.append((other[step - 1], whole.at[at, at_lane(1 - core, half)]))
    down_copies = [pltpu.make_async_copy(*c, down_sems.at[i]) for i, c in enumerate(down_copies)]
    for copy in [c for copies in up_copies for c in copies] + down_copies:
        copy.start()
    for j in range(got.shape[0]):
        tokens[8 * j : 8 * j + 8, :] = got[j, :, :full]
    total = None
    for group in range(groups):
        for copy in up_copies[group]:
            copy.wait()
        for block in range(group * each, (group + 1) * each):
            part = dot(up[block], tokens[:, block * width : (block + 1) * width], ((1,), (1,)))
            total = part if total is None else total + part
    hidden = []
    for step in range(4):
        gate = total[2 * step * cols : (2 * step + 1) * cols]
        upward = total[(2 * step + 1) * cols : (2 * step + 2) * cols]
        hidden.append(silu(gate) * upward)
    hidden = jnp.concatenate(hidden, 0).T.astype(bf16)
    for copy in down_copies:
        copy.wait()
    for block in range(blocks):
        lanes = slice(block * width, (block + 1) * width)
        out[block] = dot(hidden, whole[:, lanes], ((1,), (0,))).astype(bf16)


def shards(
    tokens,
    first_gain,
    first_gate,
    first_up,
    first_down,
    first_branch,
    second_gain,
    second_gate,
    second_up,
    second_down,
    second_branch,
):
    core, x, y, z = (lax.axis_index(name) for name in ("dp", "rx", "cb", "rz"))
    core_ref, x_ref, y_ref, z_ref = (i.astype(jnp.int32).reshape(1) for i in (core, x, y, z))
    n_tok, width = tokens.shape
    full = width * 16
    half = width // 2
    cols = first_gate.shape[1]
    part = cols // 4
    few = n_tok // 4
    w_half = jax.ShapeDtypeStruct((first_down.shape[0], full // 2), bf16)

    def kernel(body, ins, *outs, scratch=(), mib=16):
        call = pl.pallas_call(
            body,
            out_shape=list(outs) if len(outs) > 1 else outs[0],
            in_specs=ins,
            out_specs=[VMEM] * len(outs) if len(outs) > 1 else VMEM,
            scratch_shapes=list(scratch),
            compiler_params=pltpu.CompilerParams(vmem_limit_bytes=mib * 2**20),
        )

        def run(*args):
            kept = [pltpu.with_memory_space_constraint(a, pltpu.HBM) if spec is HBM else a for a, spec in zip(args, ins)]
            return call(*kept)

        return run

    dma = pltpu.SemaphoreType.DMA

    *w1, d1, d2, scaled = kernel(
        pack,
        [SMEM] * 2 + [VMEM] + [HBM] * 5,
        *[jax.ShapeDtypeStruct((half, 2 * part), bf16)] * 3,
        w_half,
        w_half,
        jax.ShapeDtypeStruct(tokens.shape, bf16),
        scratch=[pltpu.VMEM(tokens.shape, bf16), dma((9,))],
    )(core_ref, z_ref, first_gain[None], tokens, first_gate, first_up, first_down, second_down)
    w1 = [shifted(w, "rz", step) for step, w in enumerate(w1, 1)]
    x1 = [scaled] + [shifted(scaled, "rz", step) for step in (1, 2, 3)]
    w1_other = [other_core(w) for w in w1]

    side = kernel(
        message,
        [SMEM] * 2 + [VMEM] * 3 + [HBM] * 3,
        jax.ShapeDtypeStruct((16, cols // 16 + 16, width), bf16),
        scratch=[pltpu.VMEM((width, cols), bf16), dma((17,))],
    )(core_ref, y_ref, first_branch[None], second_gain[None], tokens, tokens, second_gate, second_up)
    side = exchange(side, ("rz", "rx"))
    v1 = side[:, : cols // 16]

    d1 = [shifted(d1, "rx", step) for step in (1, 2, 3)]
    d2 = [shifted(d2, "cb", step) for step in (1, 2, 3)]
    v1 = [v1] + [shifted(v1, "cb", step) for step in (1, 2, 3)]
    d1_other = [other_core(w) for w in d1]
    d2_other = [other_core(w) for w in d2]
    v1 = [w for mine in v1 for w in (mine, other_core(mine))]

    own, *sends = kernel(
        up_part,
        [SMEM] * 3 + [VMEM] + [HBM] * 11,
        jax.ShapeDtypeStruct((few, 2 * part), f32),
        *[jax.ShapeDtypeStruct((few, 2 * part), bf16)] * 3,
        scratch=[
            pltpu.VMEM((n_tok, 2 * part), f32),
            pltpu.VMEM((4, width, 2 * part), bf16),
            pltpu.VMEM((3, n_tok, width), bf16),
            dma((4, 3)),
        ],
    )(core_ref, x_ref, z_ref, x1[0], first_gate, first_up, *x1[1:], *w1, *w1_other)
    got = [shifted(send, "rx", step) for step, send in enumerate(sends, 1)]
    partial = kernel(
        down_part,
        [SMEM] * 2 + [VMEM] * 4 + [HBM] * 8,
        jax.ShapeDtypeStruct((few, full), bf16),
        scratch=[pltpu.VMEM((part, full), bf16), pltpu.VMEM((16, 16, width), bf16), dma((8,))],
    )(core_ref, x_ref, own, *got, side, first_down, *d1, *d1_other)
    got = exchange(partial.reshape(16, 8, full), ("rz", "cb"))
    send = kernel(
        join,
        [VMEM, HBM],
        jax.ShapeDtypeStruct((16, 8, full + width), bf16),
        scratch=[pltpu.VMEM((16, 16, width), bf16), dma(())],
    )(got, side)
    rows = exchange(send, ("rx", "rz"))
    partial = kernel(
        feed_forward,
        [SMEM, VMEM] + [HBM] * 15,
        jax.ShapeDtypeStruct((16, few, width), bf16),
        scratch=[
            pltpu.VMEM((few, full), bf16),
            pltpu.VMEM((16, 2 * part, width), bf16),
            pltpu.VMEM((part, full), bf16),
            dma((4, 8)),
            dma((7,)),
        ],
        mib=24,
    )(core_ref, rows, second_down, *v1, *d2, *d2_other)
    partial, branch = lax.optimization_barrier((partial, second_branch[None]))
    got = exchange(partial, ("rz", "rx"))
    out = kernel(
        finish,
        [VMEM, VMEM, HBM],
        jax.ShapeDtypeStruct((few, width), bf16),
        scratch=[pltpu.VMEM((16, 8, width), bf16), dma((1,))],
    )(got, branch, rows)
    parts = [out] + [shifted(out, "cb", step) for step in (1, 2, 3)]
    blocks = []
    for at in range(4):
        back = (y - at) % 4
        block = jnp.where(back == 0, parts[0], jnp.where(back == 1, parts[1], jnp.where(back == 2, parts[2], parts[3])))
        blocks.append(block.reshape(16, 8, width))
    return jnp.stack(blocks, 1).reshape(n_tok, width)


def solution(mesh):
    fine = Mesh(mesh.devices.reshape(4, 4, 4, 2), ("rz", "rx", "cb", "dp"))
    ra = ("rz", "rx")
    vector, up, dn = P(ra), P(ra, "cb"), P(("cb", *ra), None)
    layer = (vector, up, up, dn, vector)
    return jax.shard_map(
        shards,
        mesh=fine,
        in_specs=(P("dp", ra), *layer, *layer),
        out_specs=P("dp", ra),
        check_vma=False,
    )
```

time: 218 us -> 192 us (0.88)
  local copies, waits for them, and re-layouts: 31.9 us -> 8.66 us
  waiting for transfers between devices: 108 us -> 85.4 us
  blocking collectives: 0 us -> 21.6 us
  Pallas kernels: 16.6 us -> 21.3 us
  other arithmetic: 3.81 us -> 0.07 us
    all_to_all x0 -> x1, blocking collectives: none -> 21.6 us  [exchange(): return lax.all_to_all(x, axes, 0, 0, tiled=True)]
    all_to_all x4 -> x3, waiting for transfers between devices: 17.8 us -> 0.01 us  [exchange(): return lax.all_to_all(x, axes, 0, 0, tiled=True)]
    unnamed x70 -> x42, local copies, waits for them, and re-layouts: 24.5 us -> 7.19 us
    all_to_all x4 -> x3, starting transfers between devices: 21.5 us -> 15.6 us  [exchange(): return lax.all_to_all(x, axes, 0, 0, tiled=True)]
    ppermute x21, waiting for transfers between devices: 85.1 us -> 79.8 us  [shifted(): return lax.ppermute(x, axis, [(i, (i + step) % 4) for i in range(4)])]
    pallas_call x5 -> x7, Pallas kernels: 16.6 us -> 21.3 us  [run(): return call(*kept)]
    ppermute x21, starting transfers between devices: 32.1 us -> 36.6 us  [shifted(): return lax.ppermute(x, axis, [(i, (i + step) % 4) for i in range(4)])]
    concatenate x2 -> x0, local copies, waits for them, and re-layouts: 4.05 us -> none  [the longest x1 4.05 us: shards(): jnp.concatenate([turned, rows, side, sq, jnp.zeros((16, 4, width), bf16)]...]
  transfers between devices with their start and end apart: 38 -> 37, of which waited for: 18 -> 15; matrix products, arithmetic and copies ran while one was open for 1% -> 0% of each run, Pallas kernels for 3% -> 4%
where the time goes in v1:
time: 192 us
  waiting for transfers between devices  85.4 us (44%)
  starting transfers between devices  54.3 us (28%)
  blocking collectives  21.6 us (11%)
  Pallas kernels  21.3 us (11%)
  local copies, waits for them, and re-layouts  8.66 us (5%)
    ppermute x21, waiting for transfers between devices, shifted(): return lax.ppermute(x, axis, [(i, (i + step) % 4) for i in range(4)])  79.8 us
    ppermute x21, starting transfers between devices, shifted(): return lax.ppermute(x, axis, [(i, (i + step) % 4) for i in range(4)])  36.6 us
    all_to_all x1, blocking collectives, exchange(): return lax.all_to_all(x, axes, 0, 0, tiled=True)  21.6 us
    pallas_call x7, Pallas kernels, run(): return call(*kept)  21.3 us
    all_to_all x3, starting transfers between devices, exchange(): return lax.all_to_all(x, axes, 0, 0, tiled=True)  15.6 us
    unnamed x42, local copies, waits for them, and re-layouts  7.19 us
    ppermute x13, waiting for transfers between devices, other_core(): return lax.ppermute(x, 'dp', [(0, 1), (1, 0)])  5.56 us
  transfers between devices with their start and end apart: 37, of which 15 were waited for; matrix products, arithmetic and copies ran while one was open for 0% of the time, Pallas kernels for 4%

profile of v1, /device:TPU:0, one launch (start us, length us, event | category | flops | bytes accessed | tf_op | source)
XLA Modules:
  0.0 191.6 jit_solution(10790998228846662719)
XLA Ops:
  2.2 2.1 %collective-permute-start.3 = (bf16[128,768]{1,0:T(8,128)(2,1)S(1)}, bf16[128,768]{1,0:T(8,128)(2,1)}, u32[]{:S(2)}, u32[]{:S(2)}) collective-permute-start(bf16[128,768]{1,0:T(8,128)(2,1)S(1)} %get-tuple-element.18), channel_id=1, source_target_pairs={{0,32},{32,64},{64,96},{96,0},{1,33},{33,65},{65,97},{97,1},{2,34}... | collective-permute-start | bytes 589832 | tf_op jit(solution)/shard_map/ppermute | solution.py:26
  11.1 3.5 %shard_map.111 = bf16[16,112,256]{2,1,0:T(8,128)(2,1)} custom-call(s32[1]{0:T(128)} %bitcast.core_ref, s32[1]{0:T(128)} %bitcast.3.y_ref, bf16[1,256]{1,0:T(2,128)(2,1)S(1)} %broadcast_in_dim.13.branch, bf16[1,256]{1,0:T(2,128)(2,1)S(1)} %broadcast_in_dim.14.gain, bf16[512,256]{1,0:T(8,128)(2,1)} %tokens.3, bf16[512,256]{1,0:T(8,128)(2,1)} %tokens.3, ...), custom_call_target="tpu_custom_call" | custom-call | tf_op jit(solution)/shard_map/pallas_call | solution.py:287
  14.6 6.2 %all-to-all-start = ((bf16[16,112,256]{2,1,0:T(8,128)(2,1)}), bf16[16,112,256]{2,1,0:T(8,128)(2,1)S(1)}, u32[]{:S(2)}, u32[]{:S(2)}) async-start(bf16[16,112,256]{2,1,0:T(8,128)(2,1)} %shard_map.111), calls=%async_computation | async-start | bytes 1835008 | tf_op jit(solution)/shard_map/all_to_all | solution.py:18
  20.8 3.2 %collective-permute-start.2 = (bf16[512,256]{1,0:T(8,128)(2,1)S(1)}, bf16[512,256]{1,0:T(8,128)(2,1)S(1)}, u32[]{:S(2)}, u32[]{:S(2)}) collective-permute-start(bf16[512,256]{1,0:T(8,128)(2,1)S(1)} %get-tuple-element.17.first_x), channel_id=1, source_target_pairs={{0,96},{32,0},{64,32},{96,64},{1,97},{33,1},{65,33},{97,65},{2,98}... | collective-permute-start | bytes 786440 | tf_op jit(solution)/shard_map/ppermute | solution.py:26
  24.0 12.6 %collective-permute-done.4.refs_4_ = bf16[128,768]{1,0:T(8,128)(2,1)} collective-permute-done((bf16[128,768]{1,0:T(8,128)(2,1)S(1)}, bf16[128,768]{1,0:T(8,128)(2,1)}, u32[]{:S(2)}, u32[]{:S(2)}) %collective-permute-start.4) | collective-permute-done | bytes 196640 | tf_op jit(solution)/shard_map/ppermute | solution.py:26
  38.6 2.3 %collective-permute-start.13 = (bf16[96,2048]{1,0:T(8,128)(2,1)S(1)}, bf16[96,2048]{1,0:T(8,128)(2,1)S(1)}, u32[]{:S(2)}, u32[]{:S(2)}) collective-permute-start(bf16[96,2048]{1,0:T(8,128)(2,1)S(1)} %get-tuple-element.25), channel_id=1, source_target_pairs={{0,16},{8,24},{16,0},{24,8},{1,17},{9,25},{17,1},{25,9},{2,18},{10... | collective-permute-start | bytes 1179656 | tf_op jit(solution)/shard_map/ppermute | solution.py:26
  46.0 2.8 %shard_map.110 = (f32[128,768]{1,0:T(8,128)S(1)}, bf16[128,768]{1,0:T(8,128)(2,1)S(1)}, bf16[128,768]{1,0:T(8,128)(2,1)S(1)}, bf16[128,768]{1,0:T(8,128)(2,1)S(1)}) custom-call(s32[1]{0:T(128)} %bitcast.core_ref, s32[1]{0:T(128)} %bitcast.1.x_ref, s32[1]{0:T(128)} %bitcast.2.z_ref, bf16[512,256]{1,0:T(8,128)(2,1)S(1)} %get-tuple-element.17.first_x, ...), custom_call_target="tpu_custom_call" | custom-call | tf_op jit(solution)/shard_map/pallas_call | solution.py:287
  49.4 9.9 %collective-permute-done.13.refs_1_ = bf16[96,2048]{1,0:T(8,128)(2,1)S(1)} collective-permute-done((bf16[96,2048]{1,0:T(8,128)(2,1)S(1)}, bf16[96,2048]{1,0:T(8,128)(2,1)S(1)}, u32[]{:S(2)}, u32[]{:S(2)}) %collective-permute-start.13) | collective-permute-done | bytes 393248 | tf_op jit(solution)/shard_map/ppermute | solution.py:26
  59.8 2.0 %collective-permute-start.11 = (bf16[128,768]{1,0:T(8,128)(2,1)S(1)}, bf16[128,768]{1,0:T(8,128)(2,1)S(1)}, u32[]{:S(2)}, u32[]{:S(2)}) collective-permute-start(bf16[128,768]{1,0:T(8,128)(2,1)S(1)} %get-tuple-element.24), channel_id=1, source_target_pairs={{0,24},{8,0},{16,8},{24,16},{1,25},{9,1},{17,9},{25,17},{2,26},{10... | collective-permute-start | bytes 589832 | tf_op jit(solution)/shard_map/ppermute | solution.py:26
  63.1 2.2 %collective-permute-start.9 = (bf16[128,768]{1,0:T(8,128)(2,1)S(1)}, bf16[128,768]{1,0:T(8,128)(2,1)S(1)}, u32[]{:S(2)}, u32[]{:S(2)}) collective-permute-start(bf16[128,768]{1,0:T(8,128)(2,1)S(1)} %get-tuple-element.22), channel_id=1, source_target_pairs={{0,8},{8,16},{16,24},{24,0},{1,9},{9,17},{17,25},{25,1},{2,10},{10... | collective-permute-start | bytes 589832 | tf_op jit(solution)/shard_map/ppermute | solution.py:26
  66.8 3.9 %collective-permute-done.9.a = bf16[128,768]{1,0:T(8,128)(2,1)S(1)} collective-permute-done((bf16[128,768]{1,0:T(8,128)(2,1)S(1)}, bf16[128,768]{1,0:T(8,128)(2,1)S(1)}, u32[]{:S(2)}, u32[]{:S(2)}) %collective-permute-start.9) | collective-permute-done | bytes 196640 | tf_op jit(solution)/shard_map/ppermute | solution.py:26
  73.2 3.7 %shard_map.112 = bf16[128,4096]{1,0:T(8,128)(2,1)} custom-call(s32[1]{0:T(128)} %bitcast.core_ref, s32[1]{0:T(128)} %bitcast.1.x_ref, f32[128,768]{1,0:T(8,128)S(1)} %get-tuple-element.21.own, bf16[128,768]{1,0:T(8,128)(2,1)S(1)} %collective-permute-done.9.a, bf16[128,768]{1,0:T(8,128)(2,1)S(1)} %collective-permute-done.10.b, ...), custom_call_target="tpu_custom_call" | custom-call | tf_op jit(solution)/shard_map/pallas_call | solution.py:287
  76.9 4.7 %all-to-all-start.1 = ((bf16[16,8,4096]{2,1,0:T(8,128)(2,1)}), bf16[16,8,4096]{2,1,0:T(8,128)(2,1)S(1)}, u32[]{:S(2)}, u32[]{:S(2)}) async-start(bf16[16,8,4096]{2,1,0:T(8,128)(2,1)} %bitcast.4), calls=%async_computation.1 | async-start | bytes 2097152 | tf_op jit(solution)/shard_map/all_to_all | solution.py:18
  83.5 2.7 %collective-permute-start.26 = (bf16[96,2048]{1,0:T(8,128)(2,1)S(1)}, bf16[96,2048]{1,0:T(8,128)(2,1)}, u32[]{:S(2)}, u32[]{:S(2)}) collective-permute-start(bf16[96,2048]{1,0:T(8,128)(2,1)S(1)} %get-tuple-element.26), channel_id=1, source_target_pairs={{0,4},{2,6},{4,0},{6,2},{1,5},{3,7},{5,1},{7,3},{8,12},{10,14},{12... | collective-permute-start | bytes 1179656 | tf_op jit(solution)/shard_map/ppermute | solution.py:26
  86.4 2.9 %collective-permute-start.21 = (bf16[16,96,256]{2,1,0:T(8,128)(2,1)S(1)}, bf16[16,96,256]{2,1,0:T(8,128)(2,1)}, u32[]{:S(2)}, u32[]{:S(2)}) collective-permute-start(bf16[16,96,256]{2,1,0:T(8,128)(2,1)S(1)} %slice.4.refs_0_), channel_id=1, source_target_pairs={{0,4},{2,6},{4,0},{6,2},{1,5},{3,7},{5,1},{7,3},{8,12},{10,14},{12... | collective-permute-start | bytes 2359304 | tf_op jit(solution)/shard_map/ppermute | solution.py:26
  89.8 16.8 %collective-permute-done.25.refs_8_ = bf16[96,2048]{1,0:T(8,128)(2,1)} collective-permute-done((bf16[96,2048]{1,0:T(8,128)(2,1)S(1)}, bf16[96,2048]{1,0:T(8,128)(2,1)}, u32[]{:S(2)}, u32[]{:S(2)}) %collective-permute-start.25) | collective-permute-done | bytes 393248 | tf_op jit(solution)/shard_map/ppermute | solution.py:26
  107.1 7.9 %collective-permute-done.26.refs_9_ = bf16[96,2048]{1,0:T(8,128)(2,1)} collective-permute-done((bf16[96,2048]{1,0:T(8,128)(2,1)S(1)}, bf16[96,2048]{1,0:T(8,128)(2,1)}, u32[]{:S(2)}, u32[]{:S(2)}) %collective-permute-start.26) | collective-permute-done | bytes 393248 | tf_op jit(solution)/shard_map/ppermute | solution.py:26
  115.0 2.1 %shard_map.113 = bf16[16,8,4352]{2,1,0:T(8,128)(2,1)} custom-call(bf16[16,8,4096]{2,1,0:T(8,128)(2,1)S(1)} %all-to-all-done.1.got, bf16[16,112,256]{2,1,0:T(8,128)(2,1)} %copy-done.1), custom_call_target="tpu_custom_call" | custom-call | tf_op jit(solution)/shard_map/pallas_call | solution.py:287
  117.2 4.6 %all-to-all-start.2 = ((bf16[16,8,4352]{2,1,0:T(8,128)(2,1)}), bf16[16,8,4352]{2,1,0:T(8,128)(2,1)S(1)}, u32[]{:S(2)}, u32[]{:S(2)}) async-start(bf16[16,8,4352]{2,1,0:T(8,128)(2,1)} %shard_map.113), calls=%async_computation.2 | async-start | bytes 2228224 | tf_op jit(solution)/shard_map/all_to_all | solution.py:18
  121.8 23.0 %collective-permute-done.27.refs_10_ = bf16[96,2048]{1,0:T(8,128)(2,1)} collective-permute-done((bf16[96,2048]{1,0:T(8,128)(2,1)S(1)}, bf16[96,2048]{1,0:T(8,128)(2,1)}, u32[]{:S(2)}, u32[]{:S(2)}) %collective-permute-start.27) | collective-permute-done | bytes 393248 | tf_op jit(solution)/shard_map/ppermute | solution.py:26
  147.6 4.1 %collective-permute-done.30.refs_13_ = bf16[96,2048]{1,0:T(8,128)(2,1)S(1)} collective-permute-done((bf16[96,2048]{1,0:T(8,128)(2,1)}, bf16[96,2048]{1,0:T(8,128)(2,1)S(1)}, u32[]{:S(2)}, u32[]{:S(2)}) %collective-permute-start.30) | collective-permute-done | bytes 393248 | tf_op jit(solution)/shard_map/ppermute | solution.py:22
  154.0 6.8 %shard_map.114 = bf16[16,128,256]{2,1,0:T(8,128)(2,1)S(1)} custom-call(s32[1]{0:T(128)} %bitcast.core_ref, bf16[16,8,4352]{2,1,0:T(8,128)(2,1)S(1)} %all-to-all-done.2.got.send, bf16[96,4096]{1,0:T(8,128)(2,1)} %w_down.1, bf16[16,96,256]{2,1,0:T(8,128)(2,1)} %copy-done.3, bf16[16,96,256]{2,1,0:T(8,128)(2,1)} %copy-done.5, bf16[16,96,256]{2,1,0:T(8,128)(2,1)} %copy-done.4, ...), custom_call_target="tpu_custom_call" | custom-call | tf_op jit(solution)/shard_map/pallas_call | solution.py:287
  160.8 21.6 %all_to_all.20.got = bf16[16,128,256]{2,1,0:T(8,128)(2,1)S(1)} all-to-all(bf16[16,128,256]{2,1,0:T(8,128)(2,1)S(1)} %shard_map.114), channel_id=1, replica_groups=mesh['rz'=4,'rx'=4,'cb'=4,'dp'=2] {'rz','rx'}, dimensions={0} | all-to-all | bytes 2097152 | tf_op jit(solution)/shard_map/all_to_all | solution.py:18
  186.5 2.2 %collective-permute-start.33 = (bf16[128,256]{1,0:T(8,128)(2,1)S(1)}, bf16[128,256]{1,0:T(8,128)(2,1)S(1)}, u32[]{:S(2)}, u32[]{:S(2)}) collective-permute-start(bf16[128,256]{1,0:T(8,128)(2,1)S(1)} %shard_map.115), channel_id=1, source_target_pairs={{0,6},{2,0},{4,2},{6,4},{1,7},{3,1},{5,3},{7,5},{8,14},{10,8},{12,... | collective-permute-start | bytes 196616 | tf_op jit(solution)/shard_map/ppermute | solution.py:26
  (108 shorter events, 37.5 us)
Async XLA Ops:
  2.2 18.6 %collective-permute-start.3 = (bf16[128,768]{1,0:T(8,128)(2,1)S(1)}, bf16[128,768]{1,0:T(8,128)(2,1)}, u32[]{:S(2)}, u32[]{:S(2)}) collective-permute-start(bf16[128,768]{1,0:T(8,128)(2,1)S(1)} %get-tuple-element.18), channel_id=1, source_target_pairs={{0,32},{32,64},{64,96},{96,0},{1,33},{33,65},{65,97},{97,1},{2,34}... | collective-permute-start | bytes 589832 | tf_op jit(solution)/shard_map/ppermute | solution.py:26
  4.3 34.3 %collective-permute-start = (bf16[512,256]{1,0:T(8,128)(2,1)S(1)}, bf16[512,256]{1,0:T(8,128)(2,1)}, u32[]{:S(2)}, u32[]{:S(2)}) collective-permute-start(bf16[512,256]{1,0:T(8,128)(2,1)S(1)} %get-tuple-element.17.first_x), channel_id=1, source_target_pairs={{0,32},{32,64},{64,96},{96,0},{1,33},{33,65},{65,97},{97,1},{2,34}... | collective-permute-start | bytes 786440 | tf_op jit(solution)/shard_map/ppermute | solution.py:26
  6.2 34.7 %collective-permute-start.1 = (bf16[512,256]{1,0:T(8,128)(2,1)S(1)}, bf16[512,256]{1,0:T(8,128)(2,1)}, u32[]{:S(2)}, u32[]{:S(2)}) collective-permute-start(bf16[512,256]{1,0:T(8,128)(2,1)S(1)} %get-tuple-element.17.first_x), channel_id=1, source_target_pairs={{0,64},{32,96},{64,0},{96,32},{1,65},{33,97},{65,1},{97,33},{2,66}... | collective-permute-start | bytes 786440 | tf_op jit(solution)/shard_map/ppermute | solution.py:26
  8.0 28.6 %collective-permute-start.4 = (bf16[128,768]{1,0:T(8,128)(2,1)S(1)}, bf16[128,768]{1,0:T(8,128)(2,1)}, u32[]{:S(2)}, u32[]{:S(2)}) collective-permute-start(bf16[128,768]{1,0:T(8,128)(2,1)S(1)} %get-tuple-element.19), channel_id=1, source_target_pairs={{0,64},{32,96},{64,0},{96,32},{1,65},{33,97},{65,1},{97,33},{2,66}... | collective-permute-start | bytes 589832 | tf_op jit(solution)/shard_map/ppermute | solution.py:26
  9.8 26.9 %collective-permute-start.5 = (bf16[128,768]{1,0:T(8,128)(2,1)S(1)}, bf16[128,768]{1,0:T(8,128)(2,1)}, u32[]{:S(2)}, u32[]{:S(2)}) collective-permute-start(bf16[128,768]{1,0:T(8,128)(2,1)S(1)} %get-tuple-element.20), channel_id=1, source_target_pairs={{0,96},{32,0},{64,32},{96,64},{1,97},{33,1},{65,33},{97,65},{2,98}... | collective-permute-start | bytes 589832 | tf_op jit(solution)/shard_map/ppermute | solution.py:26
  14.6 57.7 %all-to-all-start = ((bf16[16,112,256]{2,1,0:T(8,128)(2,1)}), bf16[16,112,256]{2,1,0:T(8,128)(2,1)S(1)}, u32[]{:S(2)}, u32[]{:S(2)}) async-start(bf16[16,112,256]{2,1,0:T(8,128)(2,1)} %shard_map.111), calls=%async_computation | async-start | bytes 1835008 | tf_op jit(solution)/shard_map/all_to_all | solution.py:18
  20.8 21.5 %collective-permute-start.2 = (bf16[512,256]{1,0:T(8,128)(2,1)S(1)}, bf16[512,256]{1,0:T(8,128)(2,1)S(1)}, u32[]{:S(2)}, u32[]{:S(2)}) collective-permute-start(bf16[512,256]{1,0:T(8,128)(2,1)S(1)} %get-tuple-element.17.first_x), channel_id=1, source_target_pairs={{0,96},{32,0},{64,32},{96,64},{1,97},{33,1},{65,33},{97,65},{2,98}... | collective-permute-start | bytes 786440 | tf_op jit(solution)/shard_map/ppermute | solution.py:26
  36.6 12.8 %collective-permute-start.12 = (bf16[96,2048]{1,0:T(8,128)(2,1)S(1)}, bf16[96,2048]{1,0:T(8,128)(2,1)S(1)}, u32[]{:S(2)}, u32[]{:S(2)}) collective-permute-start(bf16[96,2048]{1,0:T(8,128)(2,1)S(1)} %get-tuple-element.25), channel_id=1, source_target_pairs={{0,8},{8,16},{16,24},{24,0},{1,9},{9,17},{17,25},{25,1},{2,10},{10... | collective-permute-start | bytes 1179656 | tf_op jit(solution)/shard_map/ppermute | solution.py:26
  38.6 20.7 %collective-permute-start.13 = (bf16[96,2048]{1,0:T(8,128)(2,1)S(1)}, bf16[96,2048]{1,0:T(8,128)(2,1)S(1)}, u32[]{:S(2)}, u32[]{:S(2)}) collective-permute-start(bf16[96,2048]{1,0:T(8,128)(2,1)S(1)} %get-tuple-element.25), channel_id=1, source_target_pairs={{0,16},{8,24},{16,0},{24,8},{1,17},{9,25},{17,1},{25,9},{2,18},{10... | collective-permute-start | bytes 1179656 | tf_op jit(solution)/shard_map/ppermute | solution.py:26
  40.9 18.4 %collective-permute-start.14 = (bf16[96,2048]{1,0:T(8,128)(2,1)S(1)}, bf16[96,2048]{1,0:T(8,128)(2,1)}, u32[]{:S(2)}, u32[]{:S(2)}) collective-permute-start(bf16[96,2048]{1,0:T(8,128)(2,1)S(1)} %get-tuple-element.25), channel_id=1, source_target_pairs={{0,24},{8,0},{16,8},{24,16},{1,25},{9,1},{17,9},{25,17},{2,26},{10... | collective-permute-start | bytes 1179656 | tf_op jit(solution)/shard_map/ppermute | solution.py:26
  48.8 14.2 %collective-permute-start.10 = (bf16[128,768]{1,0:T(8,128)(2,1)S(1)}, bf16[128,768]{1,0:T(8,128)(2,1)S(1)}, u32[]{:S(2)}, u32[]{:S(2)}) collective-permute-start(bf16[128,768]{1,0:T(8,128)(2,1)S(1)} %get-tuple-element.23), channel_id=1, source_target_pairs={{0,16},{8,24},{16,0},{24,8},{1,17},{9,25},{17,1},{25,9},{2,18},{10... | collective-permute-start | bytes 589832 | tf_op jit(solution)/shard_map/ppermute | solution.py:26
  49.4 21.3 %collective-permute-start.15 = (bf16[96,2048]{1,0:T(8,128)(2,1)S(1)}, bf16[96,2048]{1,0:T(8,128)(2,1)S(1)}, u32[]{:S(2)}, u32[]{:S(2)}) collective-permute-start(bf16[96,2048]{1,0:T(8,128)(2,1)S(1)} %collective-permute-done.12.refs_0_), channel_id=1, source_target_pairs={{0,1},{1,0},{2,3},{3,2},{4,5},{5,4},{6,7},{7,6},{8,9},{9,8},{10,11... | collective-permute-start | bytes 1179656 | tf_op jit(solution)/shard_map/ppermute | solution.py:22
  59.3 11.4 %collective-permute-start.16 = (bf16[96,2048]{1,0:T(8,128)(2,1)S(1)}, bf16[96,2048]{1,0:T(8,128)(2,1)S(1)}, u32[]{:S(2)}, u32[]{:S(2)}) collective-permute-start(bf16[96,2048]{1,0:T(8,128)(2,1)S(1)} %collective-permute-done.13.refs_1_), channel_id=1, source_target_pairs={{0,1},{1,0},{2,3},{3,2},{4,5},{5,4},{6,7},{7,6},{8,9},{9,8},{10,11... | collective-permute-start | bytes 1179656 | tf_op jit(solution)/shard_map/ppermute | solution.py:22
  59.3 12.9 %collective-permute-start.17 = (bf16[96,2048]{1,0:T(8,128)(2,1)}, bf16[96,2048]{1,0:T(8,128)(2,1)}, u32[]{:S(2)}, u32[]{:S(2)}) collective-permute-start(bf16[96,2048]{1,0:T(8,128)(2,1)} %collective-permute-done.14.refs_2_), channel_id=1, source_target_pairs={{0,1},{1,0},{2,3},{3,2},{4,5},{5,4},{6,7},{7,6},{8,9},{9,8},{10,11... | collective-permute-start | bytes 1179656 | tf_op jit(solution)/shard_map/ppermute | solution.py:22
  63.1 7.7 %collective-permute-start.9 = (bf16[128,768]{1,0:T(8,128)(2,1)S(1)}, bf16[128,768]{1,0:T(8,128)(2,1)S(1)}, u32[]{:S(2)}, u32[]{:S(2)}) collective-permute-start(bf16[128,768]{1,0:T(8,128)(2,1)S(1)} %get-tuple-element.22), channel_id=1, source_target_pairs={{0,8},{8,16},{16,24},{24,0},{1,9},{9,17},{17,25},{25,1},{2,10},{10... | collective-permute-start | bytes 589832 | tf_op jit(solution)/shard_map/ppermute | solution.py:26
  76.9 38.1 %all-to-all-start.1 = ((bf16[16,8,4096]{2,1,0:T(8,128)(2,1)}), bf16[16,8,4096]{2,1,0:T(8,128)(2,1)S(1)}, u32[]{:S(2)}, u32[]{:S(2)}) async-start(bf16[16,8,4096]{2,1,0:T(8,128)(2,1)} %bitcast.4), calls=%async_computation.1 | async-start | bytes 2097152 | tf_op jit(solution)/shard_map/all_to_all | solution.py:18
  81.6 25.0 %collective-permute-start.25 = (bf16[96,2048]{1,0:T(8,128)(2,1)S(1)}, bf16[96,2048]{1,0:T(8,128)(2,1)}, u32[]{:S(2)}, u32[]{:S(2)}) collective-permute-start(bf16[96,2048]{1,0:T(8,128)(2,1)S(1)} %get-tuple-element.26), channel_id=1, source_target_pairs={{0,2},{2,4},{4,6},{6,0},{1,3},{3,5},{5,7},{7,1},{8,10},{10,12},{12... | collective-permute-start | bytes 1179656 | tf_op jit(solution)/shard_map/ppermute | solution.py:26
  83.5 31.5 %collective-permute-start.26 = (bf16[96,2048]{1,0:T(8,128)(2,1)S(1)}, bf16[96,2048]{1,0:T(8,128)(2,1)}, u32[]{:S(2)}, u32[]{:S(2)}) collective-permute-start(bf16[96,2048]{1,0:T(8,128)(2,1)S(1)} %get-tuple-element.26), channel_id=1, source_target_pairs={{0,4},{2,6},{4,0},{6,2},{1,5},{3,7},{5,1},{7,3},{8,12},{10,14},{12... | collective-permute-start | bytes 1179656 | tf_op jit(solution)/shard_map/ppermute | solution.py:26
  86.3 59.0 %collective-permute-start.19 = (bf16[16,96,256]{2,1,0:T(8,128)(2,1)S(1)}, bf16[16,96,256]{2,1,0:T(8,128)(2,1)S(1)}, u32[]{:S(2)}, u32[]{:S(2)}) collective-permute-start(bf16[16,96,256]{2,1,0:T(8,128)(2,1)S(1)} %slice.4.refs_0_), channel_id=1, source_target_pairs={{0,2},{2,4},{4,6},{6,0},{1,3},{3,5},{5,7},{7,1},{8,10},{10,12},{12... | collective-permute-start | bytes 2359304 | tf_op jit(solution)/shard_map/ppermute | solution.py:26
  86.4 59.9 %collective-permute-start.21 = (bf16[16,96,256]{2,1,0:T(8,128)(2,1)S(1)}, bf16[16,96,256]{2,1,0:T(8,128)(2,1)}, u32[]{:S(2)}, u32[]{:S(2)}) collective-permute-start(bf16[16,96,256]{2,1,0:T(8,128)(2,1)S(1)} %slice.4.refs_0_), channel_id=1, source_target_pairs={{0,4},{2,6},{4,0},{6,2},{1,5},{3,7},{5,1},{7,3},{8,12},{10,14},{12... | collective-permute-start | bytes 2359304 | tf_op jit(solution)/shard_map/ppermute | solution.py:26
  89.3 57.0 %collective-permute-start.23 = (bf16[16,96,256]{2,1,0:T(8,128)(2,1)S(1)}, bf16[16,96,256]{2,1,0:T(8,128)(2,1)}, u32[]{:S(2)}, u32[]{:S(2)}) collective-permute-start(bf16[16,96,256]{2,1,0:T(8,128)(2,1)S(1)} %slice.4.refs_0_), channel_id=1, source_target_pairs={{0,6},{2,0},{4,2},{6,4},{1,7},{3,1},{5,3},{7,5},{8,14},{10,8},{12,... | collective-permute-start | bytes 2359304 | tf_op jit(solution)/shard_map/ppermute | solution.py:26
  106.6 38.2 %collective-permute-start.27 = (bf16[96,2048]{1,0:T(8,128)(2,1)S(1)}, bf16[96,2048]{1,0:T(8,128)(2,1)}, u32[]{:S(2)}, u32[]{:S(2)}) collective-permute-start(bf16[96,2048]{1,0:T(8,128)(2,1)S(1)} %get-tuple-element.26), channel_id=1, source_target_pairs={{0,6},{2,0},{4,2},{6,4},{1,7},{3,1},{5,3},{7,5},{8,14},{10,8},{12,... | collective-permute-start | bytes 1179656 | tf_op jit(solution)/shard_map/ppermute | solution.py:26
  115.0 29.8 %collective-permute-start.28 = (bf16[96,2048]{1,0:T(8,128)(2,1)}, bf16[96,2048]{1,0:T(8,128)(2,1)}, u32[]{:S(2)}, u32[]{:S(2)}) collective-permute-start(bf16[96,2048]{1,0:T(8,128)(2,1)} %collective-permute-done.25.refs_8_), channel_id=1, source_target_pairs={{0,1},{1,0},{2,3},{3,2},{4,5},{5,4},{6,7},{7,6},{8,9},{9,8},{10,11... | collective-permute-start | bytes 1179656 | tf_op jit(solution)/shard_map/ppermute | solution.py:22
  117.2 36.8 %all-to-all-start.2 = ((bf16[16,8,4352]{2,1,0:T(8,128)(2,1)}), bf16[16,8,4352]{2,1,0:T(8,128)(2,1)S(1)}, u32[]{:S(2)}, u32[]{:S(2)}) async-start(bf16[16,8,4352]{2,1,0:T(8,128)(2,1)} %shard_map.113), calls=%async_computation.2 | async-start | bytes 2228224 | tf_op jit(solution)/shard_map/all_to_all | solution.py:18
  (34 other events, 248.0 us)

commit v2 on v1

--- a/solution.py
+++ b/solution.py
@@ -85,17 +85,14 @@
     pairs = []
     for z in range(4):
         for x in range(4):
-            source = tokens.at[pl.ds(x * 128 + 32 * z + 8 * y, 8), :]
+            source = tokens.at[pl.ds(128 * y + 32 * x + 8 * z, 8), :]
             pairs.append((source, out.at[4 * z + x, pl.ds(each, 8), :]))
     copies = together(pairs, sems)
-    wide = here[...].astype(f32)
-    squares = lax.dot_general(
-        jnp.ones((8, width), f32),
-        wide * wide,
-        (((1,), (1,)), ((), ())),
-        precision=lax.Precision.HIGHEST,
-        preferred_element_type=f32,
-    )
+    wide = jnp.concatenate([here[128 * j + 32 * x : 128 * j + 32 * x + 32, :] for x in range(4) for j in range(4)], 0)
+    wide = wide.astype(f32)
+    wide = wide * wide
+    turned = (wide[:, :128] + wide[:, 128:]).T
+    squares = jnp.broadcast_to(jnp.sum(turned, axis=0, keepdims=True), (8, turned.shape[1]))
     high = squares.astype(bf16).astype(f32)
     mid = (squares - high).astype(bf16).astype(f32)
     low = squares - high - mid
@@ -139,9 +136,11 @@
         one = dot(tokens, whole[step], ((1,), (0,)))
         total = one if total is None else total + one
     acc[...] = total
-    own[...] = acc[pl.ds(x * 128, 128), :]
-    for step, send in enumerate(sends, 1):
-        send[...] = acc[pl.ds(((x + step) % 4) * 128, 128), :].astype(bf16)
+    for j in range(4):
+        at = slice(32 * j, 32 * j + 32)
+        own[at, :] = acc[pl.ds(128 * j + 32 * x, 32), :]
+        for step, send in enumerate(sends, 1):
+            send[at, :] = acc[pl.ds(128 * j + 32 * ((x + step) % 4), 32), :].astype(bf16)
 
 
 def down_part(core_ref, x_ref, own, a, b, c, side, w, *refs):
@@ -189,7 +188,7 @@
 
 def finish(got, branch, send, out, middle, sems):
     count, rows = send.shape[:2]
-    width = out.shape[1]
+    width = out.shape[2]
     pairs = [(send.at[:, :, pl.ds(send.shape[2] - width, width)], middle)]
     copies = together(pairs, sems)
     total = jnp.sum(got[...].astype(f32), axis=0)
@@ -197,56 +196,71 @@
     for j in range(count):
         at = slice(j * rows, (j + 1) * rows)
         mid = middle[j].astype(f32)
-        out[at, :] = (residual_scale * mid + 0.5 * branch[...].astype(f32) * total[at]).astype(bf16)
-
-
-def feed_forward(core_ref, got, w_down, *refs):
-    ups, mine, other, out = refs[:8], refs[8:11], refs[11:14], refs[14]
-    tokens, up, whole, up_sems, down_sems = refs[15:]
+        value = (residual_scale * mid + 0.5 * branch[...].astype(f32) * total[at]).astype(bf16)
+        for y in range(4):
+            out[y, at, :] = value
+
+
+def gated(core, tokens, ups, up, sems):
+    blocks, cols, width = ups[0].shape
+    groups = sems.shape[0]
+    each = blocks // groups
+    pending = []
+    for group in range(groups):
+        at = pl.ds(group * each, each)
+        pairs = []
+        for i, source in enumerate(ups):
+            place = core if i % 2 == 0 else 1 - core
+            to = up.at[at, pl.ds((i // 2) * 2 * cols + place * cols, cols), :]
+            pairs.append((source.at[at], to))
+        pending.append(together(pairs, sems.at[group]))
+
+    def finish():
+        total = None
+        for group in range(groups):
+            wait_for(pending[group])
+            for block in range(group * each, (group + 1) * each):
+                part = dot(up[block], tokens[:, block * width : (block + 1) * width], ((1,), (1,)))
+                total = part if total is None else total + part
+        hidden = []
+        for i in range(len(ups) // 2):
+            gate = total[2 * i * cols : (2 * i + 1) * cols]
+            hidden.append(silu(gate) * total[(2 * i + 1) * cols : (2 * i + 2) * cols])
+        return jnp.concatenate(hidden, 0)
+
+    return finish
+
+
+def ff_near(core_ref, got, *refs):
+    ups, out, tokens, up, sems = refs[:6], refs[6], refs[7], refs[8], refs[9]
+    finish = gated(core_ref[0], tokens, ups, up, sems)
+    for j in range(got.shape[0]):
+        tokens[8 * j : 8 * j + 8, :] = got[j, :, : tokens.shape[1]]
+    out[...] = finish()
+
+
+def ff_far(core_ref, got, near, w_down, *refs):
+    ups, mine, other, out = refs[:2], refs[2:5], refs[5:8], refs[8]
+    tokens, up, whole, up_sems, down_sems = refs[9:]
     core = core_ref[0]
-    blocks, cols, width = ups[0].shape
     rows, full = w_down.shape
     half = full // 2
-    groups = up_sems.shape[0]
-    each = blocks // groups
-    up_copies = []
-    for group in range(groups):
-        at = pl.ds(group * each, each)
-        copies = []
-        for step in range(4):
-            for side, place in enumerate((core, 1 - core)):
-                to = up.at[at, pl.ds(step * 2 * cols + place * cols, cols), :]
-                source = ups[2 * step + side].at[at]
-                copies.append(pltpu.make_async_copy(source, to, up_sems.at[group, 2 * step + side]))
-        up_copies.append(copies)
-    down_copies = [(w_down, whole.at[pl.ds(0, rows), :])]
-    for step in range(1, 4):
-        at = pl.ds(step * rows, rows)
-        down_copies.append((mine[step - 1], whole.at[at, at_lane(core, half)]))
-        down_copies.append((other[step - 1], whole.at[at, at_lane(1 - core, half)]))
-    down_copies = [pltpu.make_async_copy(*c, down_sems.at[i]) for i, c in enumerate(down_copies)]
-    for copy in [c for copies in up_copies for c in copies] + down_copies:
-        copy.start()
+    finish = gated(core, tokens, ups, up, up_sems)
+    pairs = [(w_down, whole.at[pl.ds(0, rows), :])]
+    for i, piece in enumerate((0, 2, 1), 1):
+        at = pl.ds(i * rows, rows)
+        pairs.append((mine[piece], whole.at[at, at_lane(core, half)]))
+        pairs.append((other[piece], whole.at[at, at_lane(1 - core, half)]))
+    copies = together(pairs, down_sems)
     for j in range(got.shape[0]):
         tokens[8 * j : 8 * j + 8, :] = got[j, :, :full]
-    total = None
-    for group in range(groups):
-        for copy in up_copies[group]:
-            copy.wait()
-        for block in range(group * each, (group + 1) * each):
-            part = dot(up[block], tokens[:, block * width : (block + 1) * width], ((1,), (1,)))
-            total = part if total is None else total + part
-    hidden = []
-    for step in range(4):
-        gate = total[2 * step * cols : (2 * step + 1) * cols]
-        upward = total[(2 * step + 1) * cols : (2 * step + 2) * cols]
-        hidden.append(silu(gate) * upward)
-    hidden = jnp.concatenate(hidden, 0).T.astype(bf16)
-    for copy in down_copies:
-        copy.wait()
-    for block in range(blocks):
-        lanes = slice(block * width, (block + 1) * width)
-        out[block] = dot(hidden, whole[:, lanes], ((1,), (0,))).astype(bf16)
+    hidden = jnp.concatenate([near[...], finish()], 0).T.astype(bf16)
+    wait_for(copies)
+    width = out.shape[2]
+    for z in range(4):
+        for x in range(4):
+            lanes = slice((4 * z + x) * width, (4 * z + x + 1) * width)
+            out[4 * x + z] = dot(hidden, whole[:, lanes], ((1,), (0,))).astype(bf16)
 
 
 def shards(
@@ -314,10 +328,12 @@
 
     d1 = [shifted(d1, "rx", step) for step in (1, 2, 3)]
     d2 = [shifted(d2, "cb", step) for step in (1, 2, 3)]
-    v1 = [v1] + [shifted(v1, "cb", step) for step in (1, 2, 3)]
+    near = [shifted(v1, "cb", step) for step in (1, 3)]
+    v1 = [v1, near[0], shifted(v1, "cb", 2), near[1]]
     d1_other = [other_core(w) for w in d1]
     d2_other = [other_core(w) for w in d2]
-    v1 = [w for mine in v1 for w in (mine, other_core(mine))]
+    near = [w for mine in (v1[0], v1[1], v1[3]) for w in (mine, other_core(mine))]
+    far = [v1[2], other_core(v1[2])]
 
     own, *sends = kernel(
         up_part,
@@ -335,10 +351,10 @@
     partial = kernel(
         down_part,
         [SMEM] * 2 + [VMEM] * 4 + [HBM] * 8,
-        jax.ShapeDtypeStruct((few, full), bf16),
+        pltpu.VMEM((few, full), bf16),
         scratch=[pltpu.VMEM((part, full), bf16), pltpu.VMEM((16, 16, width), bf16), dma((8,))],
     )(core_ref, x_ref, own, *got, side, first_down, *d1, *d1_other)
-    got = exchange(partial.reshape(16, 8, full), ("rz", "cb"))
+    got = exchange(partial.reshape(16, 8, full), ("cb", "rz"))
     send = kernel(
         join,
         [VMEM, HBM],
@@ -346,34 +362,34 @@
         scratch=[pltpu.VMEM((16, 16, width), bf16), dma(())],
     )(got, side)
     rows = exchange(send, ("rx", "rz"))
+    hidden = kernel(
+        ff_near,
+        [SMEM, VMEM] + [HBM] * 6,
+        jax.ShapeDtypeStruct((3 * part // 4, few), f32),
+        scratch=[pltpu.VMEM((few, full), bf16), pltpu.VMEM((16, 6 * part // 4, width), bf16), dma((4, 6))],
+    )(core_ref, rows, *near)
     partial = kernel(
-        feed_forward,
-        [SMEM, VMEM] + [HBM] * 15,
-        jax.ShapeDtypeStruct((16, few, width), bf16),
+        ff_far,
+        [SMEM, VMEM, VMEM] + [HBM] * 9,
+        pltpu.VMEM((16, few, width), bf16),
         scratch=[
             pltpu.VMEM((few, full), bf16),
-            pltpu.VMEM((16, 2 * part, width), bf16),
+            pltpu.VMEM((16, part // 2, width), bf16),
             pltpu.VMEM((part, full), bf16),
-            dma((4, 8)),
+            dma((2, 2)),
             dma((7,)),
         ],
-        mib=24,
-    )(core_ref, rows, second_down, *v1, *d2, *d2_other)
+    )(core_ref, rows, hidden, second_down, *far, *d2, *d2_other)
     partial, branch = lax.optimization_barrier((partial, second_branch[None]))
-    got = exchange(partial, ("rz", "rx"))
+    got = exchange(partial, ("rx", "rz"))
     out = kernel(
         finish,
         [VMEM, VMEM, HBM],
-        jax.ShapeDtypeStruct((few, width), bf16),
+        pltpu.VMEM((4, few, width), bf16),
         scratch=[pltpu.VMEM((16, 8, width), bf16), dma((1,))],
     )(got, branch, rows)
-    parts = [out] + [shifted(out, "cb", step) for step in (1, 2, 3)]
-    blocks = []
-    for at in range(4):
-        back = (y - at) % 4
-        block = jnp.where(back == 0, parts[0], jnp.where(back == 1, parts[1], jnp.where(back == 2, parts[2], parts[3])))
-        blocks.append(block.reshape(16, 8, width))
-    return jnp.stack(blocks, 1).reshape(n_tok, width)
+    out = exchange(out, "cb")
+    return out.reshape(n_tok, width)
 
 
 def solution(mesh):

time: 192 us -> 210 us (1.094)
  blocking collectives: 21.6 us -> 42.8 us
  starting transfers between devices: 54.3 us -> 48.3 us
  waiting for transfers between devices: 85.4 us -> 88.5 us
  local copies, waits for them, and re-layouts: 8.66 us -> 6.51 us
    all_to_all x1 -> x2, blocking collectives: 21.6 us -> 42.8 us  [exchange(): return lax.all_to_all(x, axes, 0, 0, tiled=True)]
    ppermute x21 -> x18, waiting for transfers between devices: 79.8 us -> 87.1 us  [shifted(): return lax.ppermute(x, axis, [(i, (i + step) % 4) for i in range(4)])]
    ppermute x21 -> x18, starting transfers between devices: 36.6 us -> 30.1 us  [shifted(): return lax.ppermute(x, axis, [(i, (i + step) % 4) for i in range(4)])]
    ppermute x13, waiting for transfers between devices: 5.56 us -> 1.44 us  [other_core(): return lax.ppermute(x, 'dp', [(0, 1), (1, 0)])]
    pallas_call x7 -> x8, Pallas kernels: 21.3 us -> 23.4 us  [run(): return call(*kept)]
    unnamed x42 -> x37, local copies, waits for them, and re-layouts: 7.19 us -> 5.77 us
  transfers between devices with their start and end apart: 37 -> 34, of which waited for: 15 -> 10; matrix products, arithmetic and copies ran while one was open for 0% -> 0% of each run, Pallas kernels for 4% -> 6%
where the time goes in v2:
time: 210 us
  waiting for transfers between devices  88.5 us (42%)
  starting transfers between devices  48.3 us (23%)
  blocking collectives  42.8 us (20%)
  Pallas kernels  23.4 us (11%)
  local copies, waits for them, and re-layouts  6.51 us (3%)
    ppermute x18, waiting for transfers between devices, shifted(): return lax.ppermute(x, axis, [(i, (i + step) % 4) for i in range(4)])  87.1 us
    all_to_all x2, blocking collectives, exchange(): return lax.all_to_all(x, axes, 0, 0, tiled=True)  42.8 us
    ppermute x18, starting transfers between devices, shifted(): return lax.ppermute(x, axis, [(i, (i + step) % 4) for i in range(4)])  30.1 us
    pallas_call x8, Pallas kernels, run(): return call(*kept)  23.4 us
    all_to_all x3, starting transfers between devices, exchange(): return lax.all_to_all(x, axes, 0, 0, tiled=True)  15.6 us
    unnamed x37, local copies, waits for them, and re-layouts  5.77 us
  transfers between devices with their start and end apart: 34, of which 10 were waited for; matrix products, arithmetic and copies ran while one was open for 0% of the time, Pallas kernels for 6%

profile of v2, /device:TPU:0, one launch (start us, length us, event | category | flops | bytes accessed | tf_op | source)
XLA Modules:
  0.0 209.8 jit_solution(16798232946281617264)
XLA Ops:
  2.2 2.1 collective-permute-start.3
  11.1 3.5 %shard_map.111 = bf16[16,112,256]{2,1,0:T(8,128)(2,1)} custom-call(s32[1]{0:T(128)} %bitcast.core_ref, s32[1]{0:T(128)} %bitcast.3.y_ref, bf16[1,256]{1,0:T(2,128)(2,1)S(1)} %broadcast_in_dim.13.branch, bf16[1,256]{1,0:T(2,128)(2,1)S(1)} %broadcast_in_dim.14.gain, bf16[512,256]{1,0:T(8,128)(2,1)} %tokens.3, bf16[512,256]{1,0:T(8,128)(2,1)} %tokens.3, ...), custom_call_target="tpu_custom_call" | custom-call | tf_op jit(solution)/shard_map/pallas_call | solution.py:301
  14.6 6.2 %all-to-all-start = ((bf16[16,112,256]{2,1,0:T(8,128)(2,1)}), bf16[16,112,256]{2,1,0:T(8,128)(2,1)S(1)}, u32[]{:S(2)}, u32[]{:S(2)}) async-start(bf16[16,112,256]{2,1,0:T(8,128)(2,1)} %shard_map.111), calls=%async_computation | async-start | bytes 1835008 | tf_op jit(solution)/shard_map/all_to_all | solution.py:18
  20.8 3.2 %collective-permute-start.2 = (bf16[512,256]{1,0:T(8,128)(2,1)S(1)}, bf16[512,256]{1,0:T(8,128)(2,1)S(1)}, u32[]{:S(2)}, u32[]{:S(2)}) collective-permute-start(bf16[512,256]{1,0:T(8,128)(2,1)S(1)} %get-tuple-element.17.first_x), channel_id=1, source_target_pairs={{0,96},{32,0},{64,32},{96,64},{1,97},{33,1},{65,33},{97,65},{2,98}... | collective-permute-start | bytes 786440 | tf_op jit(solution)/shard_map/ppermute | solution.py:26
  24.0 12.6 %collective-permute-done.4.refs_4_ = bf16[128,768]{1,0:T(8,128)(2,1)} collective-permute-done((bf16[128,768]{1,0:T(8,128)(2,1)S(1)}, bf16[128,768]{1,0:T(8,128)(2,1)}, u32[]{:S(2)}, u32[]{:S(2)}) %collective-permute-start.4) | collective-permute-done | bytes 196640 | tf_op jit(solution)/shard_map/ppermute | solution.py:26
  38.5 2.4 %collective-permute-start.13 = (bf16[96,2048]{1,0:T(8,128)(2,1)S(1)}, bf16[96,2048]{1,0:T(8,128)(2,1)S(1)}, u32[]{:S(2)}, u32[]{:S(2)}) collective-permute-start(bf16[96,2048]{1,0:T(8,128)(2,1)S(1)} %get-tuple-element.25), channel_id=1, source_target_pairs={{0,16},{8,24},{16,0},{24,8},{1,17},{9,25},{17,1},{25,9},{2,18},{10... | collective-permute-start | bytes 1179656 | tf_op jit(solution)/shard_map/ppermute | solution.py:26
  46.0 2.8 %shard_map.110 = (f32[128,768]{1,0:T(8,128)S(1)}, bf16[128,768]{1,0:T(8,128)(2,1)S(1)}, bf16[128,768]{1,0:T(8,128)(2,1)S(1)}, bf16[128,768]{1,0:T(8,128)(2,1)S(1)}) custom-call(s32[1]{0:T(128)} %bitcast.core_ref, s32[1]{0:T(128)} %bitcast.1.x_ref, s32[1]{0:T(128)} %bitcast.2.z_ref, bf16[512,256]{1,0:T(8,128)(2,1)S(1)} %get-tuple-element.17.first_x, ...), custom_call_target="tpu_custom_call" | custom-call | tf_op jit(solution)/shard_map/pallas_call | solution.py:301
  49.4 9.9 %collective-permute-done.13.refs_1_ = bf16[96,2048]{1,0:T(8,128)(2,1)S(1)} collective-permute-done((bf16[96,2048]{1,0:T(8,128)(2,1)S(1)}, bf16[96,2048]{1,0:T(8,128)(2,1)S(1)}, u32[]{:S(2)}, u32[]{:S(2)}) %collective-permute-start.13) | collective-permute-done | bytes 393248 | tf_op jit(solution)/shard_map/ppermute | solution.py:26
  59.8 2.0 collective-permute-start.11
  63.1 2.2 %collective-permute-start.9 = (bf16[128,768]{1,0:T(8,128)(2,1)S(1)}, bf16[128,768]{1,0:T(8,128)(2,1)S(1)}, u32[]{:S(2)}, u32[]{:S(2)}) collective-permute-start(bf16[128,768]{1,0:T(8,128)(2,1)S(1)} %get-tuple-element.22), channel_id=1, source_target_pairs={{0,8},{8,16},{16,24},{24,0},{1,9},{9,17},{17,25},{25,1},{2,10},{10... | collective-permute-start | bytes 589832 | tf_op jit(solution)/shard_map/ppermute | solution.py:26
  66.8 3.9 %collective-permute-done.9.a = bf16[128,768]{1,0:T(8,128)(2,1)S(1)} collective-permute-done((bf16[128,768]{1,0:T(8,128)(2,1)S(1)}, bf16[128,768]{1,0:T(8,128)(2,1)S(1)}, u32[]{:S(2)}, u32[]{:S(2)}) %collective-permute-start.9) | collective-permute-done | bytes 196640 | tf_op jit(solution)/shard_map/ppermute | solution.py:26
  73.2 3.7 %shard_map.112 = bf16[128,4096]{1,0:T(8,128)(2,1)} custom-call(s32[1]{0:T(128)} %bitcast.core_ref, s32[1]{0:T(128)} %bitcast.1.x_ref, f32[128,768]{1,0:T(8,128)S(1)} %get-tuple-element.21.own, bf16[128,768]{1,0:T(8,128)(2,1)S(1)} %collective-permute-done.9.a, bf16[128,768]{1,0:T(8,128)(2,1)S(1)} %collective-permute-done.10.b, ...), custom_call_target="tpu_custom_call" | custom-call | tf_op jit(solution)/shard_map/pallas_call | solution.py:301
  76.9 4.7 %all-to-all-start.1 = ((bf16[16,8,4096]{2,1,0:T(8,128)(2,1)}), bf16[16,8,4096]{2,1,0:T(8,128)(2,1)S(1)}, u32[]{:S(2)}, u32[]{:S(2)}) async-start(bf16[16,8,4096]{2,1,0:T(8,128)(2,1)} %bitcast.4), calls=%async_computation.1 | async-start | bytes 2097152 | tf_op jit(solution)/shard_map/all_to_all | solution.py:18
  81.7 2.0 collective-permute-start.19
  85.7 2.7 %collective-permute-start.23 = (bf16[16,96,256]{2,1,0:T(8,128)(2,1)S(1)}, bf16[16,96,256]{2,1,0:T(8,128)(2,1)}, u32[]{:S(2)}, u32[]{:S(2)}) collective-permute-start(bf16[16,96,256]{2,1,0:T(8,128)(2,1)S(1)} %slice.4.refs_0_), channel_id=1, source_target_pairs={{0,4},{2,6},{4,0},{6,2},{1,5},{3,7},{5,1},{7,3},{8,12},{10,14},{12... | collective-permute-start | bytes 2359304 | tf_op jit(solution)/shard_map/ppermute | solution.py:26
  89.3 33.4 %collective-permute-done.25.refs_2_ = bf16[96,2048]{1,0:T(8,128)(2,1)} collective-permute-done((bf16[96,2048]{1,0:T(8,128)(2,1)S(1)}, bf16[96,2048]{1,0:T(8,128)(2,1)}, u32[]{:S(2)}, u32[]{:S(2)}) %collective-permute-start.25) | collective-permute-done | bytes 393248 | tf_op jit(solution)/shard_map/ppermute | solution.py:26
  123.2 2.2 %shard_map.113 = bf16[16,8,4352]{2,1,0:T(8,128)(2,1)} custom-call(bf16[16,8,4096]{2,1,0:T(8,128)(2,1)S(1)} %all-to-all-done.1.got, bf16[16,112,256]{2,1,0:T(8,128)(2,1)} %copy-done.1), custom_call_target="tpu_custom_call" | custom-call | tf_op jit(solution)/shard_map/pallas_call | solution.py:301
  125.4 4.7 %all-to-all-start.2 = ((bf16[16,8,4352]{2,1,0:T(8,128)(2,1)}), bf16[16,8,4352]{2,1,0:T(8,128)(2,1)S(1)}, u32[]{:S(2)}, u32[]{:S(2)}) async-start(bf16[16,8,4352]{2,1,0:T(8,128)(2,1)} %shard_map.113), calls=%async_computation.2 | async-start | bytes 2228224 | tf_op jit(solution)/shard_map/all_to_all | solution.py:18
  130.1 16.2 %collective-permute-done.26.refs_3_ = bf16[96,2048]{1,0:T(8,128)(2,1)} collective-permute-done((bf16[96,2048]{1,0:T(8,128)(2,1)S(1)}, bf16[96,2048]{1,0:T(8,128)(2,1)}, u32[]{:S(2)}, u32[]{:S(2)}) %collective-permute-start.26) | collective-permute-done | bytes 393248 | tf_op jit(solution)/shard_map/ppermute | solution.py:26
  146.8 8.3 %collective-permute-done.27.refs_4_ = bf16[96,2048]{1,0:T(8,128)(2,1)} collective-permute-done((bf16[96,2048]{1,0:T(8,128)(2,1)S(1)}, bf16[96,2048]{1,0:T(8,128)(2,1)}, u32[]{:S(2)}, u32[]{:S(2)}) %collective-permute-start.27) | collective-permute-done | bytes 393248 | tf_op jit(solution)/shard_map/ppermute | solution.py:26
  155.8 4.8 %shard_map.114.near = f32[288,128]{1,0:T(8,128)S(1)} custom-call(s32[1]{0:T(128)} %bitcast.core_ref, bf16[16,8,4352]{2,1,0:T(8,128)(2,1)S(1)} %all-to-all-done.2.got.send, bf16[16,96,256]{2,1,0:T(8,128)(2,1)} %copy-done.3, bf16[16,96,256]{2,1,0:T(8,128)(2,1)} %collective-permute-done.18.refs_1_, bf16[16,96,256]{2,1,0:T(8,128)(2,1)} %copy-done.4, ...), custom_call_target="tpu_custom_call" | custom-call | tf_op jit(solution)/shard_map/pallas_call | solution.py:301
  161.5 4.0 %shard_map.115 = bf16[16,128,256]{2,1,0:T(8,128)(2,1)S(1)} custom-call(s32[1]{0:T(128)} %bitcast.core_ref, bf16[16,8,4352]{2,1,0:T(8,128)(2,1)S(1)} %all-to-all-done.2.got.send, f32[288,128]{1,0:T(8,128)S(1)} %shard_map.114.near, bf16[96,4096]{1,0:T(8,128)(2,1)} %w_down.1, bf16[16,96,256]{2,1,0:T(8,128)(2,1)} %collective-permute-done.23.refs_0_, ...), custom_call_target="tpu_custom_call" | custom-call | tf_op jit(solution)/shard_map/pallas_call | solution.py:301
  165.5 23.3 %all_to_all.25.got = bf16[16,128,256]{2,1,0:T(8,128)(2,1)S(1)} all-to-all(bf16[16,128,256]{2,1,0:T(8,128)(2,1)S(1)} %shard_map.115), channel_id=1, replica_groups=mesh['rz'=4,'rx'=4,'cb'=4,'dp'=2] {'rx','rz'}, dimensions={0} | all-to-all | bytes 2097152 | tf_op jit(solution)/shard_map/all_to_all | solution.py:18
  189.7 19.4 %all_to_all.26 = bf16[4,128,256]{2,1,0:T(8,128)(2,1)S(1)} all-to-all(bf16[4,128,256]{2,1,0:T(8,128)(2,1)S(1)} %shard_map.116), channel_id=1, replica_groups=mesh['rz'=4,'rx'=4,'cb'=4,'dp'=2] {'cb'}, dimensions={0} | all-to-all | bytes 524288 | tf_op jit(solution)/shard_map/all_to_all | solution.py:18
  (96 shorter events, 29.3 us)
Async XLA Ops:
  2.2 18.6 %collective-permute-start.3 = (bf16[128,768]{1,0:T(8,128)(2,1)S(1)}, bf16[128,768]{1,0:T(8,128)(2,1)}, u32[]{:S(2)}, u32[]{:S(2)}) collective-permute-start(bf16[128,768]{1,0:T(8,128)(2,1)S(1)} %get-tuple-element.18), channel_id=1, source_target_pairs={{0,32},{32,64},{64,96},{96,0},{1,33},{33,65},{65,97},{97,1},{2,34}... | collective-permute-start | bytes 589832 | tf_op jit(solution)/shard_map/ppermute | solution.py:26
  4.3 34.2 %collective-permute-start = (bf16[512,256]{1,0:T(8,128)(2,1)S(1)}, bf16[512,256]{1,0:T(8,128)(2,1)}, u32[]{:S(2)}, u32[]{:S(2)}) collective-permute-start(bf16[512,256]{1,0:T(8,128)(2,1)S(1)} %get-tuple-element.17.first_x), channel_id=1, source_target_pairs={{0,32},{32,64},{64,96},{96,0},{1,33},{33,65},{65,97},{97,1},{2,34}... | collective-permute-start | bytes 786440 | tf_op jit(solution)/shard_map/ppermute | solution.py:26
  6.2 34.7 %collective-permute-start.1 = (bf16[512,256]{1,0:T(8,128)(2,1)S(1)}, bf16[512,256]{1,0:T(8,128)(2,1)}, u32[]{:S(2)}, u32[]{:S(2)}) collective-permute-start(bf16[512,256]{1,0:T(8,128)(2,1)S(1)} %get-tuple-element.17.first_x), channel_id=1, source_target_pairs={{0,64},{32,96},{64,0},{96,32},{1,65},{33,97},{65,1},{97,33},{2,66}... | collective-permute-start | bytes 786440 | tf_op jit(solution)/shard_map/ppermute | solution.py:26
  8.0 28.6 %collective-permute-start.4 = (bf16[128,768]{1,0:T(8,128)(2,1)S(1)}, bf16[128,768]{1,0:T(8,128)(2,1)}, u32[]{:S(2)}, u32[]{:S(2)}) collective-permute-start(bf16[128,768]{1,0:T(8,128)(2,1)S(1)} %get-tuple-element.19), channel_id=1, source_target_pairs={{0,64},{32,96},{64,0},{96,32},{1,65},{33,97},{65,1},{97,33},{2,66}... | collective-permute-start | bytes 589832 | tf_op jit(solution)/shard_map/ppermute | solution.py:26
  9.8 26.9 %collective-permute-start.5 = (bf16[128,768]{1,0:T(8,128)(2,1)S(1)}, bf16[128,768]{1,0:T(8,128)(2,1)}, u32[]{:S(2)}, u32[]{:S(2)}) collective-permute-start(bf16[128,768]{1,0:T(8,128)(2,1)S(1)} %get-tuple-element.20), channel_id=1, source_target_pairs={{0,96},{32,0},{64,32},{96,64},{1,97},{33,1},{65,33},{97,65},{2,98}... | collective-permute-start | bytes 589832 | tf_op jit(solution)/shard_map/ppermute | solution.py:26
  14.6 57.6 %all-to-all-start = ((bf16[16,112,256]{2,1,0:T(8,128)(2,1)}), bf16[16,112,256]{2,1,0:T(8,128)(2,1)S(1)}, u32[]{:S(2)}, u32[]{:S(2)}) async-start(bf16[16,112,256]{2,1,0:T(8,128)(2,1)} %shard_map.111), calls=%async_computation | async-start | bytes 1835008 | tf_op jit(solution)/shard_map/all_to_all | solution.py:18
  20.8 21.4 %collective-permute-start.2 = (bf16[512,256]{1,0:T(8,128)(2,1)S(1)}, bf16[512,256]{1,0:T(8,128)(2,1)S(1)}, u32[]{:S(2)}, u32[]{:S(2)}) collective-permute-start(bf16[512,256]{1,0:T(8,128)(2,1)S(1)} %get-tuple-element.17.first_x), channel_id=1, source_target_pairs={{0,96},{32,0},{64,32},{96,64},{1,97},{33,1},{65,33},{97,65},{2,98}... | collective-permute-start | bytes 786440 | tf_op jit(solution)/shard_map/ppermute | solution.py:26
  36.6 12.8 %collective-permute-start.12 = (bf16[96,2048]{1,0:T(8,128)(2,1)S(1)}, bf16[96,2048]{1,0:T(8,128)(2,1)S(1)}, u32[]{:S(2)}, u32[]{:S(2)}) collective-permute-start(bf16[96,2048]{1,0:T(8,128)(2,1)S(1)} %get-tuple-element.25), channel_id=1, source_target_pairs={{0,8},{8,16},{16,24},{24,0},{1,9},{9,17},{17,25},{25,1},{2,10},{10... | collective-permute-start | bytes 1179656 | tf_op jit(solution)/shard_map/ppermute | solution.py:26
  38.5 20.8 %collective-permute-start.13 = (bf16[96,2048]{1,0:T(8,128)(2,1)S(1)}, bf16[96,2048]{1,0:T(8,128)(2,1)S(1)}, u32[]{:S(2)}, u32[]{:S(2)}) collective-permute-start(bf16[96,2048]{1,0:T(8,128)(2,1)S(1)} %get-tuple-element.25), channel_id=1, source_target_pairs={{0,16},{8,24},{16,0},{24,8},{1,17},{9,25},{17,1},{25,9},{2,18},{10... | collective-permute-start | bytes 1179656 | tf_op jit(solution)/shard_map/ppermute | solution.py:26
  40.9 18.4 %collective-permute-start.14 = (bf16[96,2048]{1,0:T(8,128)(2,1)S(1)}, bf16[96,2048]{1,0:T(8,128)(2,1)}, u32[]{:S(2)}, u32[]{:S(2)}) collective-permute-start(bf16[96,2048]{1,0:T(8,128)(2,1)S(1)} %get-tuple-element.25), channel_id=1, source_target_pairs={{0,24},{8,0},{16,8},{24,16},{1,25},{9,1},{17,9},{25,17},{2,26},{10... | collective-permute-start | bytes 1179656 | tf_op jit(solution)/shard_map/ppermute | solution.py:26
  48.8 14.2 %collective-permute-start.10 = (bf16[128,768]{1,0:T(8,128)(2,1)S(1)}, bf16[128,768]{1,0:T(8,128)(2,1)S(1)}, u32[]{:S(2)}, u32[]{:S(2)}) collective-permute-start(bf16[128,768]{1,0:T(8,128)(2,1)S(1)} %get-tuple-element.23), channel_id=1, source_target_pairs={{0,16},{8,24},{16,0},{24,8},{1,17},{9,25},{17,1},{25,9},{2,18},{10... | collective-permute-start | bytes 589832 | tf_op jit(solution)/shard_map/ppermute | solution.py:26
  49.4 21.3 %collective-permute-start.15 = (bf16[96,2048]{1,0:T(8,128)(2,1)S(1)}, bf16[96,2048]{1,0:T(8,128)(2,1)S(1)}, u32[]{:S(2)}, u32[]{:S(2)}) collective-permute-start(bf16[96,2048]{1,0:T(8,128)(2,1)S(1)} %collective-permute-done.12.refs_0_), channel_id=1, source_target_pairs={{0,1},{1,0},{2,3},{3,2},{4,5},{5,4},{6,7},{7,6},{8,9},{9,8},{10,11... | collective-permute-start | bytes 1179656 | tf_op jit(solution)/shard_map/ppermute | solution.py:22
  59.3 11.4 %collective-permute-start.16 = (bf16[96,2048]{1,0:T(8,128)(2,1)S(1)}, bf16[96,2048]{1,0:T(8,128)(2,1)S(1)}, u32[]{:S(2)}, u32[]{:S(2)}) collective-permute-start(bf16[96,2048]{1,0:T(8,128)(2,1)S(1)} %collective-permute-done.13.refs_1_), channel_id=1, source_target_pairs={{0,1},{1,0},{2,3},{3,2},{4,5},{5,4},{6,7},{7,6},{8,9},{9,8},{10,11... | collective-permute-start | bytes 1179656 | tf_op jit(solution)/shard_map/ppermute | solution.py:22
  59.3 12.9 %collective-permute-start.17 = (bf16[96,2048]{1,0:T(8,128)(2,1)}, bf16[96,2048]{1,0:T(8,128)(2,1)}, u32[]{:S(2)}, u32[]{:S(2)}) collective-permute-start(bf16[96,2048]{1,0:T(8,128)(2,1)} %collective-permute-done.14.refs_2_), channel_id=1, source_target_pairs={{0,1},{1,0},{2,3},{3,2},{4,5},{5,4},{6,7},{7,6},{8,9},{9,8},{10,11... | collective-permute-start | bytes 1179656 | tf_op jit(solution)/shard_map/ppermute | solution.py:22
  76.9 46.3 %all-to-all-start.1 = ((bf16[16,8,4096]{2,1,0:T(8,128)(2,1)}), bf16[16,8,4096]{2,1,0:T(8,128)(2,1)S(1)}, u32[]{:S(2)}, u32[]{:S(2)}) async-start(bf16[16,8,4096]{2,1,0:T(8,128)(2,1)} %bitcast.4), calls=%async_computation.1 | async-start | bytes 2097152 | tf_op jit(solution)/shard_map/all_to_all | solution.py:18
  81.7 41.0 %collective-permute-start.19 = (bf16[16,96,256]{2,1,0:T(8,128)(2,1)S(1)}, bf16[16,96,256]{2,1,0:T(8,128)(2,1)S(1)}, u32[]{:S(2)}, u32[]{:S(2)}) collective-permute-start(bf16[16,96,256]{2,1,0:T(8,128)(2,1)S(1)} %slice.4.refs_0_), channel_id=1, source_target_pairs={{0,2},{2,4},{4,6},{6,0},{1,3},{3,5},{5,7},{7,1},{8,10},{10,12},{12... | collective-permute-start | bytes 2359304 | tf_op jit(solution)/shard_map/ppermute | solution.py:26
  83.7 62.6 %collective-permute-start.21 = (bf16[16,96,256]{2,1,0:T(8,128)(2,1)S(1)}, bf16[16,96,256]{2,1,0:T(8,128)(2,1)}, u32[]{:S(2)}, u32[]{:S(2)}) collective-permute-start(bf16[16,96,256]{2,1,0:T(8,128)(2,1)S(1)} %slice.4.refs_0_), channel_id=1, source_target_pairs={{0,6},{2,0},{4,2},{6,4},{1,7},{3,1},{5,3},{7,5},{8,14},{10,8},{12,... | collective-permute-start | bytes 2359304 | tf_op jit(solution)/shard_map/ppermute | solution.py:26
  85.0 37.7 %collective-permute-start.25 = (bf16[96,2048]{1,0:T(8,128)(2,1)S(1)}, bf16[96,2048]{1,0:T(8,128)(2,1)}, u32[]{:S(2)}, u32[]{:S(2)}) collective-permute-start(bf16[96,2048]{1,0:T(8,128)(2,1)S(1)} %get-tuple-element.26), channel_id=1, source_target_pairs={{0,2},{2,4},{4,6},{6,0},{1,3},{3,5},{5,7},{7,1},{8,10},{10,12},{12... | collective-permute-start | bytes 1179656 | tf_op jit(solution)/shard_map/ppermute | solution.py:26
  85.7 60.6 %collective-permute-start.23 = (bf16[16,96,256]{2,1,0:T(8,128)(2,1)S(1)}, bf16[16,96,256]{2,1,0:T(8,128)(2,1)}, u32[]{:S(2)}, u32[]{:S(2)}) collective-permute-start(bf16[16,96,256]{2,1,0:T(8,128)(2,1)S(1)} %slice.4.refs_0_), channel_id=1, source_target_pairs={{0,4},{2,6},{4,0},{6,2},{1,5},{3,7},{5,1},{7,3},{8,12},{10,14},{12... | collective-permute-start | bytes 2359304 | tf_op jit(solution)/shard_map/ppermute | solution.py:26
  88.4 57.9 %collective-permute-start.26 = (bf16[96,2048]{1,0:T(8,128)(2,1)S(1)}, bf16[96,2048]{1,0:T(8,128)(2,1)}, u32[]{:S(2)}, u32[]{:S(2)}) collective-permute-start(bf16[96,2048]{1,0:T(8,128)(2,1)S(1)} %get-tuple-element.26), channel_id=1, source_target_pairs={{0,4},{2,6},{4,0},{6,2},{1,5},{3,7},{5,1},{7,3},{8,12},{10,14},{12... | collective-permute-start | bytes 1179656 | tf_op jit(solution)/shard_map/ppermute | solution.py:26
  122.7 32.5 %collective-permute-start.18 = (bf16[16,96,256]{2,1,0:T(8,128)(2,1)S(1)}, bf16[16,96,256]{2,1,0:T(8,128)(2,1)}, u32[]{:S(2)}, u32[]{:S(2)}) collective-permute-start(bf16[16,96,256]{2,1,0:T(8,128)(2,1)S(1)} %slice.4.refs_0_), channel_id=1, source_target_pairs={{0,1},{1,0},{2,3},{3,2},{4,5},{5,4},{6,7},{7,6},{8,9},{9,8},{10,11... | collective-permute-start | bytes 2359304 | tf_op jit(solution)/shard_map/ppermute | solution.py:22
  122.7 33.0 %collective-permute-start.20 = (bf16[16,96,256]{2,1,0:T(8,128)(2,1)S(1)}, bf16[16,96,256]{2,1,0:T(8,128)(2,1)}, u32[]{:S(2)}, u32[]{:S(2)}) collective-permute-start(bf16[16,96,256]{2,1,0:T(8,128)(2,1)S(1)} %collective-permute-done.19.refs_2_), channel_id=1, source_target_pairs={{0,1},{1,0},{2,3},{3,2},{4,5},{5,4},{6,7},{7,6},{8,9},{9,8},{10,11... | collective-permute-start | bytes 2359304 | tf_op jit(solution)/shard_map/ppermute | solution.py:22
  125.4 30.4 %all-to-all-start.2 = ((bf16[16,8,4352]{2,1,0:T(8,128)(2,1)}), bf16[16,8,4352]{2,1,0:T(8,128)(2,1)S(1)}, u32[]{:S(2)}, u32[]{:S(2)}) async-start(bf16[16,8,4352]{2,1,0:T(8,128)(2,1)} %shard_map.113), calls=%async_computation.2 | async-start | bytes 2228224 | tf_op jit(solution)/shard_map/all_to_all | solution.py:18
  146.3 14.3 %collective-permute-start.24 = (bf16[16,96,256]{2,1,0:T(8,128)(2,1)}, bf16[16,96,256]{2,1,0:T(8,128)(2,1)}, u32[]{:S(2)}, u32[]{:S(2)}) collective-permute-start(bf16[16,96,256]{2,1,0:T(8,128)(2,1)} %collective-permute-done.23.refs_0_), channel_id=1, source_target_pairs={{0,1},{1,0},{2,3},{3,2},{4,5},{5,4},{6,7},{7,6},{8,9},{9,8},{10,11... | collective-permute-start | bytes 2359304 | tf_op jit(solution)/shard_map/ppermute | solution.py:22
  (28 other events, 210.8 us)

commit v3 on v2

--- a/solution.py
+++ b/solution.py
@@ -69,6 +69,10 @@
     wait_for(copies[1:])
 
 
+def token_rows(x):
+    return [128 * j + 32 * x + 8 * z for z in range(4) for j in range(4)]
+
+
 def message(core_ref, y_ref, branch, gain, here, tokens, gate, upward, out, picked, sems):
     core, y = core_ref[0], y_ref[0]
     width, cols = picked.shape
@@ -88,8 +92,8 @@
             source = tokens.at[pl.ds(128 * y + 32 * x + 8 * z, 8), :]
             pairs.append((source, out.at[4 * z + x, pl.ds(each, 8), :]))
     copies = together(pairs, sems)
-    wide = jnp.concatenate([here[128 * j + 32 * x : 128 * j + 32 * x + 32, :] for x in range(4) for j in range(4)], 0)
-    wide = wide.astype(f32)
+    wide = here[...].astype(f32)
+    wide = jnp.concatenate([wide[at : at + 8] for x in range(4) for at in token_rows(x)], 0)
     wide = wide * wide
     turned = (wide[:, :128] + wide[:, 128:]).T
     squares = jnp.broadcast_to(jnp.sum(turned, axis=0, keepdims=True), (8, turned.shape[1]))
@@ -136,11 +140,13 @@
         one = dot(tokens, whole[step], ((1,), (0,)))
         total = one if total is None else total + one
     acc[...] = total
-    for j in range(4):
-        at = slice(32 * j, 32 * j + 32)
-        own[at, :] = acc[pl.ds(128 * j + 32 * x, 32), :]
-        for step, send in enumerate(sends, 1):
-            send[at, :] = acc[pl.ds(128 * j + 32 * ((x + step) % 4), 32), :].astype(bf16)
+
+    def block(to):
+        return jnp.concatenate([acc[pl.ds(at, 8), :] for at in token_rows(to)], 0)
+
+    own[...] = block(x)
+    for step, send in enumerate(sends, 1):
+        send[...] = block((x + step) % 4).astype(bf16)
 
 
 def down_part(core_ref, x_ref, own, a, b, c, side, w, *refs):
@@ -201,18 +207,20 @@
             out[y, at, :] = value
 
 
-def gated(core, tokens, ups, up, sems):
-    blocks, cols, width = ups[0].shape
+def gated(core, tokens, sources, up, sems):
+    blocks, rows, width = up.shape
+    cols = 96
     groups = sems.shape[0]
     each = blocks // groups
     pending = []
     for group in range(groups):
-        at = pl.ds(group * each, each)
         pairs = []
-        for i, source in enumerate(ups):
-            place = core if i % 2 == 0 else 1 - core
-            to = up.at[at, pl.ds((i // 2) * 2 * cols + place * cols, cols), :]
-            pairs.append((source.at[at], to))
+        for w, first, slot, side in sources:
+            begin = group * each - first
+            if 0 <= begin < w.shape[0]:
+                place = 1 - core if side else core
+                to = up.at[pl.ds(group * each, each), pl.ds(slot * 2 * cols + place * cols, cols), :]
+                pairs.append((w.at[pl.ds(begin, each), pl.ds(0, cols), :], to))
         pending.append(together(pairs, sems.at[group]))
 
     def finish():
@@ -223,7 +231,7 @@
                 part = dot(up[block], tokens[:, block * width : (block + 1) * width], ((1,), (1,)))
                 total = part if total is None else total + part
         hidden = []
-        for i in range(len(ups) // 2):
+        for i in range(rows // (2 * cols)):
             gate = total[2 * i * cols : (2 * i + 1) * cols]
             hidden.append(silu(gate) * total[(2 * i + 1) * cols : (2 * i + 2) * cols])
         return jnp.concatenate(hidden, 0)
@@ -232,20 +240,25 @@
 
 
 def ff_near(core_ref, got, *refs):
-    ups, out, tokens, up, sems = refs[:6], refs[6], refs[7], refs[8], refs[9]
-    finish = gated(core_ref[0], tokens, ups, up, sems)
+    ups, out, tokens, up, sems = refs[:10], refs[10], refs[11], refs[12], refs[13]
+    half = up.shape[0] // 2
+    sources = [(ups[0], 0, 0, 0), (ups[1], 0, 0, 1)]
+    for i, w in enumerate(ups[2:]):
+        sources.append((w, half * (i // 2 % 2), 1 + i // 4, i % 2))
+    finish = gated(core_ref[0], tokens, sources, up, sems)
     for j in range(got.shape[0]):
         tokens[8 * j : 8 * j + 8, :] = got[j, :, : tokens.shape[1]]
     out[...] = finish()
 
 
 def ff_far(core_ref, got, near, w_down, *refs):
-    ups, mine, other, out = refs[:2], refs[2:5], refs[5:8], refs[8]
-    tokens, up, whole, up_sems, down_sems = refs[9:]
+    ups, mine, other, out = refs[:4], refs[4:7], refs[7:10], refs[10]
+    tokens, up, whole, up_sems, down_sems = refs[11:]
     core = core_ref[0]
     rows, full = w_down.shape
     half = full // 2
-    finish = gated(core, tokens, ups, up, up_sems)
+    sources = [(w, up.shape[0] // 2 * (i // 2), 0, i % 2) for i, w in enumerate(ups)]
+    finish = gated(core, tokens, sources, up, up_sems)
     pairs = [(w_down, whole.at[pl.ds(0, rows), :])]
     for i, piece in enumerate((0, 2, 1), 1):
         at = pl.ds(i * rows, rows)
@@ -324,16 +337,31 @@
         scratch=[pltpu.VMEM((width, cols), bf16), dma((17,))],
     )(core_ref, y_ref, first_branch[None], second_gain[None], tokens, tokens, second_gate, second_up)
     side = exchange(side, ("rz", "rx"))
-    v1 = side[:, : cols // 16]
-
-    d1 = [shifted(d1, "rx", step) for step in (1, 2, 3)]
-    d2 = [shifted(d2, "cb", step) for step in (1, 2, 3)]
-    near = [shifted(v1, "cb", step) for step in (1, 3)]
-    v1 = [v1, near[0], shifted(v1, "cb", 2), near[1]]
-    d1_other = [other_core(w) for w in d1]
-    d2_other = [other_core(w) for w in d2]
-    near = [w for mine in (v1[0], v1[1], v1[3]) for w in (mine, other_core(mine))]
-    far = [v1[2], other_core(v1[2])]
+
+    def ring(w, axis):
+        back, ahead = shifted(w, axis, 1), shifted(w, axis, 3)
+        return [back, shifted(back, axis, 1), ahead]
+
+    def swapped(ws):
+        return [other_core(w) for w in ws]
+
+    d1 = ring(d1, "rx")
+    d2 = ring(d2, "cb")
+    (one, three), (two,) = swapped([d1[0], d1[2]]), swapped([d1[1]])
+    d1_other = [one, two, three]
+    d2_other = swapped(d2)
+    low, high = side[:8, : cols // 16], side[8:, : cols // 16]
+    low = [shifted(low, "cb", step) for step in (1, 3)]
+    high = [shifted(high, "cb", step) for step in (1, 3)]
+    far = [shifted(low[0], "cb", 1)]
+    far += [shifted(high[1], "cb", 3)]
+    low_other = swapped([side, *low])
+    high_other = swapped(high)
+    near = [side, low_other[0]]
+    for i in range(2):
+        near += [low[i], low_other[1 + i], high[i], high_other[i]]
+    far_other = swapped(far)
+    far = [far[0], far_other[0], far[1], far_other[1]]
 
     own, *sends = kernel(
         up_part,
@@ -354,7 +382,7 @@
         pltpu.VMEM((few, full), bf16),
         scratch=[pltpu.VMEM((part, full), bf16), pltpu.VMEM((16, 16, width), bf16), dma((8,))],
     )(core_ref, x_ref, own, *got, side, first_down, *d1, *d1_other)
-    got = exchange(partial.reshape(16, 8, full), ("cb", "rz"))
+    got = exchange(partial.reshape(16, 8, full), ("rz", "cb"))
     send = kernel(
         join,
         [VMEM, HBM],
@@ -364,13 +392,13 @@
     rows = exchange(send, ("rx", "rz"))
     hidden = kernel(
         ff_near,
-        [SMEM, VMEM] + [HBM] * 6,
+        [SMEM, VMEM] + [HBM] * 10,
         jax.ShapeDtypeStruct((3 * part // 4, few), f32),
         scratch=[pltpu.VMEM((few, full), bf16), pltpu.VMEM((16, 6 * part // 4, width), bf16), dma((4, 6))],
     )(core_ref, rows, *near)
     partial = kernel(
         ff_far,
-        [SMEM, VMEM, VMEM] + [HBM] * 9,
+        [SMEM, VMEM, VMEM] + [HBM] * 11,
         pltpu.VMEM((16, few, width), bf16),
         scratch=[
             pltpu.VMEM((few, full), bf16),

time: 210 us -> 175 us (0.83)
  waiting for transfers between devices: 88.5 us -> 59.3 us
  blocking collectives: 42.8 us -> 30.5 us
  starting transfers between devices: 48.3 us -> 55.7 us
    ppermute x18 -> x21, waiting for transfers between devices: 87.1 us -> 52.3 us  [shifted(): return lax.ppermute(x, axis, [(i, (i + step) % 4) for i in range(4)])]
    all_to_all x2, blocking collectives: 42.8 us -> 30.5 us  [exchange(): return lax.all_to_all(x, axes, 0, 0, tiled=True)]
    ppermute x18 -> x21, starting transfers between devices: 30.1 us -> 37.9 us  [shifted(): return lax.ppermute(x, axis, [(i, (i + step) % 4) for i in range(4)])]
    all_to_all x3, waiting for transfers between devices: 0.01 us -> 5.18 us  [exchange(): return lax.all_to_all(x, axes, 0, 0, tiled=True)]
    unnamed x37 -> x39, local copies, waits for them, and re-layouts: 5.77 us -> 3.84 us
  transfers between devices with their start and end apart: 34 -> 40, of which waited for: 10 -> 12; matrix products, arithmetic and copies ran while one was open for 0% -> 1% of each run, Pallas kernels for 6% -> 10%
where the time goes in v3:
time: 175 us
  waiting for transfers between devices  59.3 us (34%)
  starting transfers between devices  55.7 us (32%)
  blocking collectives  30.5 us (17%)
  Pallas kernels  23.4 us (13%)
  local copies, waits for them, and re-layouts  5.51 us (3%)
    ppermute x21, waiting for transfers between devices, shifted(): return lax.ppermute(x, axis, [(i, (i + step) % 4) for i in range(4)])  52.3 us
    ppermute x21, starting transfers between devices, shifted(): return lax.ppermute(x, axis, [(i, (i + step) % 4) for i in range(4)])  37.9 us
    all_to_all x2, blocking collectives, exchange(): return lax.all_to_all(x, axes, 0, 0, tiled=True)  30.5 us
    pallas_call x8, Pallas kernels, run(): return call(*kept)  23.4 us
    all_to_all x3, starting transfers between devices, exchange(): return lax.all_to_all(x, axes, 0, 0, tiled=True)  15.5 us
    all_to_all x3, waiting for transfers between devices, exchange(): return lax.all_to_all(x, axes, 0, 0, tiled=True)  5.18 us
    unnamed x39, local copies, waits for them, and re-layouts  3.84 us
  transfers between devices with their start and end apart: 40, of which 12 were waited for; matrix products, arithmetic and copies ran while one was open for 1% of the time, Pallas kernels for 10%

profile of v3, /device:TPU:0, one launch (start us, length us, event | category | flops | bytes accessed | tf_op | source)
XLA Modules:
  0.0 174.6 jit_solution(3894265632924184888)
XLA Ops:
  5.8 3.6 %collective-permute-start.4 = (bf16[128,768]{1,0:T(8,128)(2,1)S(1)}, bf16[128,768]{1,0:T(8,128)(2,1)S(1)}, u32[]{:S(2)}, u32[]{:S(2)}) collective-permute-start(bf16[128,768]{1,0:T(8,128)(2,1)S(1)} %get-tuple-element.19), channel_id=1, source_target_pairs={{0,64},{32,96},{64,0},{96,32},{1,65},{33,97},{65,1},{97,33},{2,66}... | collective-permute-start | bytes 589832 | tf_op jit(solution)/shard_map/ppermute | solution.py:26
  10.4 3.5 %shard_map.111 = bf16[16,112,256]{2,1,0:T(8,128)(2,1)} custom-call(s32[1]{0:T(128)} %bitcast.core_ref, s32[1]{0:T(128)} %bitcast.3.y_ref, bf16[1,256]{1,0:T(2,128)(2,1)S(1)} %broadcast_in_dim.13.branch, bf16[1,256]{1,0:T(2,128)(2,1)S(1)} %broadcast_in_dim.14.gain, bf16[512,256]{1,0:T(8,128)(2,1)} %tokens.3, bf16[512,256]{1,0:T(8,128)(2,1)} %tokens.3, ...), custom_call_target="tpu_custom_call" | custom-call | tf_op jit(solution)/shard_map/pallas_call | solution.py:314
  13.9 4.6 %all-to-all-start = ((bf16[16,112,256]{2,1,0:T(8,128)(2,1)}), bf16[16,112,256]{2,1,0:T(8,128)(2,1)S(1)}, u32[]{:S(2)}, u32[]{:S(2)}) async-start(bf16[16,112,256]{2,1,0:T(8,128)(2,1)} %shard_map.111), calls=%async_computation | async-start | bytes 1835008 | tf_op jit(solution)/shard_map/all_to_all | solution.py:18
  20.4 2.7 %collective-permute-start.1 = (bf16[512,256]{1,0:T(8,128)(2,1)S(1)}, bf16[512,256]{1,0:T(8,128)(2,1)S(1)}, u32[]{:S(2)}, u32[]{:S(2)}) collective-permute-start(bf16[512,256]{1,0:T(8,128)(2,1)S(1)} %get-tuple-element.17.first_x), channel_id=1, source_target_pairs={{0,64},{32,96},{64,0},{96,32},{1,65},{33,97},{65,1},{97,33},{2,66}... | collective-permute-start | bytes 786440 | tf_op jit(solution)/shard_map/ppermute | solution.py:26
  24.6 2.7 %collective-permute-start.14 = (bf16[96,2048]{1,0:T(8,128)(2,1)S(1)}, bf16[96,2048]{1,0:T(8,128)(2,1)S(1)}, u32[]{:S(2)}, u32[]{:S(2)}) collective-permute-start(bf16[96,2048]{1,0:T(8,128)(2,1)S(1)} %get-tuple-element.25), channel_id=1, source_target_pairs={{0,24},{8,0},{16,8},{24,16},{1,25},{9,1},{17,9},{25,17},{2,26},{10... | collective-permute-start | bytes 1179656 | tf_op jit(solution)/shard_map/ppermute | solution.py:26
  27.2 10.9 %collective-permute-done.refs_0_ = bf16[512,256]{1,0:T(8,128)(2,1)S(1)} collective-permute-done((bf16[512,256]{1,0:T(8,128)(2,1)S(1)}, bf16[512,256]{1,0:T(8,128)(2,1)S(1)}, u32[]{:S(2)}, u32[]{:S(2)}) %collective-permute-start) | collective-permute-done | bytes 262176 | tf_op jit(solution)/shard_map/ppermute | solution.py:26
  38.2 4.0 %collective-permute-done.1.refs_1_ = bf16[512,256]{1,0:T(8,128)(2,1)S(1)} collective-permute-done((bf16[512,256]{1,0:T(8,128)(2,1)S(1)}, bf16[512,256]{1,0:T(8,128)(2,1)S(1)}, u32[]{:S(2)}, u32[]{:S(2)}) %collective-permute-start.1) | collective-permute-done | bytes 262176 | tf_op jit(solution)/shard_map/ppermute | solution.py:26
  45.4 2.8 %shard_map.110 = (f32[128,768]{1,0:T(8,128)S(1)}, bf16[128,768]{1,0:T(8,128)(2,1)S(1)}, bf16[128,768]{1,0:T(8,128)(2,1)S(1)}, bf16[128,768]{1,0:T(8,128)(2,1)S(1)}) custom-call(s32[1]{0:T(128)} %bitcast.core_ref, s32[1]{0:T(128)} %bitcast.1.x_ref, s32[1]{0:T(128)} %bitcast.2.z_ref, bf16[512,256]{1,0:T(8,128)(2,1)S(1)} %get-tuple-element.17.first_x, ...), custom_call_target="tpu_custom_call" | custom-call | tf_op jit(solution)/shard_map/pallas_call | solution.py:314
  48.2 3.0 %collective-permute-start.10 = (bf16[128,768]{1,0:T(8,128)(2,1)S(1)}, bf16[128,768]{1,0:T(8,128)(2,1)S(1)}, u32[]{:S(2)}, u32[]{:S(2)}) collective-permute-start(bf16[128,768]{1,0:T(8,128)(2,1)S(1)} %get-tuple-element.23), channel_id=1, source_target_pairs={{0,16},{8,24},{16,0},{24,8},{1,17},{9,25},{17,1},{25,9},{2,18},{10... | collective-permute-start | bytes 589832 | tf_op jit(solution)/shard_map/ppermute | solution.py:26
  53.1 3.7 %collective-permute-done.10.b = bf16[128,768]{1,0:T(8,128)(2,1)S(1)} collective-permute-done((bf16[128,768]{1,0:T(8,128)(2,1)S(1)}, bf16[128,768]{1,0:T(8,128)(2,1)S(1)}, u32[]{:S(2)}, u32[]{:S(2)}) %collective-permute-start.10) | collective-permute-done | bytes 196640 | tf_op jit(solution)/shard_map/ppermute | solution.py:26
  65.8 3.7 %shard_map.112 = bf16[128,4096]{1,0:T(8,128)(2,1)} custom-call(s32[1]{0:T(128)} %bitcast.core_ref, s32[1]{0:T(128)} %bitcast.1.x_ref, f32[128,768]{1,0:T(8,128)S(1)} %get-tuple-element.21.own, bf16[128,768]{1,0:T(8,128)(2,1)S(1)} %collective-permute-done.9.a, bf16[128,768]{1,0:T(8,128)(2,1)S(1)} %collective-permute-done.10.b, ...), custom_call_target="tpu_custom_call" | custom-call | tf_op jit(solution)/shard_map/pallas_call | solution.py:314
  69.5 5.6 %all-to-all-start.1 = ((bf16[16,8,4096]{2,1,0:T(8,128)(2,1)}), bf16[16,8,4096]{2,1,0:T(8,128)(2,1)S(1)}, u32[]{:S(2)}, u32[]{:S(2)}) async-start(bf16[16,8,4096]{2,1,0:T(8,128)(2,1)} %bitcast.4), calls=%async_computation.1 | async-start | bytes 2097152 | tf_op jit(solution)/shard_map/all_to_all | solution.py:18
  75.1 3.1 %collective-permute-start.33 = (bf16[96,2048]{1,0:T(8,128)(2,1)S(1)}, bf16[96,2048]{1,0:T(8,128)(2,1)}, u32[]{:S(2)}, u32[]{:S(2)}) collective-permute-start(bf16[96,2048]{1,0:T(8,128)(2,1)S(1)} %get-tuple-element.26), channel_id=1, source_target_pairs={{0,6},{2,0},{4,2},{6,4},{1,7},{3,1},{5,3},{7,5},{8,14},{10,8},{12,... | collective-permute-start | bytes 1179656 | tf_op jit(solution)/shard_map/ppermute | solution.py:26
  80.0 2.4 %collective-permute-start.25 = (bf16[8,96,256]{2,1,0:T(8,128)(2,1)}, bf16[8,96,256]{2,1,0:T(8,128)(2,1)}, u32[]{:S(2)}, u32[]{:S(2)}) collective-permute-start(bf16[8,96,256]{2,1,0:T(8,128)(2,1)} %get-tuple-element.29), channel_id=1, source_target_pairs={{0,6},{2,0},{4,2},{6,4},{1,7},{3,1},{5,3},{7,5},{8,14},{10,8},{12,... | collective-permute-start | bytes 1179656 | tf_op jit(solution)/shard_map/ppermute | solution.py:26
  82.4 16.0 %collective-permute-done.33.refs_6_ = bf16[96,2048]{1,0:T(8,128)(2,1)} collective-permute-done((bf16[96,2048]{1,0:T(8,128)(2,1)S(1)}, bf16[96,2048]{1,0:T(8,128)(2,1)}, u32[]{:S(2)}, u32[]{:S(2)}) %collective-permute-start.33) | collective-permute-done | bytes 393248 | tf_op jit(solution)/shard_map/ppermute | solution.py:26
  98.5 3.2 %collective-permute-start.23 = (bf16[8,96,256]{2,1,0:T(8,128)(2,1)}, bf16[8,96,256]{2,1,0:T(8,128)(2,1)}, u32[]{:S(2)}, u32[]{:S(2)}) collective-permute-start(bf16[8,96,256]{2,1,0:T(8,128)(2,1)} %get-tuple-element.30), channel_id=1, source_target_pairs={{0,6},{2,0},{4,2},{6,4},{1,7},{3,1},{5,3},{7,5},{8,14},{10,8},{12,... | collective-permute-start | bytes 1179656 | tf_op jit(solution)/shard_map/ppermute | solution.py:26
  101.7 4.3 %collective-permute-done.19.refs_2_ = bf16[8,96,256]{2,1,0:T(8,128)(2,1)} collective-permute-done((bf16[8,96,256]{2,1,0:T(8,128)(2,1)}, bf16[8,96,256]{2,1,0:T(8,128)(2,1)}, u32[]{:S(2)}, u32[]{:S(2)}) %collective-permute-start.19) | collective-permute-done | bytes 393248 | tf_op jit(solution)/shard_map/ppermute | solution.py:26
  109.1 5.4 %all-to-all-start.2 = ((bf16[16,8,4352]{2,1,0:T(8,128)(2,1)}), bf16[16,8,4352]{2,1,0:T(8,128)(2,1)S(1)}, u32[]{:S(2)}, u32[]{:S(2)}) async-start(bf16[16,8,4352]{2,1,0:T(8,128)(2,1)} %shard_map.113), calls=%async_computation.2 | async-start | bytes 2228224 | tf_op jit(solution)/shard_map/all_to_all | solution.py:18
  118.8 9.0 %collective-permute-done.27.refs_0_ = bf16[8,96,256]{2,1,0:T(8,128)(2,1)} collective-permute-done((bf16[8,96,256]{2,1,0:T(8,128)(2,1)}, bf16[8,96,256]{2,1,0:T(8,128)(2,1)}, u32[]{:S(2)}, u32[]{:S(2)}) %collective-permute-start.27) | collective-permute-done | bytes 393248 | tf_op jit(solution)/shard_map/ppermute | solution.py:26
  128.5 5.2 %all-to-all-done.2.got.send = bf16[16,8,4352]{2,1,0:T(8,128)(2,1)S(1)} async-done(((bf16[16,8,4352]{2,1,0:T(8,128)(2,1)}), bf16[16,8,4352]{2,1,0:T(8,128)(2,1)S(1)}, u32[]{:S(2)}, u32[]{:S(2)}) %all-to-all-start.2) | async-done | bytes 1114144 | tf_op jit(solution)/shard_map/all_to_all | solution.py:18
  133.7 4.8 %shard_map.114.near = f32[288,128]{1,0:T(8,128)S(1)} custom-call(s32[1]{0:T(128)} %bitcast.core_ref, bf16[16,8,4352]{2,1,0:T(8,128)(2,1)S(1)} %all-to-all-done.2.got.send, bf16[16,112,256]{2,1,0:T(8,128)(2,1)} %copy-done.1, bf16[16,112,256]{2,1,0:T(8,128)(2,1)} %copy-done.3, bf16[8,96,256]{2,1,0:T(8,128)(2,1)} %collective-permute-done.19.refs_2_, ...), custom_call_target="tpu_custom_call" | custom-call | tf_op jit(solution)/shard_map/pallas_call | solution.py:314
  138.5 4.0 %shard_map.115 = bf16[16,128,256]{2,1,0:T(8,128)(2,1)S(1)} custom-call(s32[1]{0:T(128)} %bitcast.core_ref, bf16[16,8,4352]{2,1,0:T(8,128)(2,1)S(1)} %all-to-all-done.2.got.send, f32[288,128]{1,0:T(8,128)S(1)} %shard_map.114.near, bf16[96,4096]{1,0:T(8,128)(2,1)} %w_down.1, bf16[8,96,256]{2,1,0:T(8,128)(2,1)} %collective-permute-done.27.refs_0_, ...), custom_call_target="tpu_custom_call" | custom-call | tf_op jit(solution)/shard_map/pallas_call | solution.py:314
  142.6 19.8 %all_to_all.25.got = bf16[16,128,256]{2,1,0:T(8,128)(2,1)S(1)} all-to-all(bf16[16,128,256]{2,1,0:T(8,128)(2,1)S(1)} %shard_map.115), channel_id=1, replica_groups=mesh['rz'=4,'rx'=4,'cb'=4,'dp'=2] {'rx','rz'}, dimensions={0} | all-to-all | bytes 2097152 | tf_op jit(solution)/shard_map/all_to_all | solution.py:18
  163.3 10.7 %all_to_all.26 = bf16[4,128,256]{2,1,0:T(8,128)(2,1)S(1)} all-to-all(bf16[4,128,256]{2,1,0:T(8,128)(2,1)S(1)} %shard_map.116), channel_id=1, replica_groups=mesh['rz'=4,'rx'=4,'cb'=4,'dp'=2] {'cb'}, dimensions={0} | all-to-all | bytes 524288 | tf_op jit(solution)/shard_map/all_to_all | solution.py:18
  (110 shorter events, 35.6 us)
Async XLA Ops:
  2.2 25.0 %collective-permute-start.12 = (bf16[96,2048]{1,0:T(8,128)(2,1)S(1)}, bf16[96,2048]{1,0:T(8,128)(2,1)S(1)}, u32[]{:S(2)}, u32[]{:S(2)}) collective-permute-start(bf16[96,2048]{1,0:T(8,128)(2,1)S(1)} %get-tuple-element.25), channel_id=1, source_target_pairs={{0,8},{8,16},{16,24},{24,0},{1,9},{9,17},{17,25},{25,1},{2,10},{10... | collective-permute-start | bytes 1179656 | tf_op jit(solution)/shard_map/ppermute | solution.py:26
  3.9 16.5 %collective-permute-start.3 = (bf16[128,768]{1,0:T(8,128)(2,1)S(1)}, bf16[128,768]{1,0:T(8,128)(2,1)S(1)}, u32[]{:S(2)}, u32[]{:S(2)}) collective-permute-start(bf16[128,768]{1,0:T(8,128)(2,1)S(1)} %get-tuple-element.18), channel_id=1, source_target_pairs={{0,32},{32,64},{64,96},{96,0},{1,33},{33,65},{65,97},{97,1},{2,34}... | collective-permute-start | bytes 589832 | tf_op jit(solution)/shard_map/ppermute | solution.py:26
  5.8 17.3 %collective-permute-start.4 = (bf16[128,768]{1,0:T(8,128)(2,1)S(1)}, bf16[128,768]{1,0:T(8,128)(2,1)S(1)}, u32[]{:S(2)}, u32[]{:S(2)}) collective-permute-start(bf16[128,768]{1,0:T(8,128)(2,1)S(1)} %get-tuple-element.19), channel_id=1, source_target_pairs={{0,64},{32,96},{64,0},{96,32},{1,65},{33,97},{65,1},{97,33},{2,66}... | collective-permute-start | bytes 589832 | tf_op jit(solution)/shard_map/ppermute | solution.py:26
  9.4 15.2 %collective-permute-start.5 = (bf16[128,768]{1,0:T(8,128)(2,1)S(1)}, bf16[128,768]{1,0:T(8,128)(2,1)}, u32[]{:S(2)}, u32[]{:S(2)}) collective-permute-start(bf16[128,768]{1,0:T(8,128)(2,1)S(1)} %get-tuple-element.20), channel_id=1, source_target_pairs={{0,96},{32,0},{64,32},{96,64},{1,97},{33,1},{65,33},{97,65},{2,98}... | collective-permute-start | bytes 589832 | tf_op jit(solution)/shard_map/ppermute | solution.py:26
  13.9 50.9 %all-to-all-start = ((bf16[16,112,256]{2,1,0:T(8,128)(2,1)}), bf16[16,112,256]{2,1,0:T(8,128)(2,1)S(1)}, u32[]{:S(2)}, u32[]{:S(2)}) async-start(bf16[16,112,256]{2,1,0:T(8,128)(2,1)} %shard_map.111), calls=%async_computation | async-start | bytes 1835008 | tf_op jit(solution)/shard_map/all_to_all | solution.py:18
  18.5 19.7 %collective-permute-start = (bf16[512,256]{1,0:T(8,128)(2,1)S(1)}, bf16[512,256]{1,0:T(8,128)(2,1)S(1)}, u32[]{:S(2)}, u32[]{:S(2)}) collective-permute-start(bf16[512,256]{1,0:T(8,128)(2,1)S(1)} %get-tuple-element.17.first_x), channel_id=1, source_target_pairs={{0,32},{32,64},{64,96},{96,0},{1,33},{33,65},{65,97},{97,1},{2,34}... | collective-permute-start | bytes 786440 | tf_op jit(solution)/shard_map/ppermute | solution.py:26
  20.4 21.8 %collective-permute-start.1 = (bf16[512,256]{1,0:T(8,128)(2,1)S(1)}, bf16[512,256]{1,0:T(8,128)(2,1)S(1)}, u32[]{:S(2)}, u32[]{:S(2)}) collective-permute-start(bf16[512,256]{1,0:T(8,128)(2,1)S(1)} %get-tuple-element.17.first_x), channel_id=1, source_target_pairs={{0,64},{32,96},{64,0},{96,32},{1,65},{33,97},{65,1},{97,33},{2,66}... | collective-permute-start | bytes 786440 | tf_op jit(solution)/shard_map/ppermute | solution.py:26
  23.1 19.1 %collective-permute-start.2 = (bf16[512,256]{1,0:T(8,128)(2,1)S(1)}, bf16[512,256]{1,0:T(8,128)(2,1)S(1)}, u32[]{:S(2)}, u32[]{:S(2)}) collective-permute-start(bf16[512,256]{1,0:T(8,128)(2,1)S(1)} %get-tuple-element.17.first_x), channel_id=1, source_target_pairs={{0,96},{32,0},{64,32},{96,64},{1,97},{33,1},{65,33},{97,65},{2,98}... | collective-permute-start | bytes 786440 | tf_op jit(solution)/shard_map/ppermute | solution.py:26
  24.6 26.7 %collective-permute-start.14 = (bf16[96,2048]{1,0:T(8,128)(2,1)S(1)}, bf16[96,2048]{1,0:T(8,128)(2,1)S(1)}, u32[]{:S(2)}, u32[]{:S(2)}) collective-permute-start(bf16[96,2048]{1,0:T(8,128)(2,1)S(1)} %get-tuple-element.25), channel_id=1, source_target_pairs={{0,24},{8,0},{16,8},{24,16},{1,25},{9,1},{17,9},{25,17},{2,26},{10... | collective-permute-start | bytes 1179656 | tf_op jit(solution)/shard_map/ppermute | solution.py:26
  27.2 24.5 %collective-permute-start.13 = (bf16[96,2048]{1,0:T(8,128)(2,1)S(1)}, bf16[96,2048]{1,0:T(8,128)(2,1)S(1)}, u32[]{:S(2)}, u32[]{:S(2)}) collective-permute-start(bf16[96,2048]{1,0:T(8,128)(2,1)S(1)} %collective-permute-done.12.refs_0_), channel_id=1, source_target_pairs={{0,8},{8,16},{16,24},{24,0},{1,9},{9,17},{17,25},{25,1},{2,10},{10... | collective-permute-start | bytes 1179656 | tf_op jit(solution)/shard_map/ppermute | solution.py:26
  51.3 13.5 %collective-permute-start.17 = (bf16[96,2048]{1,0:T(8,128)(2,1)S(1)}, bf16[96,2048]{1,0:T(8,128)(2,1)}, u32[]{:S(2)}, u32[]{:S(2)}) collective-permute-start(bf16[96,2048]{1,0:T(8,128)(2,1)S(1)} %collective-permute-done.14.refs_2_), channel_id=1, source_target_pairs={{0,1},{1,0},{2,3},{3,2},{4,5},{5,4},{6,7},{7,6},{8,9},{9,8},{10,11... | collective-permute-start | bytes 1179656 | tf_op jit(solution)/shard_map/ppermute | solution.py:22
  51.8 13.1 %collective-permute-start.16 = (bf16[96,2048]{1,0:T(8,128)(2,1)S(1)}, bf16[96,2048]{1,0:T(8,128)(2,1)}, u32[]{:S(2)}, u32[]{:S(2)}) collective-permute-start(bf16[96,2048]{1,0:T(8,128)(2,1)S(1)} %collective-permute-done.13.refs_1_), channel_id=1, source_target_pairs={{0,1},{1,0},{2,3},{3,2},{4,5},{5,4},{6,7},{7,6},{8,9},{9,8},{10,11... | collective-permute-start | bytes 1179656 | tf_op jit(solution)/shard_map/ppermute | solution.py:22
  61.0 17.2 %collective-permute-start.31 = (bf16[96,2048]{1,0:T(8,128)(2,1)S(1)}, bf16[96,2048]{1,0:T(8,128)(2,1)}, u32[]{:S(2)}, u32[]{:S(2)}) collective-permute-start(bf16[96,2048]{1,0:T(8,128)(2,1)S(1)} %get-tuple-element.26), channel_id=1, source_target_pairs={{0,2},{2,4},{4,6},{6,0},{1,3},{3,5},{5,7},{7,1},{8,10},{10,12},{12... | collective-permute-start | bytes 1179656 | tf_op jit(solution)/shard_map/ppermute | solution.py:26
  69.5 37.4 %all-to-all-start.1 = ((bf16[16,8,4096]{2,1,0:T(8,128)(2,1)}), bf16[16,8,4096]{2,1,0:T(8,128)(2,1)S(1)}, u32[]{:S(2)}, u32[]{:S(2)}) async-start(bf16[16,8,4096]{2,1,0:T(8,128)(2,1)} %bitcast.4), calls=%async_computation.1 | async-start | bytes 2097152 | tf_op jit(solution)/shard_map/all_to_all | solution.py:18
  75.1 23.4 %collective-permute-start.33 = (bf16[96,2048]{1,0:T(8,128)(2,1)S(1)}, bf16[96,2048]{1,0:T(8,128)(2,1)}, u32[]{:S(2)}, u32[]{:S(2)}) collective-permute-start(bf16[96,2048]{1,0:T(8,128)(2,1)S(1)} %get-tuple-element.26), channel_id=1, source_target_pairs={{0,6},{2,0},{4,2},{6,4},{1,7},{3,1},{5,3},{7,5},{8,14},{10,8},{12,... | collective-permute-start | bytes 1179656 | tf_op jit(solution)/shard_map/ppermute | solution.py:26
  78.2 20.3 %collective-permute-start.32 = (bf16[96,2048]{1,0:T(8,128)(2,1)}, bf16[96,2048]{1,0:T(8,128)(2,1)}, u32[]{:S(2)}, u32[]{:S(2)}) collective-permute-start(bf16[96,2048]{1,0:T(8,128)(2,1)} %collective-permute-done.31.refs_4_), channel_id=1, source_target_pairs={{0,2},{2,4},{4,6},{6,0},{1,3},{3,5},{5,7},{7,1},{8,10},{10,12},{12... | collective-permute-start | bytes 1179656 | tf_op jit(solution)/shard_map/ppermute | solution.py:26
  79.2 26.8 %collective-permute-start.19 = (bf16[8,96,256]{2,1,0:T(8,128)(2,1)}, bf16[8,96,256]{2,1,0:T(8,128)(2,1)}, u32[]{:S(2)}, u32[]{:S(2)}) collective-permute-start(bf16[8,96,256]{2,1,0:T(8,128)(2,1)} %get-tuple-element.30), channel_id=1, source_target_pairs={{0,2},{2,4},{4,6},{6,0},{1,3},{3,5},{5,7},{7,1},{8,10},{10,12},{12... | collective-permute-start | bytes 1179656 | tf_op jit(solution)/shard_map/ppermute | solution.py:26
  80.0 26.9 %collective-permute-start.25 = (bf16[8,96,256]{2,1,0:T(8,128)(2,1)}, bf16[8,96,256]{2,1,0:T(8,128)(2,1)}, u32[]{:S(2)}, u32[]{:S(2)}) collective-permute-start(bf16[8,96,256]{2,1,0:T(8,128)(2,1)} %get-tuple-element.29), channel_id=1, source_target_pairs={{0,6},{2,0},{4,2},{6,4},{1,7},{3,1},{5,3},{7,5},{8,14},{10,8},{12,... | collective-permute-start | bytes 1179656 | tf_op jit(solution)/shard_map/ppermute | solution.py:26
  82.4 45.9 %collective-permute-start.18 = (bf16[16,112,256]{2,1,0:T(8,128)(2,1)S(1)}, bf16[16,112,256]{2,1,0:T(8,128)(2,1)S(1)}, u32[]{:S(2)}, u32[]{:S(2)}) collective-permute-start(bf16[16,112,256]{2,1,0:T(8,128)(2,1)S(1)} %copy-done.2), channel_id=1, source_target_pairs={{0,1},{1,0},{2,3},{3,2},{4,5},{5,4},{6,7},{7,6},{8,9},{9,8},{10,11... | collective-permute-start | bytes 2752520 | tf_op jit(solution)/shard_map/ppermute | solution.py:22
  98.5 16.0 %collective-permute-start.21 = (bf16[8,96,256]{2,1,0:T(8,128)(2,1)}, bf16[8,96,256]{2,1,0:T(8,128)(2,1)S(1)}, u32[]{:S(2)}, u32[]{:S(2)}) collective-permute-start(bf16[8,96,256]{2,1,0:T(8,128)(2,1)} %get-tuple-element.29), channel_id=1, source_target_pairs={{0,2},{2,4},{4,6},{6,0},{1,3},{3,5},{5,7},{7,1},{8,10},{10,12},{12... | collective-permute-start | bytes 1179656 | tf_op jit(solution)/shard_map/ppermute | solution.py:26
  98.5 16.3 %collective-permute-start.23 = (bf16[8,96,256]{2,1,0:T(8,128)(2,1)}, bf16[8,96,256]{2,1,0:T(8,128)(2,1)}, u32[]{:S(2)}, u32[]{:S(2)}) collective-permute-start(bf16[8,96,256]{2,1,0:T(8,128)(2,1)} %get-tuple-element.30), channel_id=1, source_target_pairs={{0,6},{2,0},{4,2},{6,4},{1,7},{3,1},{5,3},{7,5},{8,14},{10,8},{12,... | collective-permute-start | bytes 1179656 | tf_op jit(solution)/shard_map/ppermute | solution.py:26
  109.1 24.6 %all-to-all-start.2 = ((bf16[16,8,4352]{2,1,0:T(8,128)(2,1)}), bf16[16,8,4352]{2,1,0:T(8,128)(2,1)S(1)}, u32[]{:S(2)}, u32[]{:S(2)}) async-start(bf16[16,8,4352]{2,1,0:T(8,128)(2,1)} %shard_map.113), calls=%async_computation.2 | async-start | bytes 2228224 | tf_op jit(solution)/shard_map/all_to_all | solution.py:18
  118.3 20.2 %collective-permute-start.34 = (bf16[96,2048]{1,0:T(8,128)(2,1)}, bf16[96,2048]{1,0:T(8,128)(2,1)}, u32[]{:S(2)}, u32[]{:S(2)}) collective-permute-start(bf16[96,2048]{1,0:T(8,128)(2,1)} %collective-permute-done.31.refs_4_), channel_id=1, source_target_pairs={{0,1},{1,0},{2,3},{3,2},{4,5},{5,4},{6,7},{7,6},{8,9},{9,8},{10,11... | collective-permute-start | bytes 1179656 | tf_op jit(solution)/shard_map/ppermute | solution.py:22
  118.4 20.1 %collective-permute-start.36 = (bf16[96,2048]{1,0:T(8,128)(2,1)}, bf16[96,2048]{1,0:T(8,128)(2,1)}, u32[]{:S(2)}, u32[]{:S(2)}) collective-permute-start(bf16[96,2048]{1,0:T(8,128)(2,1)} %collective-permute-done.33.refs_6_), channel_id=1, source_target_pairs={{0,1},{1,0},{2,3},{3,2},{4,5},{5,4},{6,7},{7,6},{8,9},{9,8},{10,11... | collective-permute-start | bytes 1179656 | tf_op jit(solution)/shard_map/ppermute | solution.py:22
  (35 other events, 324.8 us)

commit v4 on v3

--- a/solution.py
+++ b/solution.py
@@ -209,18 +209,17 @@
 
 def gated(core, tokens, sources, up, sems):
     blocks, rows, width = up.shape
-    cols = 96
+    cols = rows // (2 * (len(sources) // 2))
     groups = sems.shape[0]
     each = blocks // groups
     pending = []
     for group in range(groups):
         pairs = []
-        for w, first, slot, side in sources:
-            begin = group * each - first
-            if 0 <= begin < w.shape[0]:
-                place = 1 - core if side else core
-                to = up.at[pl.ds(group * each, each), pl.ds(slot * 2 * cols + place * cols, cols), :]
-                pairs.append((w.at[pl.ds(begin, each), pl.ds(0, cols), :], to))
+        at = pl.ds(group * each, each)
+        for w, slot, side in sources:
+            place = 1 - core if side else core
+            to = up.at[at, pl.ds(slot * 2 * cols + place * cols, cols), :]
+            pairs.append((w.at[at, pl.ds(0, cols), :], to))
         pending.append(together(pairs, sems.at[group]))
 
     def finish():
@@ -240,11 +239,8 @@
 
 
 def ff_near(core_ref, got, *refs):
-    ups, out, tokens, up, sems = refs[:10], refs[10], refs[11], refs[12], refs[13]
-    half = up.shape[0] // 2
-    sources = [(ups[0], 0, 0, 0), (ups[1], 0, 0, 1)]
-    for i, w in enumerate(ups[2:]):
-        sources.append((w, half * (i // 2 % 2), 1 + i // 4, i % 2))
+    ups, out, tokens, up, sems = refs[:6], refs[6], refs[7], refs[8], refs[9]
+    sources = [(w, i // 2, i % 2) for i, w in enumerate(ups)]
     finish = gated(core_ref[0], tokens, sources, up, sems)
     for j in range(got.shape[0]):
         tokens[8 * j : 8 * j + 8, :] = got[j, :, : tokens.shape[1]]
@@ -252,12 +248,12 @@
 
 
 def ff_far(core_ref, got, near, w_down, *refs):
-    ups, mine, other, out = refs[:4], refs[4:7], refs[7:10], refs[10]
-    tokens, up, whole, up_sems, down_sems = refs[11:]
+    ups, mine, other, out = refs[:2], refs[2:5], refs[5:8], refs[8]
+    tokens, up, whole, up_sems, down_sems = refs[9:]
     core = core_ref[0]
     rows, full = w_down.shape
     half = full // 2
-    sources = [(w, up.shape[0] // 2 * (i // 2), 0, i % 2) for i, w in enumerate(ups)]
+    sources = [(ups[0], 0, 0), (ups[1], 0, 1)]
     finish = gated(core, tokens, sources, up, up_sems)
     pairs = [(w_down, whole.at[pl.ds(0, rows), :])]
     for i, piece in enumerate((0, 2, 1), 1):
@@ -338,30 +334,22 @@
     )(core_ref, y_ref, first_branch[None], second_gain[None], tokens, tokens, second_gate, second_up)
     side = exchange(side, ("rz", "rx"))
 
-    def ring(w, axis):
-        back, ahead = shifted(w, axis, 1), shifted(w, axis, 3)
-        return [back, shifted(back, axis, 1), ahead]
-
     def swapped(ws):
         return [other_core(w) for w in ws]
 
-    d1 = ring(d1, "rx")
-    d2 = ring(d2, "cb")
-    (one, three), (two,) = swapped([d1[0], d1[2]]), swapped([d1[1]])
-    d1_other = [one, two, three]
-    d2_other = swapped(d2)
-    low, high = side[:8, : cols // 16], side[8:, : cols // 16]
-    low = [shifted(low, "cb", step) for step in (1, 3)]
-    high = [shifted(high, "cb", step) for step in (1, 3)]
-    far = [shifted(low[0], "cb", 1)]
-    far += [shifted(high[1], "cb", 3)]
-    low_other = swapped([side, *low])
-    high_other = swapped(high)
-    near = [side, low_other[0]]
-    for i in range(2):
-        near += [low[i], low_other[1 + i], high[i], high_other[i]]
-    far_other = swapped(far)
-    far = [far[0], far_other[0], far[1], far_other[1]]
+    d1 = [shifted(d1, "rx", step) for step in (1, 2, 3)]
+    d1_other = swapped(d1)
+    back, ahead = shifted(d2, "cb", 1), shifted(d2, "cb", 3)
+    d2 = [back, shifted(back, "cb", 1), ahead]
+    one, three = swapped([back, ahead])
+    d2_other = [one, *swapped([d2[1]]), three]
+    v1 = side[:, : cols // 16]
+    back, ahead = shifted(v1, "cb", 1), shifted(v1, "cb", 3)
+    far = [shifted(v1, "cb", 2)]
+    near = [side, *swapped([side])]
+    one, three = swapped([back, ahead])
+    near += [back, one, ahead, three]
+    far += swapped(far)
 
     own, *sends = kernel(
         up_part,
@@ -386,19 +374,19 @@
     send = kernel(
         join,
         [VMEM, HBM],
-        jax.ShapeDtypeStruct((16, 8, full + width), bf16),
+        pltpu.VMEM((16, 8, full + width), bf16),
         scratch=[pltpu.VMEM((16, 16, width), bf16), dma(())],
     )(got, side)
     rows = exchange(send, ("rx", "rz"))
     hidden = kernel(
         ff_near,
-        [SMEM, VMEM] + [HBM] * 10,
+        [SMEM, VMEM] + [HBM] * 6,
         jax.ShapeDtypeStruct((3 * part // 4, few), f32),
         scratch=[pltpu.VMEM((few, full), bf16), pltpu.VMEM((16, 6 * part // 4, width), bf16), dma((4, 6))],
     )(core_ref, rows, *near)
     partial = kernel(
         ff_far,
-        [SMEM, VMEM, VMEM] + [HBM] * 11,
+        [SMEM, VMEM, VMEM] + [HBM] * 9,
         pltpu.VMEM((16, few, width), bf16),
         scratch=[
             pltpu.VMEM((few, full), bf16),

time: 175 us -> 206 us (1.18)
  waiting for transfers between devices: 59.3 us -> 82.2 us
  blocking collectives: 30.5 us -> 36 us
    ppermute x21 -> x18, waiting for transfers between devices: 52.3 us -> 80.6 us  [shifted(): return lax.ppermute(x, axis, [(i, (i + step) % 4) for i in range(4)])]
    all_to_all x2, blocking collectives: 30.5 us -> 36 us  [exchange(): return lax.all_to_all(x, axes, 0, 0, tiled=True)]
    all_to_all x3, waiting for transfers between devices: 5.18 us -> 0.01 us  [exchange(): return lax.all_to_all(x, axes, 0, 0, tiled=True)]
    unnamed x39 -> x35, local copies, waits for them, and re-layouts: 3.84 us -> 5.05 us
    ppermute x21 -> x18, starting transfers between devices: 37.9 us -> 38.6 us  [shifted(): return lax.ppermute(x, axis, [(i, (i + step) % 4) for i in range(4)])]
  transfers between devices with their start and end apart: 40 -> 34, of which waited for: 12 -> 11; matrix products, arithmetic and copies ran while one was open for 1% -> 0% of each run, Pallas kernels for 10% -> 6%
where the time goes in v4:
time: 206 us; the launch traced here: 205 us
  waiting for transfers between devices  82.2 us (40%)
  starting transfers between devices  56.4 us (27%)
  blocking collectives  36 us (17%)
  Pallas kernels  23.4 us (11%)
  local copies, waits for them, and re-layouts  6.7 us (3%)
    ppermute x18, waiting for transfers between devices, shifted(): return lax.ppermute(x, axis, [(i, (i + step) % 4) for i in range(4)])  80.6 us
    ppermute x18, starting transfers between devices, shifted(): return lax.ppermute(x, axis, [(i, (i + step) % 4) for i in range(4)])  38.6 us
    all_to_all x2, blocking collectives, exchange(): return lax.all_to_all(x, axes, 0, 0, tiled=True)  36 us
    pallas_call x8, Pallas kernels, run(): return call(*kept)  23.4 us
    all_to_all x3, starting transfers between devices, exchange(): return lax.all_to_all(x, axes, 0, 0, tiled=True)  15.7 us
    unnamed x35, local copies, waits for them, and re-layouts  5.05 us
  transfers between devices with their start and end apart: 34, of which 11 were waited for; matrix products, arithmetic and copies ran while one was open for 0% of the time, Pallas kernels for 6%

profile of v4, /device:TPU:0, one launch (start us, length us, event | category | flops | bytes accessed | tf_op | source)
XLA Modules:
  0.0 204.9 jit_solution(12506723408548361126)
XLA Ops:
  2.2 2.1 %collective-permute-start.3 = (bf16[128,768]{1,0:T(8,128)(2,1)S(1)}, bf16[128,768]{1,0:T(8,128)(2,1)}, u32[]{:S(2)}, u32[]{:S(2)}) collective-permute-start(bf16[128,768]{1,0:T(8,128)(2,1)S(1)} %get-tuple-element.18), channel_id=1, source_target_pairs={{0,32},{32,64},{64,96},{96,0},{1,33},{33,65},{65,97},{97,1},{2,34}... | collective-permute-start | bytes 589832 | tf_op jit(solution)/shard_map/ppermute | solution.py:26
  4.3 1.9 collective-permute-start
  11.1 3.5 %shard_map.111 = bf16[16,112,256]{2,1,0:T(8,128)(2,1)} custom-call(s32[1]{0:T(128)} %bitcast.core_ref, s32[1]{0:T(128)} %bitcast.3.y_ref, bf16[1,256]{1,0:T(2,128)(2,1)S(1)} %broadcast_in_dim.13.branch, bf16[1,256]{1,0:T(2,128)(2,1)S(1)} %broadcast_in_dim.14.gain, bf16[512,256]{1,0:T(8,128)(2,1)} %tokens.3, bf16[512,256]{1,0:T(8,128)(2,1)} %tokens.3, ...), custom_call_target="tpu_custom_call" | custom-call | tf_op jit(solution)/shard_map/pallas_call | solution.py:310
  14.6 6.2 %all-to-all-start = ((bf16[16,112,256]{2,1,0:T(8,128)(2,1)}), bf16[16,112,256]{2,1,0:T(8,128)(2,1)S(1)}, u32[]{:S(2)}, u32[]{:S(2)}) async-start(bf16[16,112,256]{2,1,0:T(8,128)(2,1)} %shard_map.111), calls=%async_computation | async-start | bytes 1835008 | tf_op jit(solution)/shard_map/all_to_all | solution.py:18
  20.8 3.2 %collective-permute-start.2 = (bf16[512,256]{1,0:T(8,128)(2,1)S(1)}, bf16[512,256]{1,0:T(8,128)(2,1)S(1)}, u32[]{:S(2)}, u32[]{:S(2)}) collective-permute-start(bf16[512,256]{1,0:T(8,128)(2,1)S(1)} %get-tuple-element.17.first_x), channel_id=1, source_target_pairs={{0,96},{32,0},{64,32},{96,64},{1,97},{33,1},{65,33},{97,65},{2,98}... | collective-permute-start | bytes 786440 | tf_op jit(solution)/shard_map/ppermute | solution.py:26
  24.0 12.6 %collective-permute-done.4.refs_4_ = bf16[128,768]{1,0:T(8,128)(2,1)} collective-permute-done((bf16[128,768]{1,0:T(8,128)(2,1)S(1)}, bf16[128,768]{1,0:T(8,128)(2,1)}, u32[]{:S(2)}, u32[]{:S(2)}) %collective-permute-start.4) | collective-permute-done | bytes 196640 | tf_op jit(solution)/shard_map/ppermute | solution.py:26
  38.5 2.4 %collective-permute-start.13 = (bf16[96,2048]{1,0:T(8,128)(2,1)S(1)}, bf16[96,2048]{1,0:T(8,128)(2,1)S(1)}, u32[]{:S(2)}, u32[]{:S(2)}) collective-permute-start(bf16[96,2048]{1,0:T(8,128)(2,1)S(1)} %get-tuple-element.25), channel_id=1, source_target_pairs={{0,16},{8,24},{16,0},{24,8},{1,17},{9,25},{17,1},{25,9},{2,18},{10... | collective-permute-start | bytes 1179656 | tf_op jit(solution)/shard_map/ppermute | solution.py:26
  45.1 2.8 %shard_map.110 = (f32[128,768]{1,0:T(8,128)S(1)}, bf16[128,768]{1,0:T(8,128)(2,1)S(1)}, bf16[128,768]{1,0:T(8,128)(2,1)S(1)}, bf16[128,768]{1,0:T(8,128)(2,1)S(1)}) custom-call(s32[1]{0:T(128)} %bitcast.core_ref, s32[1]{0:T(128)} %bitcast.1.x_ref, s32[1]{0:T(128)} %bitcast.2.z_ref, bf16[512,256]{1,0:T(8,128)(2,1)S(1)} %get-tuple-element.17.first_x, ...), custom_call_target="tpu_custom_call" | custom-call | tf_op jit(solution)/shard_map/pallas_call | solution.py:310
  49.4 9.9 %collective-permute-done.13.refs_1_ = bf16[96,2048]{1,0:T(8,128)(2,1)S(1)} collective-permute-done((bf16[96,2048]{1,0:T(8,128)(2,1)S(1)}, bf16[96,2048]{1,0:T(8,128)(2,1)S(1)}, u32[]{:S(2)}, u32[]{:S(2)}) %collective-permute-start.13) | collective-permute-done | bytes 393248 | tf_op jit(solution)/shard_map/ppermute | solution.py:26
  63.1 2.3 %collective-permute-start.9 = (bf16[128,768]{1,0:T(8,128)(2,1)S(1)}, bf16[128,768]{1,0:T(8,128)(2,1)S(1)}, u32[]{:S(2)}, u32[]{:S(2)}) collective-permute-start(bf16[128,768]{1,0:T(8,128)(2,1)S(1)} %get-tuple-element.22), channel_id=1, source_target_pairs={{0,8},{8,16},{16,24},{24,0},{1,9},{9,17},{17,25},{25,1},{2,10},{10... | collective-permute-start | bytes 589832 | tf_op jit(solution)/shard_map/ppermute | solution.py:26
  66.8 3.9 %collective-permute-done.9.a = bf16[128,768]{1,0:T(8,128)(2,1)S(1)} collective-permute-done((bf16[128,768]{1,0:T(8,128)(2,1)S(1)}, bf16[128,768]{1,0:T(8,128)(2,1)S(1)}, u32[]{:S(2)}, u32[]{:S(2)}) %collective-permute-start.9) | collective-permute-done | bytes 196640 | tf_op jit(solution)/shard_map/ppermute | solution.py:26
  73.2 3.7 %shard_map.112 = bf16[128,4096]{1,0:T(8,128)(2,1)} custom-call(s32[1]{0:T(128)} %bitcast.core_ref, s32[1]{0:T(128)} %bitcast.1.x_ref, f32[128,768]{1,0:T(8,128)S(1)} %get-tuple-element.21.own, bf16[128,768]{1,0:T(8,128)(2,1)S(1)} %collective-permute-done.9.a, bf16[128,768]{1,0:T(8,128)(2,1)S(1)} %collective-permute-done.10.b, ...), custom_call_target="tpu_custom_call" | custom-call | tf_op jit(solution)/shard_map/pallas_call | solution.py:310
  76.9 4.7 %all-to-all-start.1 = ((bf16[16,8,4096]{2,1,0:T(8,128)(2,1)}), bf16[16,8,4096]{2,1,0:T(8,128)(2,1)S(1)}, u32[]{:S(2)}, u32[]{:S(2)}) async-start(bf16[16,8,4096]{2,1,0:T(8,128)(2,1)} %bitcast.4), calls=%async_computation.1 | async-start | bytes 2097152 | tf_op jit(solution)/shard_map/all_to_all | solution.py:18
  82.6 1.9 collective-permute-start.19
  89.2 33.4 %collective-permute-done.25.refs_2_ = bf16[96,2048]{1,0:T(8,128)(2,1)S(1)} collective-permute-done((bf16[96,2048]{1,0:T(8,128)(2,1)S(1)}, bf16[96,2048]{1,0:T(8,128)(2,1)S(1)}, u32[]{:S(2)}, u32[]{:S(2)}) %collective-permute-start.25) | collective-permute-done | bytes 393248 | tf_op jit(solution)/shard_map/ppermute | solution.py:26
  123.9 2.2 %shard_map.113 = bf16[16,8,4352]{2,1,0:T(8,128)(2,1)} custom-call(bf16[16,8,4096]{2,1,0:T(8,128)(2,1)S(1)} %all-to-all-done.1.got, bf16[16,112,256]{2,1,0:T(8,128)(2,1)} %copy-done.1), custom_call_target="tpu_custom_call" | custom-call | tf_op jit(solution)/shard_map/pallas_call | solution.py:310
  126.1 4.8 %all-to-all-start.2 = ((bf16[16,8,4352]{2,1,0:T(8,128)(2,1)}), bf16[16,8,4352]{2,1,0:T(8,128)(2,1)S(1)}, u32[]{:S(2)}, u32[]{:S(2)}) async-start(bf16[16,8,4352]{2,1,0:T(8,128)(2,1)} %shard_map.113), calls=%async_computation.2 | async-start | bytes 2228224 | tf_op jit(solution)/shard_map/all_to_all | solution.py:18
  130.9 5.5 %collective-permute-done.27.refs_4_ = bf16[96,2048]{1,0:T(8,128)(2,1)} collective-permute-done((bf16[96,2048]{1,0:T(8,128)(2,1)S(1)}, bf16[96,2048]{1,0:T(8,128)(2,1)}, u32[]{:S(2)}, u32[]{:S(2)}) %collective-permute-start.27) | collective-permute-done | bytes 393248 | tf_op jit(solution)/shard_map/ppermute | solution.py:26
  136.4 8.2 %collective-permute-start.26 = (bf16[96,2048]{1,0:T(8,128)(2,1)}, bf16[96,2048]{1,0:T(8,128)(2,1)}, u32[]{:S(2)}, u32[]{:S(2)}) collective-permute-start(bf16[96,2048]{1,0:T(8,128)(2,1)} %copy-done.6), channel_id=1, source_target_pairs={{0,2},{2,4},{4,6},{6,0},{1,3},{3,5},{5,7},{7,1},{8,10},{10,12},{12... | collective-permute-start | bytes 1179656 | tf_op jit(solution)/shard_map/ppermute | solution.py:26
  145.1 11.6 %collective-permute-done.26.refs_3_ = bf16[96,2048]{1,0:T(8,128)(2,1)} collective-permute-done((bf16[96,2048]{1,0:T(8,128)(2,1)}, bf16[96,2048]{1,0:T(8,128)(2,1)}, u32[]{:S(2)}, u32[]{:S(2)}) %collective-permute-start.26) | collective-permute-done | bytes 393248 | tf_op jit(solution)/shard_map/ppermute | solution.py:26
  157.6 4.8 %shard_map.114.near = f32[288,128]{1,0:T(8,128)S(1)} custom-call(s32[1]{0:T(128)} %bitcast.core_ref, bf16[16,8,4352]{2,1,0:T(8,128)(2,1)S(1)} %all-to-all-done.2.got.send, bf16[16,112,256]{2,1,0:T(8,128)(2,1)} %copy-done.1, bf16[16,112,256]{2,1,0:T(8,128)(2,1)} %copy-done.3, bf16[16,96,256]{2,1,0:T(8,128)(2,1)} %collective-permute-done.19.refs_2_, ...), custom_call_target="tpu_custom_call" | custom-call | tf_op jit(solution)/shard_map/pallas_call | solution.py:310
  163.3 4.0 %shard_map.115 = bf16[16,128,256]{2,1,0:T(8,128)(2,1)S(1)} custom-call(s32[1]{0:T(128)} %bitcast.core_ref, bf16[16,8,4352]{2,1,0:T(8,128)(2,1)S(1)} %all-to-all-done.2.got.send, f32[288,128]{1,0:T(8,128)S(1)} %shard_map.114.near, bf16[96,4096]{1,0:T(8,128)(2,1)} %w_down.1, bf16[16,96,256]{2,1,0:T(8,128)(2,1)} %collective-permute-done.23.refs_0_, ...), custom_call_target="tpu_custom_call" | custom-call | tf_op jit(solution)/shard_map/pallas_call | solution.py:310
  167.4 24.5 %all_to_all.25.got = bf16[16,128,256]{2,1,0:T(8,128)(2,1)S(1)} all-to-all(bf16[16,128,256]{2,1,0:T(8,128)(2,1)S(1)} %shard_map.115), channel_id=1, replica_groups=mesh['rz'=4,'rx'=4,'cb'=4,'dp'=2] {'rx','rz'}, dimensions={0} | all-to-all | bytes 2097152 | tf_op jit(solution)/shard_map/all_to_all | solution.py:18
  192.7 11.5 %all_to_all.26 = bf16[4,128,256]{2,1,0:T(8,128)(2,1)S(1)} all-to-all(bf16[4,128,256]{2,1,0:T(8,128)(2,1)S(1)} %shard_map.116), channel_id=1, replica_groups=mesh['rz'=4,'rx'=4,'cb'=4,'dp'=2] {'cb'}, dimensions={0} | all-to-all | bytes 524288 | tf_op jit(solution)/shard_map/all_to_all | solution.py:18
  (94 shorter events, 33.0 us)
Async XLA Ops:
  2.2 18.6 %collective-permute-start.3 = (bf16[128,768]{1,0:T(8,128)(2,1)S(1)}, bf16[128,768]{1,0:T(8,128)(2,1)}, u32[]{:S(2)}, u32[]{:S(2)}) collective-permute-start(bf16[128,768]{1,0:T(8,128)(2,1)S(1)} %get-tuple-element.18), channel_id=1, source_target_pairs={{0,32},{32,64},{64,96},{96,0},{1,33},{33,65},{65,97},{97,1},{2,34}... | collective-permute-start | bytes 589832 | tf_op jit(solution)/shard_map/ppermute | solution.py:26
  4.3 34.2 %collective-permute-start = (bf16[512,256]{1,0:T(8,128)(2,1)S(1)}, bf16[512,256]{1,0:T(8,128)(2,1)}, u32[]{:S(2)}, u32[]{:S(2)}) collective-permute-start(bf16[512,256]{1,0:T(8,128)(2,1)S(1)} %get-tuple-element.17.first_x), channel_id=1, source_target_pairs={{0,32},{32,64},{64,96},{96,0},{1,33},{33,65},{65,97},{97,1},{2,34}... | collective-permute-start | bytes 786440 | tf_op jit(solution)/shard_map/ppermute | solution.py:26
  6.2 34.7 %collective-permute-start.1 = (bf16[512,256]{1,0:T(8,128)(2,1)S(1)}, bf16[512,256]{1,0:T(8,128)(2,1)S(1)}, u32[]{:S(2)}, u32[]{:S(2)}) collective-permute-start(bf16[512,256]{1,0:T(8,128)(2,1)S(1)} %get-tuple-element.17.first_x), channel_id=1, source_target_pairs={{0,64},{32,96},{64,0},{96,32},{1,65},{33,97},{65,1},{97,33},{2,66}... | collective-permute-start | bytes 786440 | tf_op jit(solution)/shard_map/ppermute | solution.py:26
  8.0 28.6 %collective-permute-start.4 = (bf16[128,768]{1,0:T(8,128)(2,1)S(1)}, bf16[128,768]{1,0:T(8,128)(2,1)}, u32[]{:S(2)}, u32[]{:S(2)}) collective-permute-start(bf16[128,768]{1,0:T(8,128)(2,1)S(1)} %get-tuple-element.19), channel_id=1, source_target_pairs={{0,64},{32,96},{64,0},{96,32},{1,65},{33,97},{65,1},{97,33},{2,66}... | collective-permute-start | bytes 589832 | tf_op jit(solution)/shard_map/ppermute | solution.py:26
  9.8 26.9 %collective-permute-start.5 = (bf16[128,768]{1,0:T(8,128)(2,1)S(1)}, bf16[128,768]{1,0:T(8,128)(2,1)}, u32[]{:S(2)}, u32[]{:S(2)}) collective-permute-start(bf16[128,768]{1,0:T(8,128)(2,1)S(1)} %get-tuple-element.20), channel_id=1, source_target_pairs={{0,96},{32,0},{64,32},{96,64},{1,97},{33,1},{65,33},{97,65},{2,98}... | collective-permute-start | bytes 589832 | tf_op jit(solution)/shard_map/ppermute | solution.py:26
  14.6 57.6 %all-to-all-start = ((bf16[16,112,256]{2,1,0:T(8,128)(2,1)}), bf16[16,112,256]{2,1,0:T(8,128)(2,1)S(1)}, u32[]{:S(2)}, u32[]{:S(2)}) async-start(bf16[16,112,256]{2,1,0:T(8,128)(2,1)} %shard_map.111), calls=%async_computation | async-start | bytes 1835008 | tf_op jit(solution)/shard_map/all_to_all | solution.py:18
  20.8 21.4 %collective-permute-start.2 = (bf16[512,256]{1,0:T(8,128)(2,1)S(1)}, bf16[512,256]{1,0:T(8,128)(2,1)S(1)}, u32[]{:S(2)}, u32[]{:S(2)}) collective-permute-start(bf16[512,256]{1,0:T(8,128)(2,1)S(1)} %get-tuple-element.17.first_x), channel_id=1, source_target_pairs={{0,96},{32,0},{64,32},{96,64},{1,97},{33,1},{65,33},{97,65},{2,98}... | collective-permute-start | bytes 786440 | tf_op jit(solution)/shard_map/ppermute | solution.py:26
  38.5 20.8 %collective-permute-start.13 = (bf16[96,2048]{1,0:T(8,128)(2,1)S(1)}, bf16[96,2048]{1,0:T(8,128)(2,1)S(1)}, u32[]{:S(2)}, u32[]{:S(2)}) collective-permute-start(bf16[96,2048]{1,0:T(8,128)(2,1)S(1)} %get-tuple-element.25), channel_id=1, source_target_pairs={{0,16},{8,24},{16,0},{24,8},{1,17},{9,25},{17,1},{25,9},{2,18},{10... | collective-permute-start | bytes 1179656 | tf_op jit(solution)/shard_map/ppermute | solution.py:26
  40.9 18.4 %collective-permute-start.14 = (bf16[96,2048]{1,0:T(8,128)(2,1)S(1)}, bf16[96,2048]{1,0:T(8,128)(2,1)S(1)}, u32[]{:S(2)}, u32[]{:S(2)}) collective-permute-start(bf16[96,2048]{1,0:T(8,128)(2,1)S(1)} %get-tuple-element.25), channel_id=1, source_target_pairs={{0,24},{8,0},{16,8},{24,16},{1,25},{9,1},{17,9},{25,17},{2,26},{10... | collective-permute-start | bytes 1179656 | tf_op jit(solution)/shard_map/ppermute | solution.py:26
  47.9 15.2 %collective-permute-start.10 = (bf16[128,768]{1,0:T(8,128)(2,1)S(1)}, bf16[128,768]{1,0:T(8,128)(2,1)S(1)}, u32[]{:S(2)}, u32[]{:S(2)}) collective-permute-start(bf16[128,768]{1,0:T(8,128)(2,1)S(1)} %get-tuple-element.23), channel_id=1, source_target_pairs={{0,16},{8,24},{16,0},{24,8},{1,17},{9,25},{17,1},{25,9},{2,18},{10... | collective-permute-start | bytes 589832 | tf_op jit(solution)/shard_map/ppermute | solution.py:26
  49.3 21.4 %collective-permute-start.15 = (bf16[96,2048]{1,0:T(8,128)(2,1)S(1)}, bf16[96,2048]{1,0:T(8,128)(2,1)S(1)}, u32[]{:S(2)}, u32[]{:S(2)}) collective-permute-start(bf16[96,2048]{1,0:T(8,128)(2,1)S(1)} %collective-permute-done.12.refs_0_), channel_id=1, source_target_pairs={{0,1},{1,0},{2,3},{3,2},{4,5},{5,4},{6,7},{7,6},{8,9},{9,8},{10,11... | collective-permute-start | bytes 1179656 | tf_op jit(solution)/shard_map/ppermute | solution.py:22
  59.3 12.9 %collective-permute-start.17 = (bf16[96,2048]{1,0:T(8,128)(2,1)S(1)}, bf16[96,2048]{1,0:T(8,128)(2,1)}, u32[]{:S(2)}, u32[]{:S(2)}) collective-permute-start(bf16[96,2048]{1,0:T(8,128)(2,1)S(1)} %collective-permute-done.14.refs_2_), channel_id=1, source_target_pairs={{0,1},{1,0},{2,3},{3,2},{4,5},{5,4},{6,7},{7,6},{8,9},{9,8},{10,11... | collective-permute-start | bytes 1179656 | tf_op jit(solution)/shard_map/ppermute | solution.py:22
  76.9 47.0 %all-to-all-start.1 = ((bf16[16,8,4096]{2,1,0:T(8,128)(2,1)}), bf16[16,8,4096]{2,1,0:T(8,128)(2,1)S(1)}, u32[]{:S(2)}, u32[]{:S(2)}) async-start(bf16[16,8,4096]{2,1,0:T(8,128)(2,1)} %bitcast.4), calls=%async_computation.1 | async-start | bytes 2097152 | tf_op jit(solution)/shard_map/all_to_all | solution.py:18
  82.6 41.3 %collective-permute-start.19 = (bf16[16,96,256]{2,1,0:T(8,128)(2,1)}, bf16[16,96,256]{2,1,0:T(8,128)(2,1)}, u32[]{:S(2)}, u32[]{:S(2)}) collective-permute-start(bf16[16,96,256]{2,1,0:T(8,128)(2,1)} %slice.4), channel_id=1, source_target_pairs={{0,2},{2,4},{4,6},{6,0},{1,3},{3,5},{5,7},{7,1},{8,10},{10,12},{12... | collective-permute-start | bytes 2359304 | tf_op jit(solution)/shard_map/ppermute | solution.py:26
  84.5 38.1 %collective-permute-start.25 = (bf16[96,2048]{1,0:T(8,128)(2,1)S(1)}, bf16[96,2048]{1,0:T(8,128)(2,1)S(1)}, u32[]{:S(2)}, u32[]{:S(2)}) collective-permute-start(bf16[96,2048]{1,0:T(8,128)(2,1)S(1)} %get-tuple-element.26), channel_id=1, source_target_pairs={{0,2},{2,4},{4,6},{6,0},{1,3},{3,5},{5,7},{7,1},{8,10},{10,12},{12... | collective-permute-start | bytes 1179656 | tf_op jit(solution)/shard_map/ppermute | solution.py:26
  86.0 58.6 %collective-permute-start.21 = (bf16[16,96,256]{2,1,0:T(8,128)(2,1)}, bf16[16,96,256]{2,1,0:T(8,128)(2,1)}, u32[]{:S(2)}, u32[]{:S(2)}) collective-permute-start(bf16[16,96,256]{2,1,0:T(8,128)(2,1)} %slice.4), channel_id=1, source_target_pairs={{0,6},{2,0},{4,2},{6,4},{1,7},{3,1},{5,3},{7,5},{8,14},{10,8},{12,... | collective-permute-start | bytes 2359304 | tf_op jit(solution)/shard_map/ppermute | solution.py:26
  87.8 56.8 %collective-permute-start.23 = (bf16[16,96,256]{2,1,0:T(8,128)(2,1)}, bf16[16,96,256]{2,1,0:T(8,128)(2,1)}, u32[]{:S(2)}, u32[]{:S(2)}) collective-permute-start(bf16[16,96,256]{2,1,0:T(8,128)(2,1)} %slice.4), channel_id=1, source_target_pairs={{0,4},{2,6},{4,0},{6,2},{1,5},{3,7},{5,1},{7,3},{8,12},{10,14},{12... | collective-permute-start | bytes 2359304 | tf_op jit(solution)/shard_map/ppermute | solution.py:26
  89.2 67.5 %collective-permute-start.18 = (bf16[16,112,256]{2,1,0:T(8,128)(2,1)S(1)}, bf16[16,112,256]{2,1,0:T(8,128)(2,1)S(1)}, u32[]{:S(2)}, u32[]{:S(2)}) collective-permute-start(bf16[16,112,256]{2,1,0:T(8,128)(2,1)S(1)} %copy-done.2), channel_id=1, source_target_pairs={{0,1},{1,0},{2,3},{3,2},{4,5},{5,4},{6,7},{7,6},{8,9},{9,8},{10,11... | collective-permute-start | bytes 2752520 | tf_op jit(solution)/shard_map/ppermute | solution.py:22
  122.6 13.8 %collective-permute-start.27 = (bf16[96,2048]{1,0:T(8,128)(2,1)S(1)}, bf16[96,2048]{1,0:T(8,128)(2,1)}, u32[]{:S(2)}, u32[]{:S(2)}) collective-permute-start(bf16[96,2048]{1,0:T(8,128)(2,1)S(1)} %get-tuple-element.26), channel_id=1, source_target_pairs={{0,6},{2,0},{4,2},{6,4},{1,7},{3,1},{5,3},{7,5},{8,14},{10,8},{12,... | collective-permute-start | bytes 1179656 | tf_op jit(solution)/shard_map/ppermute | solution.py:26
  123.9 33.3 %collective-permute-start.20 = (bf16[16,96,256]{2,1,0:T(8,128)(2,1)}, bf16[16,96,256]{2,1,0:T(8,128)(2,1)}, u32[]{:S(2)}, u32[]{:S(2)}) collective-permute-start(bf16[16,96,256]{2,1,0:T(8,128)(2,1)} %collective-permute-done.19.refs_2_), channel_id=1, source_target_pairs={{0,1},{1,0},{2,3},{3,2},{4,5},{5,4},{6,7},{7,6},{8,9},{9,8},{10,11... | collective-permute-start | bytes 2359304 | tf_op jit(solution)/shard_map/ppermute | solution.py:22
  126.1 31.2 %all-to-all-start.2 = ((bf16[16,8,4352]{2,1,0:T(8,128)(2,1)}), bf16[16,8,4352]{2,1,0:T(8,128)(2,1)S(1)}, u32[]{:S(2)}, u32[]{:S(2)}) async-start(bf16[16,8,4352]{2,1,0:T(8,128)(2,1)} %shard_map.113), calls=%async_computation.2 | async-start | bytes 2228224 | tf_op jit(solution)/shard_map/all_to_all | solution.py:18
  136.4 20.3 %collective-permute-start.26 = (bf16[96,2048]{1,0:T(8,128)(2,1)}, bf16[96,2048]{1,0:T(8,128)(2,1)}, u32[]{:S(2)}, u32[]{:S(2)}) collective-permute-start(bf16[96,2048]{1,0:T(8,128)(2,1)} %copy-done.6), channel_id=1, source_target_pairs={{0,2},{2,4},{4,6},{6,0},{1,3},{3,5},{5,7},{7,1},{8,10},{10,12},{12... | collective-permute-start | bytes 1179656 | tf_op jit(solution)/shard_map/ppermute | solution.py:26
  144.6 12.7 %collective-permute-start.22 = (bf16[16,96,256]{2,1,0:T(8,128)(2,1)}, bf16[16,96,256]{2,1,0:T(8,128)(2,1)}, u32[]{:S(2)}, u32[]{:S(2)}) collective-permute-start(bf16[16,96,256]{2,1,0:T(8,128)(2,1)} %collective-permute-done.21.refs_4_), channel_id=1, source_target_pairs={{0,1},{1,0},{2,3},{3,2},{4,5},{5,4},{6,7},{7,6},{8,9},{9,8},{10,11... | collective-permute-start | bytes 2359304 | tf_op jit(solution)/shard_map/ppermute | solution.py:22
  144.6 17.9 %collective-permute-start.24 = (bf16[16,96,256]{2,1,0:T(8,128)(2,1)}, bf16[16,96,256]{2,1,0:T(8,128)(2,1)}, u32[]{:S(2)}, u32[]{:S(2)}) collective-permute-start(bf16[16,96,256]{2,1,0:T(8,128)(2,1)} %collective-permute-done.23.refs_0_), channel_id=1, source_target_pairs={{0,1},{1,0},{2,3},{3,2},{4,5},{5,4},{6,7},{7,6},{8,9},{9,8},{10,11... | collective-permute-start | bytes 2359304 | tf_op jit(solution)/shard_map/ppermute | solution.py:22
  (27 other events, 187.3 us)

commit v5 on v1

--- a/solution.py
+++ b/solution.py
@@ -65,7 +65,7 @@
         pairs.append((w.at[:, at_lane(core, half)], mine))
     copies = together(pairs, sems)
     copies[0].wait()
-    scaled[...] = (here[...].astype(f32) * gain[...].astype(f32)).astype(bf16)
+    scaled[...] = (here[...].astype(f32) * gain[...].astype(f32).reshape(1, -1)).astype(bf16)
     wait_for(copies[1:])
 
 
@@ -189,7 +189,7 @@
 
 def finish(got, branch, send, out, middle, sems):
     count, rows = send.shape[:2]
-    width = out.shape[1]
+    width = out.shape[2]
     pairs = [(send.at[:, :, pl.ds(send.shape[2] - width, width)], middle)]
     copies = together(pairs, sems)
     total = jnp.sum(got[...].astype(f32), axis=0)
@@ -197,7 +197,9 @@
     for j in range(count):
         at = slice(j * rows, (j + 1) * rows)
         mid = middle[j].astype(f32)
-        out[at, :] = (residual_scale * mid + 0.5 * branch[...].astype(f32) * total[at]).astype(bf16)
+        value = (residual_scale * mid + 0.5 * branch[...].astype(f32) * total[at]).astype(bf16)
+        for y in range(4):
+            out[y, at, :] = value
 
 
 def feed_forward(core_ref, got, w_down, *refs):
@@ -298,7 +300,7 @@
         w_half,
         jax.ShapeDtypeStruct(tokens.shape, bf16),
         scratch=[pltpu.VMEM(tokens.shape, bf16), dma((9,))],
-    )(core_ref, z_ref, first_gain[None], tokens, first_gate, first_up, first_down, second_down)
+    )(core_ref, z_ref, first_gain, tokens, first_gate, first_up, first_down, second_down)
     w1 = [shifted(w, "rz", step) for step, w in enumerate(w1, 1)]
     x1 = [scaled] + [shifted(scaled, "rz", step) for step in (1, 2, 3)]
     w1_other = [other_core(w) for w in w1]
@@ -314,7 +316,8 @@
 
     d1 = [shifted(d1, "rx", step) for step in (1, 2, 3)]
     d2 = [shifted(d2, "cb", step) for step in (1, 2, 3)]
-    v1 = [v1] + [shifted(v1, "cb", step) for step in (1, 2, 3)]
+    near = [shifted(v1, "cb", step) for step in (1, 3)]
+    v1 = [v1, near[0], shifted(v1, "cb", 2), near[1]]
     d1_other = [other_core(w) for w in d1]
     d2_other = [other_core(w) for w in d2]
     v1 = [w for mine in v1 for w in (mine, other_core(mine))]
@@ -335,7 +338,7 @@
     partial = kernel(
         down_part,
         [SMEM] * 2 + [VMEM] * 4 + [HBM] * 8,
-        jax.ShapeDtypeStruct((few, full), bf16),
+        pltpu.VMEM((few, full), bf16),
         scratch=[pltpu.VMEM((part, full), bf16), pltpu.VMEM((16, 16, width), bf16), dma((8,))],
     )(core_ref, x_ref, own, *got, side, first_down, *d1, *d1_other)
     got = exchange(partial.reshape(16, 8, full), ("rz", "cb"))
@@ -349,7 +352,7 @@
     partial = kernel(
         feed_forward,
         [SMEM, VMEM] + [HBM] * 15,
-        jax.ShapeDtypeStruct((16, few, width), bf16),
+        pltpu.VMEM((16, few, width), bf16),
         scratch=[
             pltpu.VMEM((few, full), bf16),
             pltpu.VMEM((16, 2 * part, width), bf16),
@@ -364,16 +367,11 @@
     out = kernel(
         finish,
         [VMEM, VMEM, HBM],
-        jax.ShapeDtypeStruct((few, width), bf16),
+        pltpu.VMEM((4, few, width), bf16),
         scratch=[pltpu.VMEM((16, 8, width), bf16), dma((1,))],
     )(got, branch, rows)
-    parts = [out] + [shifted(out, "cb", step) for step in (1, 2, 3)]
-    blocks = []
-    for at in range(4):
-        back = (y - at) % 4
-        block = jnp.where(back == 0, parts[0], jnp.where(back == 1, parts[1], jnp.where(back == 2, parts[2], parts[3])))
-        blocks.append(block.reshape(16, 8, width))
-    return jnp.stack(blocks, 1).reshape(n_tok, width)
+    out = exchange(out, "cb")
+    return out.reshape(4, 16, 8, width).transpose(1, 0, 2, 3).reshape(n_tok, width)
 
 
 def solution(mesh):

time: 192 us -> 195 us (1.016)
  blocking collectives: 21.6 us -> 32.1 us
  starting transfers between devices: 54.3 us -> 48.9 us
  waiting for transfers between devices: 85.4 us -> 83.3 us
    all_to_all x1 -> x2, blocking collectives: 21.6 us -> 32.1 us  [exchange(): return lax.all_to_all(x, axes, 0, 0, tiled=True)]
    ppermute x21 -> x18, starting transfers between devices: 36.6 us -> 31.2 us  [shifted(): return lax.ppermute(x, axis, [(i, (i + step) % 4) for i in range(4)])]
    ppermute x21 -> x18, waiting for transfers between devices: 79.8 us -> 77.7 us  [shifted(): return lax.ppermute(x, axis, [(i, (i + step) % 4) for i in range(4)])]
    unnamed x42 -> x44, local copies, waits for them, and re-layouts: 7.19 us -> 7.92 us
  transfers between devices with their start and end apart: 37 -> 34, of which waited for: 15 -> 12; matrix products, arithmetic and copies ran while one was open for 0% -> 0% of each run, Pallas kernels for 4% -> 4%
where the time goes in v5:
time: 195 us
  waiting for transfers between devices  83.3 us (43%)
  starting transfers between devices  48.9 us (25%)
  blocking collectives  32.1 us (16%)
  Pallas kernels  21.3 us (11%)
  local copies, waits for them, and re-layouts  8.73 us (4%)
    ppermute x18, waiting for transfers between devices, shifted(): return lax.ppermute(x, axis, [(i, (i + step) % 4) for i in range(4)])  77.7 us
    all_to_all x2, blocking collectives, exchange(): return lax.all_to_all(x, axes, 0, 0, tiled=True)  32.1 us
    ppermute x18, starting transfers between devices, shifted(): return lax.ppermute(x, axis, [(i, (i + step) % 4) for i in range(4)])  31.2 us
    pallas_call x7, Pallas kernels, run(): return call(*kept)  21.3 us
    all_to_all x3, starting transfers between devices, exchange(): return lax.all_to_all(x, axes, 0, 0, tiled=True)  15.6 us
    unnamed x44, local copies, waits for them, and re-layouts  7.92 us
    ppermute x13, waiting for transfers between devices, other_core(): return lax.ppermute(x, 'dp', [(0, 1), (1, 0)])  5.56 us
  transfers between devices with their start and end apart: 34, of which 12 were waited for; matrix products, arithmetic and copies ran while one was open for 0% of the time, Pallas kernels for 4%

profile of v5, /device:TPU:0, one launch (start us, length us, event | category | flops | bytes accessed | tf_op | source)
XLA Modules:
  0.0 194.5 jit_solution(14105396203967189650)
XLA Ops:
  2.2 2.1 %collective-permute-start.3 = (bf16[128,768]{1,0:T(8,128)(2,1)S(1)}, bf16[128,768]{1,0:T(8,128)(2,1)}, u32[]{:S(2)}, u32[]{:S(2)}) collective-permute-start(bf16[128,768]{1,0:T(8,128)(2,1)S(1)} %get-tuple-element.18), channel_id=1, source_target_pairs={{0,32},{32,64},{64,96},{96,0},{1,33},{33,65},{65,97},{97,1},{2,34}... | collective-permute-start | bytes 589832 | tf_op jit(solution)/shard_map/ppermute | solution.py:26
  11.1 3.5 %shard_map.111 = bf16[16,112,256]{2,1,0:T(8,128)(2,1)} custom-call(s32[1]{0:T(128)} %bitcast.core_ref, s32[1]{0:T(128)} %bitcast.3.y_ref, bf16[1,256]{1,0:T(2,128)(2,1)S(1)} %broadcast_in_dim.9.branch, bf16[1,256]{1,0:T(2,128)(2,1)S(1)} %broadcast_in_dim.10.gain, bf16[512,256]{1,0:T(8,128)(2,1)} %tokens.3, bf16[512,256]{1,0:T(8,128)(2,1)} %tokens.3, ...), custom_call_target="tpu_custom_call" | custom-call | tf_op jit(solution)/shard_map/pallas_call | solution.py:289
  14.6 6.2 %all-to-all-start = ((bf16[16,112,256]{2,1,0:T(8,128)(2,1)}), bf16[16,112,256]{2,1,0:T(8,128)(2,1)S(1)}, u32[]{:S(2)}, u32[]{:S(2)}) async-start(bf16[16,112,256]{2,1,0:T(8,128)(2,1)} %shard_map.111), calls=%async_computation | async-start | bytes 1835008 | tf_op jit(solution)/shard_map/all_to_all | solution.py:18
  20.8 3.2 %collective-permute-start.2 = (bf16[512,256]{1,0:T(8,128)(2,1)S(1)}, bf16[512,256]{1,0:T(8,128)(2,1)S(1)}, u32[]{:S(2)}, u32[]{:S(2)}) collective-permute-start(bf16[512,256]{1,0:T(8,128)(2,1)S(1)} %get-tuple-element.17.first_x), channel_id=1, source_target_pairs={{0,96},{32,0},{64,32},{96,64},{1,97},{33,1},{65,33},{97,65},{2,98}... | collective-permute-start | bytes 786440 | tf_op jit(solution)/shard_map/ppermute | solution.py:26
  24.0 12.6 %collective-permute-done.4.refs_4_ = bf16[128,768]{1,0:T(8,128)(2,1)} collective-permute-done((bf16[128,768]{1,0:T(8,128)(2,1)S(1)}, bf16[128,768]{1,0:T(8,128)(2,1)}, u32[]{:S(2)}, u32[]{:S(2)}) %collective-permute-start.4) | collective-permute-done | bytes 196640 | tf_op jit(solution)/shard_map/ppermute | solution.py:26
  38.6 2.3 %collective-permute-start.13 = (bf16[96,2048]{1,0:T(8,128)(2,1)S(1)}, bf16[96,2048]{1,0:T(8,128)(2,1)S(1)}, u32[]{:S(2)}, u32[]{:S(2)}) collective-permute-start(bf16[96,2048]{1,0:T(8,128)(2,1)S(1)} %get-tuple-element.25), channel_id=1, source_target_pairs={{0,16},{8,24},{16,0},{24,8},{1,17},{9,25},{17,1},{25,9},{2,18},{10... | collective-permute-start | bytes 1179656 | tf_op jit(solution)/shard_map/ppermute | solution.py:26
  46.0 2.8 %shard_map.110 = (f32[128,768]{1,0:T(8,128)S(1)}, bf16[128,768]{1,0:T(8,128)(2,1)S(1)}, bf16[128,768]{1,0:T(8,128)(2,1)S(1)}, bf16[128,768]{1,0:T(8,128)(2,1)S(1)}) custom-call(s32[1]{0:T(128)} %bitcast.core_ref, s32[1]{0:T(128)} %bitcast.1.x_ref, s32[1]{0:T(128)} %bitcast.2.z_ref, bf16[512,256]{1,0:T(8,128)(2,1)S(1)} %get-tuple-element.17.first_x, ...), custom_call_target="tpu_custom_call" | custom-call | tf_op jit(solution)/shard_map/pallas_call | solution.py:289
  49.4 9.9 %collective-permute-done.13.refs_1_ = bf16[96,2048]{1,0:T(8,128)(2,1)S(1)} collective-permute-done((bf16[96,2048]{1,0:T(8,128)(2,1)S(1)}, bf16[96,2048]{1,0:T(8,128)(2,1)S(1)}, u32[]{:S(2)}, u32[]{:S(2)}) %collective-permute-start.13) | collective-permute-done | bytes 393248 | tf_op jit(solution)/shard_map/ppermute | solution.py:26
  59.8 2.0 %collective-permute-start.11 = (bf16[128,768]{1,0:T(8,128)(2,1)S(1)}, bf16[128,768]{1,0:T(8,128)(2,1)S(1)}, u32[]{:S(2)}, u32[]{:S(2)}) collective-permute-start(bf16[128,768]{1,0:T(8,128)(2,1)S(1)} %get-tuple-element.24), channel_id=1, source_target_pairs={{0,24},{8,0},{16,8},{24,16},{1,25},{9,1},{17,9},{25,17},{2,26},{10... | collective-permute-start | bytes 589832 | tf_op jit(solution)/shard_map/ppermute | solution.py:26
  63.1 2.2 %collective-permute-start.9 = (bf16[128,768]{1,0:T(8,128)(2,1)S(1)}, bf16[128,768]{1,0:T(8,128)(2,1)S(1)}, u32[]{:S(2)}, u32[]{:S(2)}) collective-permute-start(bf16[128,768]{1,0:T(8,128)(2,1)S(1)} %get-tuple-element.22), channel_id=1, source_target_pairs={{0,8},{8,16},{16,24},{24,0},{1,9},{9,17},{17,25},{25,1},{2,10},{10... | collective-permute-start | bytes 589832 | tf_op jit(solution)/shard_map/ppermute | solution.py:26
  66.8 3.9 %collective-permute-done.9.a = bf16[128,768]{1,0:T(8,128)(2,1)S(1)} collective-permute-done((bf16[128,768]{1,0:T(8,128)(2,1)S(1)}, bf16[128,768]{1,0:T(8,128)(2,1)S(1)}, u32[]{:S(2)}, u32[]{:S(2)}) %collective-permute-start.9) | collective-permute-done | bytes 196640 | tf_op jit(solution)/shard_map/ppermute | solution.py:26
  73.2 3.7 %shard_map.112 = bf16[128,4096]{1,0:T(8,128)(2,1)} custom-call(s32[1]{0:T(128)} %bitcast.core_ref, s32[1]{0:T(128)} %bitcast.1.x_ref, f32[128,768]{1,0:T(8,128)S(1)} %get-tuple-element.21.own, bf16[128,768]{1,0:T(8,128)(2,1)S(1)} %collective-permute-done.9.a, bf16[128,768]{1,0:T(8,128)(2,1)S(1)} %collective-permute-done.10.b, ...), custom_call_target="tpu_custom_call" | custom-call | tf_op jit(solution)/shard_map/pallas_call | solution.py:289
  76.9 4.7 %all-to-all-start.1 = ((bf16[16,8,4096]{2,1,0:T(8,128)(2,1)}), bf16[16,8,4096]{2,1,0:T(8,128)(2,1)S(1)}, u32[]{:S(2)}, u32[]{:S(2)}) async-start(bf16[16,8,4096]{2,1,0:T(8,128)(2,1)} %bitcast.4), calls=%async_computation.1 | async-start | bytes 2097152 | tf_op jit(solution)/shard_map/all_to_all | solution.py:18
  83.6 2.7 %collective-permute-start.26 = (bf16[96,2048]{1,0:T(8,128)(2,1)S(1)}, bf16[96,2048]{1,0:T(8,128)(2,1)}, u32[]{:S(2)}, u32[]{:S(2)}) collective-permute-start(bf16[96,2048]{1,0:T(8,128)(2,1)S(1)} %get-tuple-element.26), channel_id=1, source_target_pairs={{0,4},{2,6},{4,0},{6,2},{1,5},{3,7},{5,1},{7,3},{8,12},{10,14},{12... | collective-permute-start | bytes 1179656 | tf_op jit(solution)/shard_map/ppermute | solution.py:26
  86.4 2.9 %collective-permute-start.21 = (bf16[16,96,256]{2,1,0:T(8,128)(2,1)S(1)}, bf16[16,96,256]{2,1,0:T(8,128)(2,1)}, u32[]{:S(2)}, u32[]{:S(2)}) collective-permute-start(bf16[16,96,256]{2,1,0:T(8,128)(2,1)S(1)} %slice.4.refs_0_), channel_id=1, source_target_pairs={{0,4},{2,6},{4,0},{6,2},{1,5},{3,7},{5,1},{7,3},{8,12},{10,14},{12... | collective-permute-start | bytes 2359304 | tf_op jit(solution)/shard_map/ppermute | solution.py:26
  89.9 16.8 %collective-permute-done.25.refs_8_ = bf16[96,2048]{1,0:T(8,128)(2,1)} collective-permute-done((bf16[96,2048]{1,0:T(8,128)(2,1)S(1)}, bf16[96,2048]{1,0:T(8,128)(2,1)}, u32[]{:S(2)}, u32[]{:S(2)}) %collective-permute-start.25) | collective-permute-done | bytes 393248 | tf_op jit(solution)/shard_map/ppermute | solution.py:26
  107.1 7.9 %collective-permute-done.26.refs_9_ = bf16[96,2048]{1,0:T(8,128)(2,1)} collective-permute-done((bf16[96,2048]{1,0:T(8,128)(2,1)S(1)}, bf16[96,2048]{1,0:T(8,128)(2,1)}, u32[]{:S(2)}, u32[]{:S(2)}) %collective-permute-start.26) | collective-permute-done | bytes 393248 | tf_op jit(solution)/shard_map/ppermute | solution.py:26
  115.1 2.1 %shard_map.113 = bf16[16,8,4352]{2,1,0:T(8,128)(2,1)} custom-call(bf16[16,8,4096]{2,1,0:T(8,128)(2,1)S(1)} %all-to-all-done.1.got, bf16[16,112,256]{2,1,0:T(8,128)(2,1)} %copy-done.2), custom_call_target="tpu_custom_call" | custom-call | tf_op jit(solution)/shard_map/pallas_call | solution.py:289
  117.2 4.6 %all-to-all-start.2 = ((bf16[16,8,4352]{2,1,0:T(8,128)(2,1)}), bf16[16,8,4352]{2,1,0:T(8,128)(2,1)S(1)}, u32[]{:S(2)}, u32[]{:S(2)}) async-start(bf16[16,8,4352]{2,1,0:T(8,128)(2,1)} %shard_map.113), calls=%async_computation.2 | async-start | bytes 2228224 | tf_op jit(solution)/shard_map/all_to_all | solution.py:18
  121.8 23.0 %collective-permute-done.27.refs_10_ = bf16[96,2048]{1,0:T(8,128)(2,1)} collective-permute-done((bf16[96,2048]{1,0:T(8,128)(2,1)S(1)}, bf16[96,2048]{1,0:T(8,128)(2,1)}, u32[]{:S(2)}, u32[]{:S(2)}) %collective-permute-start.27) | collective-permute-done | bytes 393248 | tf_op jit(solution)/shard_map/ppermute | solution.py:26
  147.7 4.1 %collective-permute-done.30.refs_13_ = bf16[96,2048]{1,0:T(8,128)(2,1)S(1)} collective-permute-done((bf16[96,2048]{1,0:T(8,128)(2,1)}, bf16[96,2048]{1,0:T(8,128)(2,1)S(1)}, u32[]{:S(2)}, u32[]{:S(2)}) %collective-permute-start.30) | collective-permute-done | bytes 393248 | tf_op jit(solution)/shard_map/ppermute | solution.py:22
  154.0 6.8 %shard_map.114 = bf16[16,128,256]{2,1,0:T(8,128)(2,1)S(1)} custom-call(s32[1]{0:T(128)} %bitcast.core_ref, bf16[16,8,4352]{2,1,0:T(8,128)(2,1)S(1)} %all-to-all-done.2.got.send, bf16[96,4096]{1,0:T(8,128)(2,1)} %w_down.1, bf16[16,96,256]{2,1,0:T(8,128)(2,1)} %copy-done.4, bf16[16,96,256]{2,1,0:T(8,128)(2,1)} %copy-done.6, bf16[16,96,256]{2,1,0:T(8,128)(2,1)} %copy-done.5, ...), custom_call_target="tpu_custom_call" | custom-call | tf_op jit(solution)/shard_map/pallas_call | solution.py:289
  160.8 21.6 %all_to_all.25.got = bf16[16,128,256]{2,1,0:T(8,128)(2,1)S(1)} all-to-all(bf16[16,128,256]{2,1,0:T(8,128)(2,1)S(1)} %shard_map.114), channel_id=1, replica_groups=mesh['rz'=4,'rx'=4,'cb'=4,'dp'=2] {'rz','rx'}, dimensions={0} | all-to-all | bytes 2097152 | tf_op jit(solution)/shard_map/all_to_all | solution.py:18
  183.3 10.5 %all_to_all.26 = bf16[4,128,256]{2,1,0:T(8,128)(2,1)S(1)} all-to-all(bf16[4,128,256]{2,1,0:T(8,128)(2,1)S(1)} %shard_map.115), channel_id=1, replica_groups=mesh['rz'=4,'rx'=4,'cb'=4,'dp'=2] {'cb'}, dimensions={0} | all-to-all | bytes 524288 | tf_op jit(solution)/shard_map/all_to_all | solution.py:18
  (102 shorter events, 32.2 us)
Async XLA Ops:
  2.2 18.6 %collective-permute-start.3 = (bf16[128,768]{1,0:T(8,128)(2,1)S(1)}, bf16[128,768]{1,0:T(8,128)(2,1)}, u32[]{:S(2)}, u32[]{:S(2)}) collective-permute-start(bf16[128,768]{1,0:T(8,128)(2,1)S(1)} %get-tuple-element.18), channel_id=1, source_target_pairs={{0,32},{32,64},{64,96},{96,0},{1,33},{33,65},{65,97},{97,1},{2,34}... | collective-permute-start | bytes 589832 | tf_op jit(solution)/shard_map/ppermute | solution.py:26
  4.3 34.3 %collective-permute-start = (bf16[512,256]{1,0:T(8,128)(2,1)S(1)}, bf16[512,256]{1,0:T(8,128)(2,1)}, u32[]{:S(2)}, u32[]{:S(2)}) collective-permute-start(bf16[512,256]{1,0:T(8,128)(2,1)S(1)} %get-tuple-element.17.first_x), channel_id=1, source_target_pairs={{0,32},{32,64},{64,96},{96,0},{1,33},{33,65},{65,97},{97,1},{2,34}... | collective-permute-start | bytes 786440 | tf_op jit(solution)/shard_map/ppermute | solution.py:26
  6.2 34.7 %collective-permute-start.1 = (bf16[512,256]{1,0:T(8,128)(2,1)S(1)}, bf16[512,256]{1,0:T(8,128)(2,1)}, u32[]{:S(2)}, u32[]{:S(2)}) collective-permute-start(bf16[512,256]{1,0:T(8,128)(2,1)S(1)} %get-tuple-element.17.first_x), channel_id=1, source_target_pairs={{0,64},{32,96},{64,0},{96,32},{1,65},{33,97},{65,1},{97,33},{2,66}... | collective-permute-start | bytes 786440 | tf_op jit(solution)/shard_map/ppermute | solution.py:26
  8.0 28.6 %collective-permute-start.4 = (bf16[128,768]{1,0:T(8,128)(2,1)S(1)}, bf16[128,768]{1,0:T(8,128)(2,1)}, u32[]{:S(2)}, u32[]{:S(2)}) collective-permute-start(bf16[128,768]{1,0:T(8,128)(2,1)S(1)} %get-tuple-element.19), channel_id=1, source_target_pairs={{0,64},{32,96},{64,0},{96,32},{1,65},{33,97},{65,1},{97,33},{2,66}... | collective-permute-start | bytes 589832 | tf_op jit(solution)/shard_map/ppermute | solution.py:26
  9.8 26.9 %collective-permute-start.5 = (bf16[128,768]{1,0:T(8,128)(2,1)S(1)}, bf16[128,768]{1,0:T(8,128)(2,1)}, u32[]{:S(2)}, u32[]{:S(2)}) collective-permute-start(bf16[128,768]{1,0:T(8,128)(2,1)S(1)} %get-tuple-element.20), channel_id=1, source_target_pairs={{0,96},{32,0},{64,32},{96,64},{1,97},{33,1},{65,33},{97,65},{2,98}... | collective-permute-start | bytes 589832 | tf_op jit(solution)/shard_map/ppermute | solution.py:26
  14.6 57.7 %all-to-all-start = ((bf16[16,112,256]{2,1,0:T(8,128)(2,1)}), bf16[16,112,256]{2,1,0:T(8,128)(2,1)S(1)}, u32[]{:S(2)}, u32[]{:S(2)}) async-start(bf16[16,112,256]{2,1,0:T(8,128)(2,1)} %shard_map.111), calls=%async_computation | async-start | bytes 1835008 | tf_op jit(solution)/shard_map/all_to_all | solution.py:18
  20.8 21.5 %collective-permute-start.2 = (bf16[512,256]{1,0:T(8,128)(2,1)S(1)}, bf16[512,256]{1,0:T(8,128)(2,1)S(1)}, u32[]{:S(2)}, u32[]{:S(2)}) collective-permute-start(bf16[512,256]{1,0:T(8,128)(2,1)S(1)} %get-tuple-element.17.first_x), channel_id=1, source_target_pairs={{0,96},{32,0},{64,32},{96,64},{1,97},{33,1},{65,33},{97,65},{2,98}... | collective-permute-start | bytes 786440 | tf_op jit(solution)/shard_map/ppermute | solution.py:26
  36.6 12.8 %collective-permute-start.12 = (bf16[96,2048]{1,0:T(8,128)(2,1)S(1)}, bf16[96,2048]{1,0:T(8,128)(2,1)S(1)}, u32[]{:S(2)}, u32[]{:S(2)}) collective-permute-start(bf16[96,2048]{1,0:T(8,128)(2,1)S(1)} %get-tuple-element.25), channel_id=1, source_target_pairs={{0,8},{8,16},{16,24},{24,0},{1,9},{9,17},{17,25},{25,1},{2,10},{10... | collective-permute-start | bytes 1179656 | tf_op jit(solution)/shard_map/ppermute | solution.py:26
  38.6 20.7 %collective-permute-start.13 = (bf16[96,2048]{1,0:T(8,128)(2,1)S(1)}, bf16[96,2048]{1,0:T(8,128)(2,1)S(1)}, u32[]{:S(2)}, u32[]{:S(2)}) collective-permute-start(bf16[96,2048]{1,0:T(8,128)(2,1)S(1)} %get-tuple-element.25), channel_id=1, source_target_pairs={{0,16},{8,24},{16,0},{24,8},{1,17},{9,25},{17,1},{25,9},{2,18},{10... | collective-permute-start | bytes 1179656 | tf_op jit(solution)/shard_map/ppermute | solution.py:26
  40.9 18.4 %collective-permute-start.14 = (bf16[96,2048]{1,0:T(8,128)(2,1)S(1)}, bf16[96,2048]{1,0:T(8,128)(2,1)}, u32[]{:S(2)}, u32[]{:S(2)}) collective-permute-start(bf16[96,2048]{1,0:T(8,128)(2,1)S(1)} %get-tuple-element.25), channel_id=1, source_target_pairs={{0,24},{8,0},{16,8},{24,16},{1,25},{9,1},{17,9},{25,17},{2,26},{10... | collective-permute-start | bytes 1179656 | tf_op jit(solution)/shard_map/ppermute | solution.py:26
  48.8 14.2 %collective-permute-start.10 = (bf16[128,768]{1,0:T(8,128)(2,1)S(1)}, bf16[128,768]{1,0:T(8,128)(2,1)S(1)}, u32[]{:S(2)}, u32[]{:S(2)}) collective-permute-start(bf16[128,768]{1,0:T(8,128)(2,1)S(1)} %get-tuple-element.23), channel_id=1, source_target_pairs={{0,16},{8,24},{16,0},{24,8},{1,17},{9,25},{17,1},{25,9},{2,18},{10... | collective-permute-start | bytes 589832 | tf_op jit(solution)/shard_map/ppermute | solution.py:26
  49.4 21.3 %collective-permute-start.15 = (bf16[96,2048]{1,0:T(8,128)(2,1)S(1)}, bf16[96,2048]{1,0:T(8,128)(2,1)S(1)}, u32[]{:S(2)}, u32[]{:S(2)}) collective-permute-start(bf16[96,2048]{1,0:T(8,128)(2,1)S(1)} %collective-permute-done.12.refs_0_), channel_id=1, source_target_pairs={{0,1},{1,0},{2,3},{3,2},{4,5},{5,4},{6,7},{7,6},{8,9},{9,8},{10,11... | collective-permute-start | bytes 1179656 | tf_op jit(solution)/shard_map/ppermute | solution.py:22
  59.3 11.4 %collective-permute-start.16 = (bf16[96,2048]{1,0:T(8,128)(2,1)S(1)}, bf16[96,2048]{1,0:T(8,128)(2,1)S(1)}, u32[]{:S(2)}, u32[]{:S(2)}) collective-permute-start(bf16[96,2048]{1,0:T(8,128)(2,1)S(1)} %collective-permute-done.13.refs_1_), channel_id=1, source_target_pairs={{0,1},{1,0},{2,3},{3,2},{4,5},{5,4},{6,7},{7,6},{8,9},{9,8},{10,11... | collective-permute-start | bytes 1179656 | tf_op jit(solution)/shard_map/ppermute | solution.py:22
  59.3 12.9 %collective-permute-start.17 = (bf16[96,2048]{1,0:T(8,128)(2,1)}, bf16[96,2048]{1,0:T(8,128)(2,1)}, u32[]{:S(2)}, u32[]{:S(2)}) collective-permute-start(bf16[96,2048]{1,0:T(8,128)(2,1)} %collective-permute-done.14.refs_2_), channel_id=1, source_target_pairs={{0,1},{1,0},{2,3},{3,2},{4,5},{5,4},{6,7},{7,6},{8,9},{9,8},{10,11... | collective-permute-start | bytes 1179656 | tf_op jit(solution)/shard_map/ppermute | solution.py:22
  76.9 38.2 %all-to-all-start.1 = ((bf16[16,8,4096]{2,1,0:T(8,128)(2,1)}), bf16[16,8,4096]{2,1,0:T(8,128)(2,1)S(1)}, u32[]{:S(2)}, u32[]{:S(2)}) async-start(bf16[16,8,4096]{2,1,0:T(8,128)(2,1)} %bitcast.4), calls=%async_computation.1 | async-start | bytes 2097152 | tf_op jit(solution)/shard_map/all_to_all | solution.py:18
  81.6 25.0 %collective-permute-start.25 = (bf16[96,2048]{1,0:T(8,128)(2,1)S(1)}, bf16[96,2048]{1,0:T(8,128)(2,1)}, u32[]{:S(2)}, u32[]{:S(2)}) collective-permute-start(bf16[96,2048]{1,0:T(8,128)(2,1)S(1)} %get-tuple-element.26), channel_id=1, source_target_pairs={{0,2},{2,4},{4,6},{6,0},{1,3},{3,5},{5,7},{7,1},{8,10},{10,12},{12... | collective-permute-start | bytes 1179656 | tf_op jit(solution)/shard_map/ppermute | solution.py:26
  83.6 31.5 %collective-permute-start.26 = (bf16[96,2048]{1,0:T(8,128)(2,1)S(1)}, bf16[96,2048]{1,0:T(8,128)(2,1)}, u32[]{:S(2)}, u32[]{:S(2)}) collective-permute-start(bf16[96,2048]{1,0:T(8,128)(2,1)S(1)} %get-tuple-element.26), channel_id=1, source_target_pairs={{0,4},{2,6},{4,0},{6,2},{1,5},{3,7},{5,1},{7,3},{8,12},{10,14},{12... | collective-permute-start | bytes 1179656 | tf_op jit(solution)/shard_map/ppermute | solution.py:26
  86.3 59.0 %collective-permute-start.19 = (bf16[16,96,256]{2,1,0:T(8,128)(2,1)S(1)}, bf16[16,96,256]{2,1,0:T(8,128)(2,1)S(1)}, u32[]{:S(2)}, u32[]{:S(2)}) collective-permute-start(bf16[16,96,256]{2,1,0:T(8,128)(2,1)S(1)} %slice.4.refs_0_), channel_id=1, source_target_pairs={{0,2},{2,4},{4,6},{6,0},{1,3},{3,5},{5,7},{7,1},{8,10},{10,12},{12... | collective-permute-start | bytes 2359304 | tf_op jit(solution)/shard_map/ppermute | solution.py:26
  86.4 59.9 %collective-permute-start.21 = (bf16[16,96,256]{2,1,0:T(8,128)(2,1)S(1)}, bf16[16,96,256]{2,1,0:T(8,128)(2,1)}, u32[]{:S(2)}, u32[]{:S(2)}) collective-permute-start(bf16[16,96,256]{2,1,0:T(8,128)(2,1)S(1)} %slice.4.refs_0_), channel_id=1, source_target_pairs={{0,4},{2,6},{4,0},{6,2},{1,5},{3,7},{5,1},{7,3},{8,12},{10,14},{12... | collective-permute-start | bytes 2359304 | tf_op jit(solution)/shard_map/ppermute | solution.py:26
  89.3 57.0 %collective-permute-start.23 = (bf16[16,96,256]{2,1,0:T(8,128)(2,1)S(1)}, bf16[16,96,256]{2,1,0:T(8,128)(2,1)}, u32[]{:S(2)}, u32[]{:S(2)}) collective-permute-start(bf16[16,96,256]{2,1,0:T(8,128)(2,1)S(1)} %slice.4.refs_0_), channel_id=1, source_target_pairs={{0,6},{2,0},{4,2},{6,4},{1,7},{3,1},{5,3},{7,5},{8,14},{10,8},{12,... | collective-permute-start | bytes 2359304 | tf_op jit(solution)/shard_map/ppermute | solution.py:26
  106.6 38.1 %collective-permute-start.27 = (bf16[96,2048]{1,0:T(8,128)(2,1)S(1)}, bf16[96,2048]{1,0:T(8,128)(2,1)}, u32[]{:S(2)}, u32[]{:S(2)}) collective-permute-start(bf16[96,2048]{1,0:T(8,128)(2,1)S(1)} %get-tuple-element.26), channel_id=1, source_target_pairs={{0,6},{2,0},{4,2},{6,4},{1,7},{3,1},{5,3},{7,5},{8,14},{10,8},{12,... | collective-permute-start | bytes 1179656 | tf_op jit(solution)/shard_map/ppermute | solution.py:26
  115.0 29.7 %collective-permute-start.28 = (bf16[96,2048]{1,0:T(8,128)(2,1)}, bf16[96,2048]{1,0:T(8,128)(2,1)}, u32[]{:S(2)}, u32[]{:S(2)}) collective-permute-start(bf16[96,2048]{1,0:T(8,128)(2,1)} %collective-permute-done.25.refs_8_), channel_id=1, source_target_pairs={{0,1},{1,0},{2,3},{3,2},{4,5},{5,4},{6,7},{7,6},{8,9},{9,8},{10,11... | collective-permute-start | bytes 1179656 | tf_op jit(solution)/shard_map/ppermute | solution.py:22
  117.2 36.8 %all-to-all-start.2 = ((bf16[16,8,4352]{2,1,0:T(8,128)(2,1)}), bf16[16,8,4352]{2,1,0:T(8,128)(2,1)S(1)}, u32[]{:S(2)}, u32[]{:S(2)}) async-start(bf16[16,8,4352]{2,1,0:T(8,128)(2,1)} %shard_map.113), calls=%async_computation.2 | async-start | bytes 2228224 | tf_op jit(solution)/shard_map/all_to_all | solution.py:18
  146.3 7.7 %collective-permute-start.24 = (bf16[16,96,256]{2,1,0:T(8,128)(2,1)}, bf16[16,96,256]{2,1,0:T(8,128)(2,1)}, u32[]{:S(2)}, u32[]{:S(2)}) collective-permute-start(bf16[16,96,256]{2,1,0:T(8,128)(2,1)} %collective-permute-done.23.refs_6_), channel_id=1, source_target_pairs={{0,1},{1,0},{2,3},{3,2},{4,5},{5,4},{6,7},{7,6},{8,9},{9,8},{10,11... | collective-permute-start | bytes 2359304 | tf_op jit(solution)/shard_map/ppermute | solution.py:22
  (32 other events, 233.3 us)

commit v6 on v5

--- a/solution.py
+++ b/solution.py
@@ -12,6 +12,7 @@
 VMEM = pl.BlockSpec(memory_space=pltpu.VMEM)
 SMEM = pl.BlockSpec(memory_space=pltpu.SMEM)
 HBM = pl.BlockSpec(memory_space=pltpu.HBM)
+ANY = pl.BlockSpec(memory_space=pl.ANY)
 
 
 def exchange(x, axes):
@@ -324,7 +325,7 @@
 
     own, *sends = kernel(
         up_part,
-        [SMEM] * 3 + [VMEM] + [HBM] * 11,
+        [SMEM] * 3 + [VMEM] + [HBM] * 2 + [ANY] * 9,
         jax.ShapeDtypeStruct((few, 2 * part), f32),
         *[jax.ShapeDtypeStruct((few, 2 * part), bf16)] * 3,
         scratch=[
@@ -337,7 +338,7 @@
     got = [shifted(send, "rx", step) for step, send in enumerate(sends, 1)]
     partial = kernel(
         down_part,
-        [SMEM] * 2 + [VMEM] * 4 + [HBM] * 8,
+        [SMEM] * 2 + [VMEM] * 4 + [HBM] * 5 + [ANY] * 3,
         pltpu.VMEM((few, full), bf16),
         scratch=[pltpu.VMEM((part, full), bf16), pltpu.VMEM((16, 16, width), bf16), dma((8,))],
     )(core_ref, x_ref, own, *got, side, first_down, *d1, *d1_other)
@@ -351,7 +352,7 @@
     rows = exchange(send, ("rx", "rz"))
     partial = kernel(
         feed_forward,
-        [SMEM, VMEM] + [HBM] * 15,
+        [SMEM, VMEM] + [HBM] * 4 + [ANY] * 3 + [HBM, ANY] + [HBM] * 6,
         pltpu.VMEM((16, few, width), bf16),
         scratch=[
             pltpu.VMEM((few, full), bf16),

time: 195 us -> 194 us (level)
    unnamed x44 -> x24, local copies, waits for them, and re-layouts: 7.92 us -> 4.62 us
    slice x1, local copies, waits for them, and re-layouts: 0.07 us -> 2.06 us  [shards(): v1 = side[:, :cols // 16]]
  transfers between devices with their start and end apart: 34 -> 34, of which waited for: 12 -> 13; matrix products, arithmetic and copies ran while one was open for 0% -> 1% of each run, Pallas kernels for 4% -> 5%
where the time goes in v6:
time: 194 us; the launch traced here: 193 us
  waiting for transfers between devices  82.4 us (42%)
  starting transfers between devices  49 us (25%)
  blocking collectives  33.1 us (17%)
  Pallas kernels  21 us (11%)
  local copies, waits for them, and re-layouts  7.43 us (4%)
    ppermute x18, waiting for transfers between devices, shifted(): return lax.ppermute(x, axis, [(i, (i + step) % 4) for i in range(4)])  77 us
    all_to_all x2, blocking collectives, exchange(): return lax.all_to_all(x, axes, 0, 0, tiled=True)  33.1 us
    ppermute x18, starting transfers between devices, shifted(): return lax.ppermute(x, axis, [(i, (i + step) % 4) for i in range(4)])  31 us
    pallas_call x7, Pallas kernels, run(): return call(*kept)  21 us
    all_to_all x3, starting transfers between devices, exchange(): return lax.all_to_all(x, axes, 0, 0, tiled=True)  15.7 us
    ppermute x13, waiting for transfers between devices, other_core(): return lax.ppermute(x, 'dp', [(0, 1), (1, 0)])  5.41 us
    unnamed x24, local copies, waits for them, and re-layouts  4.62 us
  transfers between devices with their start and end apart: 34, of which 13 were waited for; matrix products, arithmetic and copies ran while one was open for 1% of the time, Pallas kernels for 5%

profile of v6, /device:TPU:0, one launch (start us, length us, event | category | flops | bytes accessed | tf_op | source)
XLA Modules:
  0.0 193.1 jit_solution(16273797878292582867)
XLA Ops:
  2.2 2.1 %collective-permute-start.3 = (bf16[128,768]{1,0:T(8,128)(2,1)S(1)}, bf16[128,768]{1,0:T(8,128)(2,1)S(1)}, u32[]{:S(2)}, u32[]{:S(2)}) collective-permute-start(bf16[128,768]{1,0:T(8,128)(2,1)S(1)} %get-tuple-element.18), channel_id=1, source_target_pairs={{0,32},{32,64},{64,96},{96,0},{1,33},{33,65},{65,97},{97,1},{2,34}... | collective-permute-start | bytes 589832 | tf_op jit(solution)/shard_map/ppermute | solution.py:27
  11.1 3.5 %shard_map.111 = bf16[16,112,256]{2,1,0:T(8,128)(2,1)} custom-call(s32[1]{0:T(128)} %bitcast.core_ref, s32[1]{0:T(128)} %bitcast.3.y_ref, bf16[1,256]{1,0:T(2,128)(2,1)S(1)} %broadcast_in_dim.9.branch, bf16[1,256]{1,0:T(2,128)(2,1)S(1)} %broadcast_in_dim.10.gain, bf16[512,256]{1,0:T(8,128)(2,1)} %tokens.3, bf16[512,256]{1,0:T(8,128)(2,1)} %tokens.3, ...), custom_call_target="tpu_custom_call" | custom-call | tf_op jit(solution)/shard_map/pallas_call | solution.py:290
  14.6 6.3 %all-to-all-start = ((bf16[16,112,256]{2,1,0:T(8,128)(2,1)}), bf16[16,112,256]{2,1,0:T(8,128)(2,1)}, u32[]{:S(2)}, u32[]{:S(2)}) async-start(bf16[16,112,256]{2,1,0:T(8,128)(2,1)} %shard_map.111), calls=%async_computation | async-start | bytes 1835008 | tf_op jit(solution)/shard_map/all_to_all | solution.py:19
  20.9 3.2 %collective-permute-start.2 = (bf16[512,256]{1,0:T(8,128)(2,1)S(1)}, bf16[512,256]{1,0:T(8,128)(2,1)S(1)}, u32[]{:S(2)}, u32[]{:S(2)}) collective-permute-start(bf16[512,256]{1,0:T(8,128)(2,1)S(1)} %get-tuple-element.17.first_x), channel_id=1, source_target_pairs={{0,96},{32,0},{64,32},{96,64},{1,97},{33,1},{65,33},{97,65},{2,98}... | collective-permute-start | bytes 786440 | tf_op jit(solution)/shard_map/ppermute | solution.py:27
  24.0 12.5 %collective-permute-done.4.refs_4_ = bf16[128,768]{1,0:T(8,128)(2,1)S(1)} collective-permute-done((bf16[128,768]{1,0:T(8,128)(2,1)S(1)}, bf16[128,768]{1,0:T(8,128)(2,1)S(1)}, u32[]{:S(2)}, u32[]{:S(2)}) %collective-permute-start.4) | collective-permute-done | bytes 196640 | tf_op jit(solution)/shard_map/ppermute | solution.py:27
  38.4 2.4 %collective-permute-start.13 = (bf16[96,2048]{1,0:T(8,128)(2,1)S(1)}, bf16[96,2048]{1,0:T(8,128)(2,1)}, u32[]{:S(2)}, u32[]{:S(2)}) collective-permute-start(bf16[96,2048]{1,0:T(8,128)(2,1)S(1)} %get-tuple-element.25), channel_id=1, source_target_pairs={{0,16},{8,24},{16,0},{24,8},{1,17},{9,25},{17,1},{25,9},{2,18},{10... | collective-permute-start | bytes 1179656 | tf_op jit(solution)/shard_map/ppermute | solution.py:27
  43.9 3.1 %shard_map.110 = (f32[128,768]{1,0:T(8,128)S(1)}, bf16[128,768]{1,0:T(8,128)(2,1)S(1)}, bf16[128,768]{1,0:T(8,128)(2,1)S(1)}, bf16[128,768]{1,0:T(8,128)(2,1)S(1)}) custom-call(s32[1]{0:T(128)} %bitcast.core_ref, s32[1]{0:T(128)} %bitcast.1.x_ref, s32[1]{0:T(128)} %bitcast.2.z_ref, bf16[512,256]{1,0:T(8,128)(2,1)S(1)} %get-tuple-element.17.first_x, ...), custom_call_target="tpu_custom_call" | custom-call | tf_op jit(solution)/shard_map/pallas_call | solution.py:290
  49.3 10.0 %collective-permute-done.13.refs_1_ = bf16[96,2048]{1,0:T(8,128)(2,1)} collective-permute-done((bf16[96,2048]{1,0:T(8,128)(2,1)S(1)}, bf16[96,2048]{1,0:T(8,128)(2,1)}, u32[]{:S(2)}, u32[]{:S(2)}) %collective-permute-start.13) | collective-permute-done | bytes 393248 | tf_op jit(solution)/shard_map/ppermute | solution.py:27
  62.9 2.2 %collective-permute-start.9 = (bf16[128,768]{1,0:T(8,128)(2,1)S(1)}, bf16[128,768]{1,0:T(8,128)(2,1)S(1)}, u32[]{:S(2)}, u32[]{:S(2)}) collective-permute-start(bf16[128,768]{1,0:T(8,128)(2,1)S(1)} %get-tuple-element.22), channel_id=1, source_target_pairs={{0,8},{8,16},{16,24},{24,0},{1,9},{9,17},{17,25},{25,1},{2,10},{10... | collective-permute-start | bytes 589832 | tf_op jit(solution)/shard_map/ppermute | solution.py:27
  66.7 3.9 %collective-permute-done.9.a = bf16[128,768]{1,0:T(8,128)(2,1)S(1)} collective-permute-done((bf16[128,768]{1,0:T(8,128)(2,1)S(1)}, bf16[128,768]{1,0:T(8,128)(2,1)S(1)}, u32[]{:S(2)}, u32[]{:S(2)}) %collective-permute-start.9) | collective-permute-done | bytes 196640 | tf_op jit(solution)/shard_map/ppermute | solution.py:27
  70.6 3.3 %shard_map.112 = bf16[128,4096]{1,0:T(8,128)(2,1)} custom-call(s32[1]{0:T(128)} %bitcast.core_ref, s32[1]{0:T(128)} %bitcast.1.x_ref, f32[128,768]{1,0:T(8,128)S(1)} %get-tuple-element.21.own, bf16[128,768]{1,0:T(8,128)(2,1)S(1)} %collective-permute-done.9.a, bf16[128,768]{1,0:T(8,128)(2,1)S(1)} %collective-permute-done.10.b, ...), custom_call_target="tpu_custom_call" | custom-call | tf_op jit(solution)/shard_map/pallas_call | solution.py:290
  74.0 4.6 %all-to-all-start.1 = ((bf16[16,8,4096]{2,1,0:T(8,128)(2,1)}), bf16[16,8,4096]{2,1,0:T(8,128)(2,1)S(1)}, u32[]{:S(2)}, u32[]{:S(2)}) async-start(bf16[16,8,4096]{2,1,0:T(8,128)(2,1)} %bitcast.4), calls=%async_computation.1 | async-start | bytes 2097152 | tf_op jit(solution)/shard_map/all_to_all | solution.py:19
  80.5 2.7 %collective-permute-start.26 = (bf16[96,2048]{1,0:T(8,128)(2,1)S(1)}, bf16[96,2048]{1,0:T(8,128)(2,1)}, u32[]{:S(2)}, u32[]{:S(2)}) collective-permute-start(bf16[96,2048]{1,0:T(8,128)(2,1)S(1)} %get-tuple-element.26), channel_id=1, source_target_pairs={{0,4},{2,6},{4,0},{6,2},{1,5},{3,7},{5,1},{7,3},{8,12},{10,14},{12... | collective-permute-start | bytes 1179656 | tf_op jit(solution)/shard_map/ppermute | solution.py:27
  83.2 2.1 %slice.4.refs_0_ = bf16[16,96,256]{2,1,0:T(8,128)(2,1)} slice(bf16[16,112,256]{2,1,0:T(8,128)(2,1)} %all-to-all-done.side), slice={[0:16], [0:96], [0:256]} | slice | bytes 1572864 | tf_op jit(solution)/shard_map/slice | solution.py:316
  85.3 2.9 %collective-permute-start.21 = (bf16[16,96,256]{2,1,0:T(8,128)(2,1)}, bf16[16,96,256]{2,1,0:T(8,128)(2,1)S(1)}, u32[]{:S(2)}, u32[]{:S(2)}) collective-permute-start(bf16[16,96,256]{2,1,0:T(8,128)(2,1)} %slice.4.refs_0_), channel_id=1, source_target_pairs={{0,4},{2,6},{4,0},{6,2},{1,5},{3,7},{5,1},{7,3},{8,12},{10,14},{12... | collective-permute-start | bytes 2359304 | tf_op jit(solution)/shard_map/ppermute | solution.py:27
  88.7 14.7 %collective-permute-done.25.refs_8_ = bf16[96,2048]{1,0:T(8,128)(2,1)S(1)} collective-permute-done((bf16[96,2048]{1,0:T(8,128)(2,1)S(1)}, bf16[96,2048]{1,0:T(8,128)(2,1)S(1)}, u32[]{:S(2)}, u32[]{:S(2)}) %collective-permute-start.25) | collective-permute-done | bytes 393248 | tf_op jit(solution)/shard_map/ppermute | solution.py:27
  104.0 8.0 %collective-permute-done.26.refs_9_ = bf16[96,2048]{1,0:T(8,128)(2,1)} collective-permute-done((bf16[96,2048]{1,0:T(8,128)(2,1)S(1)}, bf16[96,2048]{1,0:T(8,128)(2,1)}, u32[]{:S(2)}, u32[]{:S(2)}) %collective-permute-start.26) | collective-permute-done | bytes 393248 | tf_op jit(solution)/shard_map/ppermute | solution.py:27
  112.0 2.1 %shard_map.113 = bf16[16,8,4352]{2,1,0:T(8,128)(2,1)} custom-call(bf16[16,8,4096]{2,1,0:T(8,128)(2,1)S(1)} %all-to-all-done.1.got, bf16[16,112,256]{2,1,0:T(8,128)(2,1)} %all-to-all-done.side), custom_call_target="tpu_custom_call" | custom-call | tf_op jit(solution)/shard_map/pallas_call | solution.py:290
  114.2 4.9 %all-to-all-start.2 = ((bf16[16,8,4352]{2,1,0:T(8,128)(2,1)}), bf16[16,8,4352]{2,1,0:T(8,128)(2,1)S(1)}, u32[]{:S(2)}, u32[]{:S(2)}) async-start(bf16[16,8,4352]{2,1,0:T(8,128)(2,1)} %shard_map.113), calls=%async_computation.2 | async-start | bytes 2228224 | tf_op jit(solution)/shard_map/all_to_all | solution.py:19
  119.0 22.7 %collective-permute-done.27.refs_10_ = bf16[96,2048]{1,0:T(8,128)(2,1)} collective-permute-done((bf16[96,2048]{1,0:T(8,128)(2,1)S(1)}, bf16[96,2048]{1,0:T(8,128)(2,1)}, u32[]{:S(2)}, u32[]{:S(2)}) %collective-permute-start.27) | collective-permute-done | bytes 393248 | tf_op jit(solution)/shard_map/ppermute | solution.py:27
  144.6 4.2 %collective-permute-done.30.refs_13_ = bf16[96,2048]{1,0:T(8,128)(2,1)S(1)} collective-permute-done((bf16[96,2048]{1,0:T(8,128)(2,1)}, bf16[96,2048]{1,0:T(8,128)(2,1)S(1)}, u32[]{:S(2)}, u32[]{:S(2)}) %collective-permute-start.30) | collective-permute-done | bytes 393248 | tf_op jit(solution)/shard_map/ppermute | solution.py:23
  151.8 6.6 %shard_map.114 = bf16[16,128,256]{2,1,0:T(8,128)(2,1)S(1)} custom-call(s32[1]{0:T(128)} %bitcast.core_ref, bf16[16,8,4352]{2,1,0:T(8,128)(2,1)S(1)} %all-to-all-done.2.got.send, bf16[96,4096]{1,0:T(8,128)(2,1)} %w_down.1, bf16[16,96,256]{2,1,0:T(8,128)(2,1)} %slice.4.refs_0_, bf16[16,96,256]{2,1,0:T(8,128)(2,1)} %copy-done.4, ...), custom_call_target="tpu_custom_call" | custom-call | tf_op jit(solution)/shard_map/pallas_call | solution.py:290
  158.4 22.6 %all_to_all.25.got = bf16[16,128,256]{2,1,0:T(8,128)(2,1)S(1)} all-to-all(bf16[16,128,256]{2,1,0:T(8,128)(2,1)S(1)} %shard_map.114), channel_id=1, replica_groups=mesh['rz'=4,'rx'=4,'cb'=4,'dp'=2] {'rz','rx'}, dimensions={0} | all-to-all | bytes 2097152 | tf_op jit(solution)/shard_map/all_to_all | solution.py:19
  181.9 10.4 %all_to_all.26 = bf16[4,128,256]{2,1,0:T(8,128)(2,1)S(1)} all-to-all(bf16[4,128,256]{2,1,0:T(8,128)(2,1)S(1)} %shard_map.115), channel_id=1, replica_groups=mesh['rz'=4,'rx'=4,'cb'=4,'dp'=2] {'cb'}, dimensions={0} | all-to-all | bytes 524288 | tf_op jit(solution)/shard_map/all_to_all | solution.py:19
  (82 shorter events, 32.0 us)
Async XLA Ops:
  2.2 18.7 %collective-permute-start.3 = (bf16[128,768]{1,0:T(8,128)(2,1)S(1)}, bf16[128,768]{1,0:T(8,128)(2,1)S(1)}, u32[]{:S(2)}, u32[]{:S(2)}) collective-permute-start(bf16[128,768]{1,0:T(8,128)(2,1)S(1)} %get-tuple-element.18), channel_id=1, source_target_pairs={{0,32},{32,64},{64,96},{96,0},{1,33},{33,65},{65,97},{97,1},{2,34}... | collective-permute-start | bytes 589832 | tf_op jit(solution)/shard_map/ppermute | solution.py:27
  4.3 34.1 %collective-permute-start = (bf16[512,256]{1,0:T(8,128)(2,1)S(1)}, bf16[512,256]{1,0:T(8,128)(2,1)S(1)}, u32[]{:S(2)}, u32[]{:S(2)}) collective-permute-start(bf16[512,256]{1,0:T(8,128)(2,1)S(1)} %get-tuple-element.17.first_x), channel_id=1, source_target_pairs={{0,32},{32,64},{64,96},{96,0},{1,33},{33,65},{65,97},{97,1},{2,34}... | collective-permute-start | bytes 786440 | tf_op jit(solution)/shard_map/ppermute | solution.py:27
  6.2 34.6 %collective-permute-start.1 = (bf16[512,256]{1,0:T(8,128)(2,1)S(1)}, bf16[512,256]{1,0:T(8,128)(2,1)S(1)}, u32[]{:S(2)}, u32[]{:S(2)}) collective-permute-start(bf16[512,256]{1,0:T(8,128)(2,1)S(1)} %get-tuple-element.17.first_x), channel_id=1, source_target_pairs={{0,64},{32,96},{64,0},{96,32},{1,65},{33,97},{65,1},{97,33},{2,66}... | collective-permute-start | bytes 786440 | tf_op jit(solution)/shard_map/ppermute | solution.py:27
  8.0 28.5 %collective-permute-start.4 = (bf16[128,768]{1,0:T(8,128)(2,1)S(1)}, bf16[128,768]{1,0:T(8,128)(2,1)S(1)}, u32[]{:S(2)}, u32[]{:S(2)}) collective-permute-start(bf16[128,768]{1,0:T(8,128)(2,1)S(1)} %get-tuple-element.19), channel_id=1, source_target_pairs={{0,64},{32,96},{64,0},{96,32},{1,65},{33,97},{65,1},{97,33},{2,66}... | collective-permute-start | bytes 589832 | tf_op jit(solution)/shard_map/ppermute | solution.py:27
  9.8 26.7 %collective-permute-start.5 = (bf16[128,768]{1,0:T(8,128)(2,1)S(1)}, bf16[128,768]{1,0:T(8,128)(2,1)S(1)}, u32[]{:S(2)}, u32[]{:S(2)}) collective-permute-start(bf16[128,768]{1,0:T(8,128)(2,1)S(1)} %get-tuple-element.20), channel_id=1, source_target_pairs={{0,96},{32,0},{64,32},{96,64},{1,97},{33,1},{65,33},{97,65},{2,98}... | collective-permute-start | bytes 589832 | tf_op jit(solution)/shard_map/ppermute | solution.py:27
  14.6 56.1 %all-to-all-start = ((bf16[16,112,256]{2,1,0:T(8,128)(2,1)}), bf16[16,112,256]{2,1,0:T(8,128)(2,1)}, u32[]{:S(2)}, u32[]{:S(2)}) async-start(bf16[16,112,256]{2,1,0:T(8,128)(2,1)} %shard_map.111), calls=%async_computation | async-start | bytes 1835008 | tf_op jit(solution)/shard_map/all_to_all | solution.py:19
  20.9 21.3 %collective-permute-start.2 = (bf16[512,256]{1,0:T(8,128)(2,1)S(1)}, bf16[512,256]{1,0:T(8,128)(2,1)S(1)}, u32[]{:S(2)}, u32[]{:S(2)}) collective-permute-start(bf16[512,256]{1,0:T(8,128)(2,1)S(1)} %get-tuple-element.17.first_x), channel_id=1, source_target_pairs={{0,96},{32,0},{64,32},{96,64},{1,97},{33,1},{65,33},{97,65},{2,98}... | collective-permute-start | bytes 786440 | tf_op jit(solution)/shard_map/ppermute | solution.py:27
  36.5 12.8 %collective-permute-start.12 = (bf16[96,2048]{1,0:T(8,128)(2,1)S(1)}, bf16[96,2048]{1,0:T(8,128)(2,1)}, u32[]{:S(2)}, u32[]{:S(2)}) collective-permute-start(bf16[96,2048]{1,0:T(8,128)(2,1)S(1)} %get-tuple-element.25), channel_id=1, source_target_pairs={{0,8},{8,16},{16,24},{24,0},{1,9},{9,17},{17,25},{25,1},{2,10},{10... | collective-permute-start | bytes 1179656 | tf_op jit(solution)/shard_map/ppermute | solution.py:27
  38.4 20.9 %collective-permute-start.13 = (bf16[96,2048]{1,0:T(8,128)(2,1)S(1)}, bf16[96,2048]{1,0:T(8,128)(2,1)}, u32[]{:S(2)}, u32[]{:S(2)}) collective-permute-start(bf16[96,2048]{1,0:T(8,128)(2,1)S(1)} %get-tuple-element.25), channel_id=1, source_target_pairs={{0,16},{8,24},{16,0},{24,8},{1,17},{9,25},{17,1},{25,9},{2,18},{10... | collective-permute-start | bytes 1179656 | tf_op jit(solution)/shard_map/ppermute | solution.py:27
  40.8 18.5 %collective-permute-start.14 = (bf16[96,2048]{1,0:T(8,128)(2,1)S(1)}, bf16[96,2048]{1,0:T(8,128)(2,1)}, u32[]{:S(2)}, u32[]{:S(2)}) collective-permute-start(bf16[96,2048]{1,0:T(8,128)(2,1)S(1)} %get-tuple-element.25), channel_id=1, source_target_pairs={{0,24},{8,0},{16,8},{24,16},{1,25},{9,1},{17,9},{25,17},{2,26},{10... | collective-permute-start | bytes 1179656 | tf_op jit(solution)/shard_map/ppermute | solution.py:27
  47.0 15.9 %collective-permute-start.10 = (bf16[128,768]{1,0:T(8,128)(2,1)S(1)}, bf16[128,768]{1,0:T(8,128)(2,1)S(1)}, u32[]{:S(2)}, u32[]{:S(2)}) collective-permute-start(bf16[128,768]{1,0:T(8,128)(2,1)S(1)} %get-tuple-element.23), channel_id=1, source_target_pairs={{0,16},{8,24},{16,0},{24,8},{1,17},{9,25},{17,1},{25,9},{2,18},{10... | collective-permute-start | bytes 589832 | tf_op jit(solution)/shard_map/ppermute | solution.py:27
  49.3 21.3 %collective-permute-start.15 = (bf16[96,2048]{1,0:T(8,128)(2,1)}, bf16[96,2048]{1,0:T(8,128)(2,1)S(1)}, u32[]{:S(2)}, u32[]{:S(2)}) collective-permute-start(bf16[96,2048]{1,0:T(8,128)(2,1)} %collective-permute-done.12.refs_0_), channel_id=1, source_target_pairs={{0,1},{1,0},{2,3},{3,2},{4,5},{5,4},{6,7},{7,6},{8,9},{9,8},{10,11... | collective-permute-start | bytes 1179656 | tf_op jit(solution)/shard_map/ppermute | solution.py:23
  59.3 11.3 %collective-permute-start.16 = (bf16[96,2048]{1,0:T(8,128)(2,1)}, bf16[96,2048]{1,0:T(8,128)(2,1)S(1)}, u32[]{:S(2)}, u32[]{:S(2)}) collective-permute-start(bf16[96,2048]{1,0:T(8,128)(2,1)} %collective-permute-done.13.refs_1_), channel_id=1, source_target_pairs={{0,1},{1,0},{2,3},{3,2},{4,5},{5,4},{6,7},{7,6},{8,9},{9,8},{10,11... | collective-permute-start | bytes 1179656 | tf_op jit(solution)/shard_map/ppermute | solution.py:23
  59.3 11.3 %collective-permute-start.17 = (bf16[96,2048]{1,0:T(8,128)(2,1)}, bf16[96,2048]{1,0:T(8,128)(2,1)S(1)}, u32[]{:S(2)}, u32[]{:S(2)}) collective-permute-start(bf16[96,2048]{1,0:T(8,128)(2,1)} %collective-permute-done.14.refs_2_), channel_id=1, source_target_pairs={{0,1},{1,0},{2,3},{3,2},{4,5},{5,4},{6,7},{7,6},{8,9},{9,8},{10,11... | collective-permute-start | bytes 1179656 | tf_op jit(solution)/shard_map/ppermute | solution.py:23
  62.9 7.7 %collective-permute-start.9 = (bf16[128,768]{1,0:T(8,128)(2,1)S(1)}, bf16[128,768]{1,0:T(8,128)(2,1)S(1)}, u32[]{:S(2)}, u32[]{:S(2)}) collective-permute-start(bf16[128,768]{1,0:T(8,128)(2,1)S(1)} %get-tuple-element.22), channel_id=1, source_target_pairs={{0,8},{8,16},{16,24},{24,0},{1,9},{9,17},{17,25},{25,1},{2,10},{10... | collective-permute-start | bytes 589832 | tf_op jit(solution)/shard_map/ppermute | solution.py:27
  74.0 38.0 %all-to-all-start.1 = ((bf16[16,8,4096]{2,1,0:T(8,128)(2,1)}), bf16[16,8,4096]{2,1,0:T(8,128)(2,1)S(1)}, u32[]{:S(2)}, u32[]{:S(2)}) async-start(bf16[16,8,4096]{2,1,0:T(8,128)(2,1)} %bitcast.4), calls=%async_computation.1 | async-start | bytes 2097152 | tf_op jit(solution)/shard_map/all_to_all | solution.py:19
  78.6 24.9 %collective-permute-start.25 = (bf16[96,2048]{1,0:T(8,128)(2,1)S(1)}, bf16[96,2048]{1,0:T(8,128)(2,1)S(1)}, u32[]{:S(2)}, u32[]{:S(2)}) collective-permute-start(bf16[96,2048]{1,0:T(8,128)(2,1)S(1)} %get-tuple-element.26), channel_id=1, source_target_pairs={{0,2},{2,4},{4,6},{6,0},{1,3},{3,5},{5,7},{7,1},{8,10},{10,12},{12... | collective-permute-start | bytes 1179656 | tf_op jit(solution)/shard_map/ppermute | solution.py:27
  80.5 31.5 %collective-permute-start.26 = (bf16[96,2048]{1,0:T(8,128)(2,1)S(1)}, bf16[96,2048]{1,0:T(8,128)(2,1)}, u32[]{:S(2)}, u32[]{:S(2)}) collective-permute-start(bf16[96,2048]{1,0:T(8,128)(2,1)S(1)} %get-tuple-element.26), channel_id=1, source_target_pairs={{0,4},{2,6},{4,0},{6,2},{1,5},{3,7},{5,1},{7,3},{8,12},{10,14},{12... | collective-permute-start | bytes 1179656 | tf_op jit(solution)/shard_map/ppermute | solution.py:27
  85.2 57.0 %collective-permute-start.19 = (bf16[16,96,256]{2,1,0:T(8,128)(2,1)}, bf16[16,96,256]{2,1,0:T(8,128)(2,1)}, u32[]{:S(2)}, u32[]{:S(2)}) collective-permute-start(bf16[16,96,256]{2,1,0:T(8,128)(2,1)} %slice.4.refs_0_), channel_id=1, source_target_pairs={{0,2},{2,4},{4,6},{6,0},{1,3},{3,5},{5,7},{7,1},{8,10},{10,12},{12... | collective-permute-start | bytes 2359304 | tf_op jit(solution)/shard_map/ppermute | solution.py:27
  85.3 57.9 %collective-permute-start.21 = (bf16[16,96,256]{2,1,0:T(8,128)(2,1)}, bf16[16,96,256]{2,1,0:T(8,128)(2,1)S(1)}, u32[]{:S(2)}, u32[]{:S(2)}) collective-permute-start(bf16[16,96,256]{2,1,0:T(8,128)(2,1)} %slice.4.refs_0_), channel_id=1, source_target_pairs={{0,4},{2,6},{4,0},{6,2},{1,5},{3,7},{5,1},{7,3},{8,12},{10,14},{12... | collective-permute-start | bytes 2359304 | tf_op jit(solution)/shard_map/ppermute | solution.py:27
  88.2 55.0 %collective-permute-start.23 = (bf16[16,96,256]{2,1,0:T(8,128)(2,1)}, bf16[16,96,256]{2,1,0:T(8,128)(2,1)}, u32[]{:S(2)}, u32[]{:S(2)}) collective-permute-start(bf16[16,96,256]{2,1,0:T(8,128)(2,1)} %slice.4.refs_0_), channel_id=1, source_target_pairs={{0,6},{2,0},{4,2},{6,4},{1,7},{3,1},{5,3},{7,5},{8,14},{10,8},{12,... | collective-permute-start | bytes 2359304 | tf_op jit(solution)/shard_map/ppermute | solution.py:27
  103.5 38.3 %collective-permute-start.27 = (bf16[96,2048]{1,0:T(8,128)(2,1)S(1)}, bf16[96,2048]{1,0:T(8,128)(2,1)}, u32[]{:S(2)}, u32[]{:S(2)}) collective-permute-start(bf16[96,2048]{1,0:T(8,128)(2,1)S(1)} %get-tuple-element.26), channel_id=1, source_target_pairs={{0,6},{2,0},{4,2},{6,4},{1,7},{3,1},{5,3},{7,5},{8,14},{10,8},{12,... | collective-permute-start | bytes 1179656 | tf_op jit(solution)/shard_map/ppermute | solution.py:27
  112.0 29.8 %collective-permute-start.28 = (bf16[96,2048]{1,0:T(8,128)(2,1)S(1)}, bf16[96,2048]{1,0:T(8,128)(2,1)S(1)}, u32[]{:S(2)}, u32[]{:S(2)}) collective-permute-start(bf16[96,2048]{1,0:T(8,128)(2,1)S(1)} %collective-permute-done.25.refs_8_), channel_id=1, source_target_pairs={{0,1},{1,0},{2,3},{3,2},{4,5},{5,4},{6,7},{7,6},{8,9},{9,8},{10,11... | collective-permute-start | bytes 1179656 | tf_op jit(solution)/shard_map/ppermute | solution.py:23
  114.2 36.5 %all-to-all-start.2 = ((bf16[16,8,4352]{2,1,0:T(8,128)(2,1)}), bf16[16,8,4352]{2,1,0:T(8,128)(2,1)S(1)}, u32[]{:S(2)}, u32[]{:S(2)}) async-start(bf16[16,8,4352]{2,1,0:T(8,128)(2,1)} %shard_map.113), calls=%async_computation.2 | async-start | bytes 2228224 | tf_op jit(solution)/shard_map/all_to_all | solution.py:19
  (22 other events, 122.1 us)
